TPU v7x, 256 devices: a whole 4x4x8 slice. The times are simulated.
256 devices in a mesh: ep: 128 (over z, y, x), tp: 2 (over core).
Axes of the slice: x: 4, y: 4, z: 8, core: 2. Of those that a mesh axis runs over, the one named last changes fastest.
Arguments:
- tokens: bfloat16 [512, 2048], P('ep'), may hold values from -6 to 6
- lengths: int32 [512], P('ep'), may hold values from 1 to 1024
- cache_keys: bfloat16 [512, 1024, 512], P('ep', None, 'tp'), may hold values from -640 to 640
- cache_values: bfloat16 [512, 1024, 512], P('ep', None, 'tp'), may hold values from -6 to 6
- norm0_gain: float32 [2048], replicated, may hold values from 0.1 to 1.9
- query_weight: bfloat16 [2048, 1536], P('ep', 'tp'), may hold values from -0.125 to 0.125
- key_weight: bfloat16 [2048, 512], P('ep', 'tp'), may hold values from -0.21875 to 0.21875
- value_weight: bfloat16 [2048, 512], P('ep', 'tp'), may hold values from -0.125 to 0.125
- mix_lambda: float32 [6], P('tp'), may hold values from 0.3 to 0.8
- head_gain: float32 [256], replicated, may hold values from 0.1 to 1.9
- out_weight: bfloat16 [1536, 2048], P('tp', 'ep'), may hold values from -0.15625 to 0.15625
- norm1_gain: float32 [2048], replicated, may hold values from 0.1 to 1.9
- group_ids: int32 [512], P('ep'), may hold values from 0 to 31, as said below
- member_ids: int32 [512, 2], P('ep'), may hold values from 0 to 3, as said below
- group_weight: float32 [512], P('ep'), may hold values from 0.3 to 1
- member_weights: float32 [512, 2], P('ep'), may hold values from 0.2 to 1
- expert_gate: bfloat16 [128, 2048, 512], P('ep', None, 'tp'), may hold values from -0.125 to 0.125
- expert_up: bfloat16 [128, 2048, 512], P('ep', None, 'tp'), may hold values from -0.125 to 0.125
- expert_down: bfloat16 [128, 512, 2048], P('ep', 'tp'), may hold values from -0.25 to 0.25
- norm2_gain: float32 [2048], P('tp'), may hold values from 0.1 to 1.9
Outputs:
- result: bfloat16 [512, 2048], P('ep', 'tp')
Inputs may be any that keep to these rules, and one draw needn't show every extreme that they name: `group_ids`: every group is named by exactly 16 tokens; the 4 tokens of one device name different groups. `member_ids`: A token's 2 members are different; no expert is used by more than 16 tokens, and some expert by exactly 16.
All inputs are finite; a program needn't handle non-finite values.
Results may differ from a plain program's by a relative error of at most 0.015.
Values may be sent and summed in bfloat16 or wider, within the bound.
No kernel may reach another device: no remote copies, remote signals or barrier semaphores. Data moves between devices by JAX's collectives and lax.ppermute only.
A program may use at most 64 MiB of HBM per device.

v0:
```python
import jax
import jax.numpy as jnp
from jax import lax
from jax.sharding import Mesh
from jax.sharding import PartitionSpec as P

EPG = 4
EP = ("ep_0", "ep_1", "ep_2")


ALPHA = 2.0**0.25
EPS = 1e-05


def side_by_side(arrays, axis, dim, along):
    both = jnp.concatenate(arrays, axis=along)
    filled, at, done = (lax.all_gather(both, axis, axis=dim, tiled=True), 0, [])
    for a in arrays:
        done.append(lax.slice_in_dim(filled, at, at + a.shape[along], axis=along))
        at += a.shape[along]
    return tuple(done)


def gather_axes(shard, axes, dim):
    for axis in reversed(axes):
        shard = lax.all_gather(shard, axis, axis=dim, tiled=True)
    return shard


def sent_to_all(shard, axis):
    length = lax.axis_size(axis)
    return lax.all_to_all(
        jnp.broadcast_to(shard[None], (length, *shard.shape)), axis, 0, 0, tiled=True
    )


def of_everyone(shard, axis):
    return sent_to_all(shard, axis).astype(jnp.float32).sum(axis=0)


def in_blocks(shard, dim, length):
    before, after = (shard.shape[:dim], shard.shape[dim + 1 :])
    return jnp.moveaxis(shard.reshape(*before, length, -1, *after), dim, 0)


def sum_at_owner(shard, axis, dim):
    length = lax.axis_size(axis)
    pieces = lax.all_to_all(in_blocks(shard, dim, length), axis, 0, 0, tiled=True)
    return jnp.sum(pieces.astype(jnp.float32), axis=0)


def gathered_total(shard, axis):
    return lax.all_gather(shard, axis).sum(0)


def layer_norm(values, gain):
    mean = jnp.mean(values, -1, keepdims=True)
    spread = jnp.mean(jnp.square(values - mean), -1, keepdims=True)
    return (values - mean) * lax.rsqrt(spread + EPS) * gain


def attend(queries, new_keys, new_values, cache_keys, cache_values, lengths, mix_lambda, head_gain):
    seqs = queries.shape[0]
    span = cache_keys.shape[1]
    vwidth = head_gain.shape[0]
    kv_local = cache_values.shape[2] // vwidth
    hwidth = cache_keys.shape[2] // (2 * kv_local)
    heads_local = mix_lambda.shape[0]
    group = heads_local // kv_local
    query_grid = queries.reshape(seqs, kv_local, group, 2, hwidth)
    cached_keys = cache_keys.reshape(seqs, span, kv_local, 2, hwidth)
    fresh_keys = new_keys.reshape(seqs, kv_local, 2, hwidth)
    cached_values = cache_values.reshape(seqs, span, kv_local, vwidth)
    fresh_values = new_values.reshape(seqs, kv_local, vwidth)
    valid = (jnp.arange(span, dtype=jnp.int32)[None, :] < lengths[:, None])[:, None, None, :]
    scale = hwidth ** (-0.5)
    maps = []
    for which in range(2):
        cached = (
            jnp.einsum(
                "sghd,scgd->sghc",
                query_grid[:, :, :, which],
                cached_keys[:, :, :, which],
                preferred_element_type=jnp.float32,
            )
            * scale
        )
        fresh = (
            jnp.einsum(
                "sghd,sgd->sgh",
                query_grid[:, :, :, which],
                fresh_keys[:, :, which],
                preferred_element_type=jnp.float32,
            )
            * scale
        )
        highest = jnp.maximum(jnp.max(jnp.where(valid, cached, -1e30), -1), fresh)
        spread = jnp.where(valid, jnp.exp(cached - highest[..., None]), 0.0)
        itself = jnp.exp(fresh - highest)
        total = jnp.sum(spread, -1) + itself
        maps.append((spread / total[..., None], itself / total))
    lambdas = mix_lambda.reshape(1, kv_local, group)
    cached_weight = (maps[0][0] - lambdas[..., None] * maps[1][0]).astype(jnp.bfloat16)
    fresh_weight = (maps[0][1] - lambdas * maps[1][1]).astype(jnp.bfloat16)
    head_out = jnp.einsum(
        "sghc,scgv->sghv", cached_weight, cached_values, preferred_element_type=jnp.float32
    )
    head_out = (
        head_out
        + fresh_weight.astype(jnp.float32)[..., None]
        * fresh_values.astype(jnp.float32)[:, :, None, :]
    )
    head_out = (
        head_out * lax.rsqrt(jnp.mean(head_out * head_out, -1, keepdims=True) + EPS) * head_gain
    )
    return head_out.astype(jnp.bfloat16).reshape(seqs, heads_local * vwidth)


def shards(
    tokens,
    lengths,
    cache_keys,
    cache_values,
    norm0_gain,
    query_weight,
    key_weight,
    value_weight,
    mix_lambda,
    head_gain,
    out_weight,
    norm1_gain,
    group_ids,
    member_ids,
    group_weight,
    member_weights,
    expert_gate,
    expert_up,
    expert_down,
    norm2_gain,
):
    width = tokens.shape[1]
    expert_ids = group_ids[:, None] * EPG + member_ids
    share = group_weight[:, None] * member_weights
    normed = layer_norm(tokens.astype(jnp.float32), norm0_gain).astype(jnp.bfloat16)
    query_cols = query_weight.shape[1]
    key_cols = key_weight.shape[1]
    pieces = side_by_side((query_weight, key_weight, value_weight), EP, 0, 1)
    columns = normed
    parts = tuple((jnp.dot(columns, piece, preferred_element_type=jnp.float32) for piece in pieces))
    projected = jnp.concatenate(parts, 1)
    projected = projected.astype(jnp.bfloat16)
    queries = projected[:, :query_cols]
    new_keys = projected[:, query_cols : query_cols + key_cols]
    new_values = projected[:, query_cols + key_cols :]
    attended = attend(
        queries, new_keys, new_values, cache_keys, cache_values, lengths, mix_lambda, head_gain
    )
    partial_mix = jnp.dot(
        attended, gather_axes(out_weight, EP, 1), preferred_element_type=jnp.float32
    )
    mix = (
        of_everyone(partial_mix.astype(jnp.bfloat16), "tp").astype(jnp.float32).astype(jnp.bfloat16)
    )
    stream = (ALPHA * normed.astype(jnp.float32) + mix.astype(jnp.float32)).astype(jnp.bfloat16)
    settled_own = layer_norm(stream.astype(jnp.float32), norm1_gain).astype(jnp.bfloat16)
    experts_all = lax.axis_size(EP)
    targets = lax.iota(jnp.int32, experts_all)
    select = jnp.any(expert_ids[None, :, :] == targets[:, None, None], 2).astype(jnp.bfloat16)
    sending = jnp.dot(select, settled_own, preferred_element_type=jnp.float32).astype(jnp.bfloat16)
    rows = lax.all_to_all(sending, EP, split_axis=0, concat_axis=0, tiled=True)
    gate = jnp.dot(rows, expert_gate[0], preferred_element_type=jnp.float32)
    upward = jnp.dot(rows, expert_up[0], preferred_element_type=jnp.float32)
    hidden = (jax.nn.silu(gate) * upward).astype(jnp.bfloat16)
    output = jnp.dot(hidden, expert_down[0], preferred_element_type=jnp.float32)
    halves = sum_at_owner(output.astype(jnp.bfloat16), "tp", 1)
    returned = lax.all_to_all(
        halves.astype(jnp.bfloat16), EP, split_axis=0, concat_axis=0, tiled=True
    ).astype(halves.dtype)
    columns = lax.iota(jnp.int32, experts_all)
    combine = jnp.sum(
        jnp.where(expert_ids[:, :, None] == columns[None, None, :], share[:, :, None], 0.0), 1
    )
    routed = jnp.dot(combine, returned)
    half = width // lax.axis_size("tp")
    own = lax.dynamic_slice_in_dim(settled_own, lax.axis_index("tp") * half, half, 1)
    mixed = ALPHA * own.astype(jnp.float32) + routed
    first, second = (
        gathered_total(jnp.sum(mixed, 1), "tp"),
        gathered_total(jnp.sum(mixed * mixed, 1), "tp"),
    )
    mean = first / width
    spread = second / width - mean * mean
    result = (mixed - mean[:, None]) * lax.rsqrt(spread[:, None] + EPS) * norm2_gain
    return result.astype(jnp.bfloat16)


def solution(mesh):
    torus = Mesh(mesh.devices.reshape(8, 4, 4, mesh.shape["tp"]), ("ep_0", "ep_1", "ep_2", "tp"))
    return jax.shard_map(
        shards,
        mesh=torus,
        in_specs=(
            P(EP, None),
            P(EP),
            P(EP, None, "tp"),
            P(EP, None, "tp"),
            P(),
            P(EP, "tp"),
            P(EP, "tp"),
            P(EP, "tp"),
            P("tp"),
            P(),
            P("tp", EP),
            P(),
            P(EP),
            P(EP, None),
            P(EP),
            P(EP, None),
            P(EP, None, "tp"),
            P(EP, None, "tp"),
            P(EP, "tp", None),
            P("tp"),
        ),
        out_specs=P(EP, "tp"),
        check_vma=False,
    )
```

profile of v0, /device:TPU:1, one launch (start us, length us, event | category | flops | bytes accessed | tf_op | source)
XLA Modules:
  0.0 267.1 jit_solution(13785300198532340724)
XLA Ops:
  6.6 1.5 pad_maximum_fusion
  8.2 10.4 %all_gather.25 = bf16[768,64]{0,1:T(8,128)(2,1)S(1)} all-gather(bf16[768,16]{0,1:T(8,128)(2,1)} %param.30), channel_id=1, replica_groups=mesh['ep_0'=8,'ep_1'=4,'ep_2'=4,'tp'=2] {'ep_2'}, dimensions={1}, use_global_device_ids=true | all-gather | bytes 122880 | tf_op jit(solution)/shard_map/all_gather | solution.py:26
  18.6 10.9 %all_gather.26 = bf16[768,256]{0,1:T(8,128)(2,1)} all-gather(bf16[768,64]{0,1:T(8,128)(2,1)S(1)} %all_gather.25), channel_id=1, replica_groups=mesh['ep_0'=8,'ep_1'=4,'ep_2'=4,'tp'=2] {'ep_1'}, dimensions={1}, use_global_device_ids=true | all-gather | bytes 491520 | tf_op jit(solution)/shard_map/all_gather | solution.py:26
  29.5 4.0 %copy.62 = bf16[4,1024,256]{1,2,0:T(8,128)(2,1)} copy(bf16[4,1024,256]{2,1,0:T(8,128)(2,1)} %param.22) | data formatting | bytes 4194304 | tf_op args[2]
  34.1 95.2 %all-gather.5.cloned.1.call-done = bf16[2048,1280]{1,0:T(8,128)(2,1)} async-done(((bf16[16,1280]{1,0:T(8,128)(2,1)}), bf16[2048,1280]{1,0:T(8,128)(2,1)}) %all-gather.5.cloned.1.call-update) | async-done | bytes 5242896 | tf_op jit(solution)/shard_map/all_gather | solution.py:17
  129.3 2.4 fusion.4
  131.7 1.5 fusion.8
  133.4 1.6 select_reduce_fusion.1
  135.1 1.6 fusion.31
  136.9 1.5 fusion.7
  138.4 0.5 multiply_reduce_fusion.1
  139.0 36.9 %all-gather.7.cloned.1.call-done = bf16[768,2048]{0,1:T(8,128)(2,1)} async-done(((bf16[768,256]{0,1:T(8,128)(2,1)}), bf16[768,2048]{0,1:T(8,128)(2,1)}) %all-gather.7.cloned.1.call-update) | async-done | bytes 3145744 | tf_op jit(solution)/shard_map/all_gather | solution.py:26
  176.0 2.8 %convolution_convert_fusion.2 = bf16[4,2048]{1,0:T(4,128)(2,1)S(1)} fusion(bf16[4,768]{1,0:T(4,128)(2,1)S(1)} %bitcast.89, bf16[768,2048]{0,1:T(8,128)(2,1)} %all-gather.7.cloned.1.call-done), kind=kOutput, calls=%fused_computation.5 | convolution fusion | flops 12591104 | bytes 3168256 | tf_op jit(solution)/shard_map/dot_general | solution.py:158
  178.8 4.6 %all_to_all.34 = bf16[2,4,2048]{2,1,0:T(4,128)(2,1)S(1)} all-to-all(bf16[2,4,2048]{2,1,0:T(4,128)(2,1)S(1)} %broadcast_in_dim.39), channel_id=1, replica_groups=mesh['ep_0'=8,'ep_1'=4,'ep_2'=4,'tp'=2] {'tp'}, dimensions={0} | all-to-all | bytes 65536 | tf_op jit(solution)/shard_map/all_to_all | solution.py:32
  184.0 0.4 fusion.2
  184.3 0.5 broadcast.197
  184.8 1.0 reduce.12
  185.8 0.4 reshape.250
  186.2 29.9 %all_to_all.35 = bf16[128,2,1024]{2,1,0:T(2,128)(2,1)} all-to-all(bf16[128,2,1024]{2,1,0:T(2,128)(2,1)S(1)} %reshape.250), channel_id=1, replica_groups=mesh['ep_0'=8,'ep_1'=4,'ep_2'=4,'tp'=2] {'ep_0','ep_1','ep_2'}, dimensions={0} | all-to-all | bytes 1048576 | tf_op jit(solution)/shard_map/all_to_all | solution.py:170
  216.1 3.6 %reshape.251 = bf16[128,1,2048]{2,1,0:T(2,128)(2,1)S(1)} reshape(bf16[128,2,1024]{2,1,0:T(2,128)(2,1)} %all_to_all.35) | data formatting | bytes 1048576
  219.7 1.7 fusion.14
  221.4 3.2 %convolution_convert_fusion = bf16[128,2048]{1,0:T(8,128)(2,1)} fusion(bf16[1,256,2048]{2,1,0:T(8,128)(2,1)} %param.38, bf16[1,2048,256]{2,1,0:T(8,128)(2,1)} %param.37, bf16[128,1,2048]{2,1,0:T(2,128)(2,1)S(1)} %reshape.251, f32[128,256]{1,0:T(8,128)S(1)} %fusion.14), kind=kOutput, calls=%fused_computation.2 | convolution fusion | flops 268894208 | bytes 3276800 | tf_op jit(solution)/shard_map/dot_general | solution.py:174
  224.6 1.1 copy.113
  225.7 6.5 %all_to_all.36 = bf16[2,128,1024]{2,1,0:T(8,128)(2,1)S(1)} all-to-all(bf16[2,128,1024]{2,1,0:T(8,128)(2,1)S(1)} %bitcast.87), channel_id=1, replica_groups=mesh['ep_0'=8,'ep_1'=4,'ep_2'=4,'tp'=2] {'tp'}, dimensions={0} | all-to-all | bytes 1048576 | tf_op jit(solution)/shard_map/all_to_all | solution.py:48
  232.3 0.8 reduce.13
  233.1 0.9 reshape.252
  234.0 6.2 %all-to-all-start.3 = ((bf16[128,2,512]{2,1,0:T(2,128)(2,1)}), bf16[128,2,512]{2,1,0:T(2,128)(2,1)S(1)}, u32[]{:S(2)}, u32[]{:S(2)}) async-start(bf16[128,2,512]{2,1,0:T(2,128)(2,1)} %reshape.252), calls=%async_computation.3 | async-start | bytes 524288 | tf_op jit(solution)/shard_map/all_to_all | solution.py:176
  240.2 0.6 dynamic-slice
  241.5 12.6 %all-to-all-done.3 = bf16[128,2,512]{2,1,0:T(2,128)(2,1)S(1)} async-done(((bf16[128,2,512]{2,1,0:T(2,128)(2,1)}), bf16[128,2,512]{2,1,0:T(2,128)(2,1)S(1)}, u32[]{:S(2)}, u32[]{:S(2)}) %all-to-all-start.3) | async-done | bytes 262176 | tf_op jit(solution)/shard_map/all_to_all | solution.py:176
  254.3 0.3 fusion.62
  255.1 4.2 %all-reduce.2 = (f32[8]{0:T(128)S(1)}, f32[8]{0:T(128)S(1)}) all-reduce(f32[8]{0:T(128)S(1)} %dynamic-update-slice.1, f32[8]{0:T(128)S(1)} %dynamic-update-slice), channel_id=3, replica_groups=mesh['ep_0'=8,'ep_1'=4,'ep_2'=4,'tp'=2] {'tp'}, use_global_device_ids=true, to_apply=%add.1 | all-reduce | flops 16 | bytes 128
  259.6 0.7 multiply_convert_fusion
  (70 shorter events, 2.9 us)
Async XLA Ops:
  6.5 131.8 %copy-start = (bf16[4,1024,256]{2,1,0:T(8,128)(2,1)S(1)}, bf16[4,1024,256]{2,1,0:T(8,128)(2,1)}, u32[]{:S(2)}) copy-start(bf16[4,1024,256]{2,1,0:T(8,128)(2,1)} %param.23) | copy-start | bytes 6291460
  6.5 27.0 %copy-start.1 = (bf16[4,2048]{1,0:T(4,128)(2,1)S(1)}, bf16[4,2048]{1,0:T(4,128)(2,1)}, u32[]{:S(2)}) copy-start(bf16[4,2048]{1,0:T(4,128)(2,1)} %param.20) | copy-start | bytes 49156
  6.5 27.1 %copy-start.11 = (s32[4]{0:T(128)S(1)}, s32[4]{0:T(128)}, u32[]{:S(2)}) copy-start(s32[4]{0:T(128)} %param.32) | copy-start | bytes 52
  6.5 27.1 %copy-start.6 = (s32[4,2]{0,1:T(2,128)S(1)}, s32[4,2]{0,1:T(2,128)}, u32[]{:S(2)}) copy-start(s32[4,2]{0,1:T(2,128)} %param.33) | copy-start | bytes 100
  6.5 27.4 %copy-start.8 = (s32[4]{0:T(128)S(1)}, s32[4]{0:T(128)}, u32[]{:S(2)}) copy-start(s32[4]{0:T(128)} %param.21) | copy-start | bytes 52
  6.5 122.7 %copy-start.2 = (f32[2048]{0:T(1024)S(1)}, f32[2048]{0:T(1024)}, u32[]{:S(2)}) copy-start(f32[2048]{0:T(1024)} %param.24) | copy-start | bytes 24580
  6.6 122.7 %all-gather.5.cloned.1.call-start = ((), (), s32[]{:S(2)}) async-start(), calls=%async_computation.4 | async-start | bytes 5283840 | tf_op jit(solution)/shard_map/all_gather | solution.py:17
  8.2 167.8 %all-gather.7.cloned.1.call-start = ((), (), s32[]{:S(2)}) async-start(), calls=%async_computation.5 | async-start | bytes 3538944 | tf_op jit(solution)/shard_map/all_gather | solution.py:26
  34.1 102.8 %copy-start.9 = (f32[3]{0:T(128)S(1)}, f32[3]{0:T(128)}, u32[]{:S(2)}) copy-start(f32[3]{0:T(128)} %param.28) | copy-start | bytes 40
  133.2 5.7 %copy-start.5 = (f32[256]{0:T(256)S(1)}, f32[256]{0:T(256)}, u32[]{:S(2)}) copy-start(f32[256]{0:T(256)} %param.29) | copy-start | bytes 3076
  138.4 45.5 %copy-start.3 = (f32[2048]{0:T(1024)S(1)}, f32[2048]{0:T(1024)}, u32[]{:S(2)}) copy-start(f32[2048]{0:T(1024)} %param.31) | copy-start | bytes 24580
  221.4 18.8 %copy-start.12 = (u32[256]{0:T(256)S(1)}, u32[256]{0:T(256)}, u32[]{:S(2)}) copy-start(u32[256]{0:T(256)} %constant.65) | copy-start | bytes 3076
  221.4 20.0 %copy-start.7 = (f32[4,2]{0,1:T(2,128)S(1)}, f32[4,2]{0,1:T(2,128)}, u32[]{:S(2)}) copy-start(f32[4,2]{0,1:T(2,128)} %param.35) | copy-start | bytes 100
  221.4 20.0 %copy-start.10 = (f32[4]{0:T(128)S(1)}, f32[4]{0:T(128)}, u32[]{:S(2)}) copy-start(f32[4]{0:T(128)} %param.34) | copy-start | bytes 52
  224.6 35.0 %copy-start.4 = (f32[1024]{0:T(1024)S(1)}, f32[1024]{0:T(1024)}, u32[]{:S(2)}) copy-start(f32[1024]{0:T(1024)} %param.39) | copy-start | bytes 12292
  234.0 20.1 %all-to-all-start.3 = ((bf16[128,2,512]{2,1,0:T(2,128)(2,1)}), bf16[128,2,512]{2,1,0:T(2,128)(2,1)S(1)}, u32[]{:S(2)}, u32[]{:S(2)}) async-start(bf16[128,2,512]{2,1,0:T(2,128)(2,1)} %reshape.252), calls=%async_computation.3 | async-start | bytes 524288 | tf_op jit(solution)/shard_map/all_to_all | solution.py:176
Sparse Core Ops, SparseCore 0:
  11.0 118.2 all-gather.4
  131.0 44.8 all-gather.6
where the time goes:
time: 268 us; the launch traced here: 267 us
  waiting for transfers between devices  145 us (54%)
  blocking collectives  66.6 us (25%)
  matrix products  17.7 us (7%)
  between operations  14.3 us (5%)
  local copies, waits for them, and re-layouts  11.9 us (4%)
  starting transfers between devices  6.25 us (2%)
  other arithmetic  5.57 us (2%)
    all_gather x1, waiting for transfers between devices, side_by_side(): filled, at, done = (lax.all_gather(both, axis, axis=dim, tiled=True), 0, [])  95.2 us
    all_gather x1, waiting for transfers between devices, gather_axes(): shard = lax.all_gather(shard, axis, axis=dim, tiled=True)  36.9 us
    all_to_all x1, blocking collectives, shards(): rows = lax.all_to_all(sending, EP, split_axis=0, concat_axis=0, tiled=True)  29.9 us
    all_gather x2, blocking collectives, gather_axes(): shard = lax.all_gather(shard, axis, axis=dim, tiled=True)  21.3 us
    all_to_all x1, waiting for transfers between devices, shards(): lax.all_to_all(halves.astype(jnp.bfloat16), EP, split_axis=0, concat_axis...  12.6 us
    unnamed x37, local copies, waits for them, and re-layouts  10.1 us
    all_to_all x1, blocking collectives, sum_at_owner(): lax.all_to_all(in_blocks(shard, dim, length), axis, 0, 0, tiled=True)  6.55 us
    all_to_all x1, starting transfers between devices, shards(): lax.all_to_all(halves.astype(jnp.bfloat16), EP, split_axis=0, concat_axis...  6.17 us
  transfers between devices with their start and end apart: 3, of which 3 were waited for; matrix products, arithmetic and copies ran while one was open for 6% of the time, Pallas kernels for 0%

commit v1 on v0

--- a/solution.py
+++ b/solution.py
@@ -5,52 +5,19 @@
 from jax.sharding import PartitionSpec as P
 
 EPG = 4
-EP = ("ep_0", "ep_1", "ep_2")
-
+EP = ("z", "y", "x")
+ROW = ("y", "x")
 
 ALPHA = 2.0**0.25
 EPS = 1e-05
 
 
-def side_by_side(arrays, axis, dim, along):
-    both = jnp.concatenate(arrays, axis=along)
-    filled, at, done = (lax.all_gather(both, axis, axis=dim, tiled=True), 0, [])
-    for a in arrays:
-        done.append(lax.slice_in_dim(filled, at, at + a.shape[along], axis=along))
-        at += a.shape[along]
-    return tuple(done)
-
-
-def gather_axes(shard, axes, dim):
-    for axis in reversed(axes):
-        shard = lax.all_gather(shard, axis, axis=dim, tiled=True)
-    return shard
-
-
-def sent_to_all(shard, axis):
-    length = lax.axis_size(axis)
-    return lax.all_to_all(
-        jnp.broadcast_to(shard[None], (length, *shard.shape)), axis, 0, 0, tiled=True
-    )
-
-
-def of_everyone(shard, axis):
-    return sent_to_all(shard, axis).astype(jnp.float32).sum(axis=0)
-
-
-def in_blocks(shard, dim, length):
-    before, after = (shard.shape[:dim], shard.shape[dim + 1 :])
-    return jnp.moveaxis(shard.reshape(*before, length, -1, *after), dim, 0)
-
-
-def sum_at_owner(shard, axis, dim):
-    length = lax.axis_size(axis)
-    pieces = lax.all_to_all(in_blocks(shard, dim, length), axis, 0, 0, tiled=True)
-    return jnp.sum(pieces.astype(jnp.float32), axis=0)
-
-
-def gathered_total(shard, axis):
-    return lax.all_gather(shard, axis).sum(0)
+def swap(array, axis):
+    return lax.all_to_all(array, axis, 0, 0, tiled=True)
+
+
+def to_all(array, axis):
+    return swap(jnp.broadcast_to(array[None], (lax.axis_size(axis), *array.shape)), axis)
 
 
 def layer_norm(values, gain):
@@ -138,64 +105,78 @@
     expert_down,
     norm2_gain,
 ):
-    width = tokens.shape[1]
+    seqs, width = tokens.shape
+    deep = lax.axis_size("z")
+    experts = lax.axis_size(EP)
+    halves = lax.axis_size("tp")
+    half = width // halves
+    block = width // deep
+    query_cols = query_weight.shape[1]
+    key_cols = key_weight.shape[1]
+    value_cols = value_weight.shape[1]
+    proj_cols = query_cols + key_cols + value_cols
     expert_ids = group_ids[:, None] * EPG + member_ids
     share = group_weight[:, None] * member_weights
+
+    own_weights = jnp.concatenate((query_weight, key_weight, value_weight, out_weight.T), 1)
+    weights = to_all(own_weights, ROW).reshape(block, -1)
+    weight_in = weights[:, :proj_cols]
+    weight_out = weights[:, proj_cols:]
+
     normed = layer_norm(tokens.astype(jnp.float32), norm0_gain).astype(jnp.bfloat16)
-    query_cols = query_weight.shape[1]
-    key_cols = key_weight.shape[1]
-    pieces = side_by_side((query_weight, key_weight, value_weight), EP, 0, 1)
-    columns = normed
-    parts = tuple((jnp.dot(columns, piece, preferred_element_type=jnp.float32) for piece in pieces))
-    projected = jnp.concatenate(parts, 1)
-    projected = projected.astype(jnp.bfloat16)
+    columns = swap(normed.reshape(seqs, deep, block).transpose(1, 0, 2), "z")
+    partial = jnp.dot(
+        columns.reshape(deep * seqs, block), weight_in, preferred_element_type=jnp.float32
+    )
+    projected = jnp.sum(swap(partial.reshape(deep, seqs, proj_cols), "z"), 0).astype(jnp.bfloat16)
     queries = projected[:, :query_cols]
     new_keys = projected[:, query_cols : query_cols + key_cols]
     new_values = projected[:, query_cols + key_cols :]
     attended = attend(
         queries, new_keys, new_values, cache_keys, cache_values, lengths, mix_lambda, head_gain
     )
-    partial_mix = jnp.dot(
-        attended, gather_axes(out_weight, EP, 1), preferred_element_type=jnp.float32
-    )
-    mix = (
-        of_everyone(partial_mix.astype(jnp.bfloat16), "tp").astype(jnp.float32).astype(jnp.bfloat16)
-    )
+    everyone = to_all(attended, "z").reshape(deep * seqs, -1)
+    partial_mix = lax.dot_general(
+        everyone, weight_out, (((1,), (1,)), ((), ())), preferred_element_type=jnp.float32
+    ).astype(jnp.bfloat16)
+    doubled = jnp.broadcast_to(
+        partial_mix.reshape(deep, 1, seqs, block), (deep, halves, seqs, block)
+    )
+    back = swap(doubled.reshape(deep * halves, seqs, block), ("z", "tp"))
+    mix = jnp.sum(back.astype(jnp.float32).reshape(deep, halves, seqs, block), 1)
+    mix = mix.transpose(1, 0, 2).reshape(seqs, width).astype(jnp.bfloat16)
     stream = (ALPHA * normed.astype(jnp.float32) + mix.astype(jnp.float32)).astype(jnp.bfloat16)
-    settled_own = layer_norm(stream.astype(jnp.float32), norm1_gain).astype(jnp.bfloat16)
-    experts_all = lax.axis_size(EP)
-    targets = lax.iota(jnp.int32, experts_all)
-    select = jnp.any(expert_ids[None, :, :] == targets[:, None, None], 2).astype(jnp.bfloat16)
-    sending = jnp.dot(select, settled_own, preferred_element_type=jnp.float32).astype(jnp.bfloat16)
-    rows = lax.all_to_all(sending, EP, split_axis=0, concat_axis=0, tiled=True)
+    settled = layer_norm(stream.astype(jnp.float32), norm1_gain).astype(jnp.bfloat16)
+
+    targets = lax.iota(jnp.int32, experts)
+    select = jnp.any(expert_ids[None, :, :] == targets[:, None, None], 2)
+    tiles = settled.reshape(1, seqs, width // 128, 128)
+    sending = jnp.sum(
+        jnp.where(select[:, :, None, None], tiles, jnp.zeros_like(tiles)).astype(jnp.float32), 1
+    ).astype(jnp.bfloat16)
+    rows = swap(sending, EP).reshape(experts, width)
     gate = jnp.dot(rows, expert_gate[0], preferred_element_type=jnp.float32)
     upward = jnp.dot(rows, expert_up[0], preferred_element_type=jnp.float32)
     hidden = (jax.nn.silu(gate) * upward).astype(jnp.bfloat16)
     output = jnp.dot(hidden, expert_down[0], preferred_element_type=jnp.float32)
-    halves = sum_at_owner(output.astype(jnp.bfloat16), "tp", 1)
-    returned = lax.all_to_all(
-        halves.astype(jnp.bfloat16), EP, split_axis=0, concat_axis=0, tiled=True
-    ).astype(halves.dtype)
-    columns = lax.iota(jnp.int32, experts_all)
+    output = output.astype(jnp.bfloat16).reshape(experts * halves, half // 128, 128)
+    returned = swap(output, EP + ("tp",)).reshape(experts, halves, half // 128, 128)
+    both = jnp.sum(returned.astype(jnp.float32), 1)
     combine = jnp.sum(
-        jnp.where(expert_ids[:, :, None] == columns[None, None, :], share[:, :, None], 0.0), 1
-    )
-    routed = jnp.dot(combine, returned)
-    half = width // lax.axis_size("tp")
-    own = lax.dynamic_slice_in_dim(settled_own, lax.axis_index("tp") * half, half, 1)
+        jnp.where(expert_ids[:, :, None] == targets[None, None, :], share[:, :, None], 0.0), 1
+    )
+    routed = jnp.sum(combine[:, :, None, None] * both[None], 1).reshape(seqs, half)
+    own = lax.dynamic_slice_in_dim(settled, lax.axis_index("tp") * half, half, 1)
     mixed = ALPHA * own.astype(jnp.float32) + routed
-    first, second = (
-        gathered_total(jnp.sum(mixed, 1), "tp"),
-        gathered_total(jnp.sum(mixed * mixed, 1), "tp"),
-    )
-    mean = first / width
-    spread = second / width - mean * mean
+    sums = lax.psum(jnp.stack((jnp.sum(mixed, 1), jnp.sum(mixed * mixed, 1))), "tp")
+    mean = sums[0] / width
+    spread = sums[1] / width - mean * mean
     result = (mixed - mean[:, None]) * lax.rsqrt(spread[:, None] + EPS) * norm2_gain
     return result.astype(jnp.bfloat16)
 
 
 def solution(mesh):
-    torus = Mesh(mesh.devices.reshape(8, 4, 4, mesh.shape["tp"]), ("ep_0", "ep_1", "ep_2", "tp"))
+    torus = Mesh(mesh.devices.reshape(8, 4, 4, mesh.shape["tp"]), ("z", "y", "x", "tp"))
     return jax.shard_map(
         shards,
         mesh=torus,

time: 268 us -> 150 us (0.56)
  waiting for transfers between devices: 145 us -> 43.9 us
  starting transfers between devices: 6.25 us -> 31.8 us
  blocking collectives: 66.6 us -> 49.9 us
  between operations: 14.3 us -> 0.31 us
  matrix products: 17.7 us -> 8.88 us
  local copies, waits for them, and re-layouts: 11.9 us -> 6.71 us
    all_gather x2 -> x0, waiting for transfers between devices: 132 us -> none  [the longest x1 95.2 us: side_by_side(): filled, at, done = (lax.all_gather(both, axis, axis=dim, tiled=True), 0, [])]
    all_to_all x1 -> x5, waiting for transfers between devices: 12.6 us -> 43.9 us  [swap(): return lax.all_to_all(array, axis, 0, 0, tiled=True)]
    all_to_all x1 -> x5, starting transfers between devices: 6.17 us -> 31.8 us  [swap(): return lax.all_to_all(array, axis, 0, 0, tiled=True)]
    all_gather x2 -> x0, blocking collectives: 21.3 us -> none  [gather_axes(): shard = lax.all_gather(shard, axis, axis=dim, tiled=True)]
    dot_general x6 -> x2, matrix products: 8.96 us -> 1.12 us  [the longest x1 0.91 us: shards(): jnp.dot(columns.reshape(deep * seqs, block), weight_in, preferred_element...]
    unnamed x37 -> x28, local copies, waits for them, and re-layouts: 10.1 us -> 4.09 us
    all_to_all x3 -> x2, blocking collectives: 41.1 us -> 46.9 us  [swap(): return lax.all_to_all(array, axis, 0, 0, tiled=True)]
    unnamed x1 -> x0, blocking collectives: 4.24 us -> none
  transfers between devices with their start and end apart: 3 -> 5, of which waited for: 3 -> 5; matrix products, arithmetic and copies ran while one was open for 6% -> 4% of each run, Pallas kernels for 0% -> 0%
where the time goes in v1:
time: 150 us
  blocking collectives  49.9 us (33%)
  waiting for transfers between devices  43.9 us (29%)
  starting transfers between devices  31.8 us (21%)
  matrix products  8.88 us (6%)
  other arithmetic  8 us (5%)
  local copies, waits for them, and re-layouts  6.71 us (4%)
    all_to_all x2, blocking collectives, swap(): return lax.all_to_all(array, axis, 0, 0, tiled=True)  46.9 us
    all_to_all x5, waiting for transfers between devices, swap(): return lax.all_to_all(array, axis, 0, 0, tiled=True)  43.9 us
    all_to_all x5, starting transfers between devices, swap(): return lax.all_to_all(array, axis, 0, 0, tiled=True)  31.8 us
    unnamed x28, local copies, waits for them, and re-layouts  4.09 us
    dot_general x2, matrix products, attend(): jnp.einsum('sghd,scgd->sghc', query_grid[:, :, :, which], cached_keys[:,...  3.14 us
    psum x1, blocking collectives, shards(): lax.psum(jnp.stack((jnp.sum(mixed, 1), jnp.sum(mixed * mixed, 1))), 'tp')  3.04 us
  transfers between devices with their start and end apart: 5, of which 5 were waited for; matrix products, arithmetic and copies ran while one was open for 4% of the time, Pallas kernels for 0%

profile of v1, /device:TPU:1, one launch (start us, length us, event | category | flops | bytes accessed | tf_op | source)
XLA Modules:
  0.0 149.5 jit_solution(3451434910616258476)
XLA Ops:
  0.0 1.0 convert_reduce_fusion.2
  1.0 0.9 fusion.31
  1.9 1.4 fusion.33
  3.3 9.0 %all-to-all-start = ((bf16[8,4,256]{2,1,0:T(4,128)(2,1)}), bf16[8,4,256]{2,1,0:T(4,128)(2,1)S(1)}, u32[]{:S(2)}, u32[]{:S(2)}) async-start(bf16[8,4,256]{2,1,0:T(4,128)(2,1)} %bitcast.1), calls=%async_computation | async-start | bytes 32768 | tf_op jit(solution)/shard_map/all_to_all | solution.py:16
  12.3 0.8 pad_maximum_fusion
  13.1 5.8 %all-to-all-done = bf16[8,4,256]{2,1,0:T(4,128)(2,1)S(1)} async-done(((bf16[8,4,256]{2,1,0:T(4,128)(2,1)}), bf16[8,4,256]{2,1,0:T(4,128)(2,1)S(1)}, u32[]{:S(2)}, u32[]{:S(2)}) %all-to-all-start) | async-done | bytes 16416 | tf_op jit(solution)/shard_map/all_to_all | solution.py:16
  19.1 22.2 %all_to_all.35 = bf16[16,16,2048]{2,1,0:T(8,128)(2,1)S(1)} all-to-all(bf16[16,16,2048]{2,1,0:T(8,128)(2,1)S(1)} %broadcast_in_dim.116), channel_id=1, replica_groups=mesh['z'=8,'y'=4,'x'=4,'tp'=2] {'y','x'}, dimensions={0} | all-to-all | bytes 2097152 | tf_op jit(solution)/shard_map/all_to_all | solution.py:16
  41.3 0.9 fusion.6
  42.2 3.4 %all-to-all-start.2 = ((f32[8,4,1280]{2,1,0:T(4,128)}), f32[8,4,1280]{2,1,0:T(4,128)S(1)}, u32[]{:S(2)}, u32[]{:S(2)}) async-start(f32[8,4,1280]{2,1,0:T(4,128)} %fusion.6), calls=%async_computation.2 | async-start | bytes 327680 | tf_op jit(solution)/shard_map/all_to_all | solution.py:16
  45.6 4.0 %copy.53 = bf16[4,1024,256]{1,2,0:T(8,128)(2,1)} copy(bf16[4,1024,256]{2,1,0:T(8,128)(2,1)} %param.22) | data formatting | bytes 4194304 | tf_op args[2]
  49.7 4.1 %all-to-all-done.2 = f32[8,4,1280]{2,1,0:T(4,128)S(1)} async-done(((f32[8,4,1280]{2,1,0:T(4,128)}), f32[8,4,1280]{2,1,0:T(4,128)S(1)}, u32[]{:S(2)}, u32[]{:S(2)}) %all-to-all-start.2) | async-done | bytes 163872 | tf_op jit(solution)/shard_map/all_to_all | solution.py:16
  53.9 1.6 %select_reduce_fusion.2 = (f32[4,3]{1,0:T(4,128)S(1)}, f32[4,3,1024]{2,1,0:T(4,128)S(1)}) fusion(pred[4,1024]{1,0:T(4,128)(4,1)S(1)} %iota_compare_fusion, bf16[4,1024,1,2,128]{1,4,3,0,2:T(8,128)(2,1)} %bitcast.111, bf16[4,1,3,1,128]{4,0,3,2,1:T(4,128)(2,1)S(1)} %get-tuple-element.17), kind=kOutput, calls=%fused_computation.34 | convolution fusion | flops 3182580 | bytes 1104944 | tf_op jit(solution)/shard_map/sghd,scgd->sghc/dot_general | solution.py:47
  55.6 1.6 %fusion.21 = (f32[4,3]{1,0:T(4,128)S(1)}, f32[4,3]{1,0:T(4,128)S(1)}, f32[4,3,1024]{2,1,0:T(4,128)S(1)}) fusion(f32[4,3,1024]{2,1,0:T(4,128)S(1)} %get-tuple-element.21, f32[4,3]{1,0:T(4,128)S(1)} %multiply_maximum_fusion.1, pred[4,1024]{1,0:T(4,128)(4,1)S(1)} %iota_compare_fusion, bf16[4,1024,1,2,128]{1,4,3,0,2:T(8,128)(2,1)} %bitcast.112, ...), kind=kOutput, calls=%fused_computation.36 | convolution fusion | flops 3219432 | bytes 1154192 | tf_op jit(solution)/shard_map/sghd,scgd->sghc/dot_general | solution.py:47
  57.4 0.5 multiply_reduce_fusion.2
  58.1 0.6 broadcast_in_dim.120
  58.7 3.3 %all-to-all-start.3 = ((bf16[8,4,768]{2,1,0:T(4,128)(2,1)}), bf16[8,4,768]{2,1,0:T(4,128)(2,1)S(1)}, u32[]{:S(2)}, u32[]{:S(2)}) async-start(bf16[8,4,768]{2,1,0:T(4,128)(2,1)} %broadcast_in_dim.120), calls=%async_computation.3 | async-start | bytes 98304 | tf_op jit(solution)/shard_map/all_to_all | solution.py:16
  62.1 6.9 %all-to-all-done.3 = bf16[8,4,768]{2,1,0:T(4,128)(2,1)S(1)} async-done(((bf16[8,4,768]{2,1,0:T(4,128)(2,1)}), bf16[8,4,768]{2,1,0:T(4,128)(2,1)S(1)}, u32[]{:S(2)}, u32[]{:S(2)}) %all-to-all-start.3) | async-done | bytes 49184 | tf_op jit(solution)/shard_map/all_to_all | solution.py:16
  69.1 0.2 convolution_convert_fusion.1
  69.3 0.6 broadcast_in_dim.122
  70.0 8.5 %all-to-all-start.4 = ((bf16[16,4,256]{2,1,0:T(4,128)(2,1)}), bf16[16,4,256]{2,1,0:T(4,128)(2,1)S(1)}, u32[]{:S(2)}, u32[]{:S(2)}) async-start(bf16[16,4,256]{2,1,0:T(4,128)(2,1)} %bitcast.20), calls=%async_computation.4 | async-start | bytes 65536 | tf_op jit(solution)/shard_map/all_to_all | solution.py:16
  78.7 7.3 %all-to-all-done.4 = bf16[16,4,256]{2,1,0:T(4,128)(2,1)S(1)} async-done(((bf16[16,4,256]{2,1,0:T(4,128)(2,1)}), bf16[16,4,256]{2,1,0:T(4,128)(2,1)S(1)}, u32[]{:S(2)}, u32[]{:S(2)}) %all-to-all-start.4) | async-done | bytes 32800 | tf_op jit(solution)/shard_map/all_to_all | solution.py:16
  86.1 0.2 convert_reduce_fusion.1
  86.6 1.0 select_reduce_fusion
  87.6 24.7 %all_to_all.36 = bf16[128,16,128]{2,1,0:T(8,128)(2,1)S(1)} all-to-all(bf16[128,16,128]{2,1,0:T(8,128)(2,1)S(1)} %select_reduce_fusion), channel_id=1, replica_groups=mesh['z'=8,'y'=4,'x'=4,'tp'=2] {'z','y','x'}, dimensions={0} | all-to-all | bytes 1048576 | tf_op jit(solution)/shard_map/all_to_all | solution.py:16
  112.3 1.5 %fusion.4 = f32[128,256]{1,0:T(8,128)S(1)} fusion(bf16[1,2048,256]{2,1,0:T(8,128)(2,1)} %param.36, bf16[16,8,16,128]{3,2,1,0:T(8,128)(2,1)S(1)} %bitcast.107), kind=kOutput, calls=%fused_computation.14 | convolution fusion | flops 134217728 | bytes 1703936 | tf_op jit(solution)/shard_map/dot_general | solution.py:158
  113.8 2.3 %convolution_convert_fusion = bf16[128,2048]{1,0:T(8,128)(2,1)S(1)} fusion(bf16[1,256,2048]{2,1,0:T(8,128)(2,1)} %param.38, bf16[1,2048,256]{2,1,0:T(8,128)(2,1)} %param.37, bf16[16,8,16,128]{3,2,1,0:T(8,128)(2,1)S(1)} %bitcast.108, f32[128,256]{1,0:T(8,128)S(1)} %fusion.4), kind=kOutput, calls=%fused_computation | convolution fusion | flops 268894208 | bytes 3276800 | tf_op jit(solution)/shard_map/dot_general | solution.py:161
  116.2 1.0 reshape.284
  117.2 7.5 %all-to-all-start.6 = ((bf16[256,8,128]{2,1,0:T(8,128)(2,1)}), bf16[256,8,128]{2,1,0:T(8,128)(2,1)S(1)}, u32[]{:S(2)}, u32[]{:S(2)}) async-start(bf16[256,8,128]{2,1,0:T(8,128)(2,1)} %reshape.284), calls=%async_computation.6 | async-start | bytes 1048576 | tf_op jit(solution)/shard_map/all_to_all | solution.py:16
  124.9 19.8 %all-to-all-done.6 = bf16[256,8,128]{2,1,0:T(8,128)(2,1)S(1)} async-done(((bf16[256,8,128]{2,1,0:T(8,128)(2,1)}), bf16[256,8,128]{2,1,0:T(8,128)(2,1)S(1)}, u32[]{:S(2)}, u32[]{:S(2)}) %all-to-all-start.6) | async-done | bytes 524320 | tf_op jit(solution)/shard_map/all_to_all | solution.py:16
  144.9 0.7 multiply_reduce_fusion
  145.8 3.0 %psum.7 = f32[2,4]{1,0:T(2,128)S(1)} all-reduce(f32[2,4]{1,0:T(2,128)S(1)} %pad_maximum_fusion.1), channel_id=1, replica_groups=mesh['z'=8,'y'=4,'x'=4,'tp'=2] {'tp'}, use_global_device_ids=true, to_apply=%region_18.19 | all-reduce | flops 8 | bytes 64 | tf_op jit(solution)/shard_map/psum | solution.py:171
  148.8 0.7 multiply_convert_fusion
  (64 shorter events, 2.0 us)
Async XLA Ops:
  0.0 57.4 %copy-start = (bf16[4,1024,256]{2,1,0:T(8,128)(2,1)S(1)}, bf16[4,1024,256]{2,1,0:T(8,128)(2,1)}, u32[]{:S(2)}) copy-start(bf16[4,1024,256]{2,1,0:T(8,128)(2,1)} %param.23) | copy-start | bytes 6291460
  3.3 15.6 %all-to-all-start = ((bf16[8,4,256]{2,1,0:T(4,128)(2,1)}), bf16[8,4,256]{2,1,0:T(4,128)(2,1)S(1)}, u32[]{:S(2)}, u32[]{:S(2)}) async-start(bf16[8,4,256]{2,1,0:T(4,128)(2,1)} %bitcast.1), calls=%async_computation | async-start | bytes 32768 | tf_op jit(solution)/shard_map/all_to_all | solution.py:16
  13.1 32.4 %copy-start.11 = (s32[4]{0:T(128)S(1)}, s32[4]{0:T(128)}, u32[]{:S(2)}) copy-start(s32[4]{0:T(128)} %param.32) | copy-start | bytes 52
  42.2 11.6 %all-to-all-start.2 = ((f32[8,4,1280]{2,1,0:T(4,128)}), f32[8,4,1280]{2,1,0:T(4,128)S(1)}, u32[]{:S(2)}, u32[]{:S(2)}) async-start(f32[8,4,1280]{2,1,0:T(4,128)} %fusion.6), calls=%async_computation.2 | async-start | bytes 327680 | tf_op jit(solution)/shard_map/all_to_all | solution.py:16
  45.6 4.0 %copy-start.8 = (s32[4]{0:T(128)S(1)}, s32[4]{0:T(128)}, u32[]{:S(2)}) copy-start(s32[4]{0:T(128)} %param.21) | copy-start | bytes 52
  49.6 7.8 %copy-start.9 = (f32[3]{0:T(128)S(1)}, f32[3]{0:T(128)}, u32[]{:S(2)}) copy-start(f32[3]{0:T(128)} %param.28) | copy-start | bytes 40
  55.5 2.5 %copy-start.5 = (f32[256]{0:T(256)S(1)}, f32[256]{0:T(256)}, u32[]{:S(2)}) copy-start(f32[256]{0:T(256)} %param.29) | copy-start | bytes 3076
  55.5 6.6 %copy-start.6 = (s32[4,2]{0,1:T(2,128)S(1)}, s32[4,2]{0,1:T(2,128)}, u32[]{:S(2)}) copy-start(s32[4,2]{0,1:T(2,128)} %param.33) | copy-start | bytes 100
  57.2 28.8 %copy-start.1 = (bf16[4,2048]{1,0:T(4,128)(2,1)S(1)}, bf16[4,2048]{1,0:T(4,128)(2,1)}, u32[]{:S(2)}) copy-start(bf16[4,2048]{1,0:T(4,128)(2,1)} %param.20) | copy-start | bytes 49156
  57.2 28.8 %copy-start.2 = (f32[2048]{0:T(1024)S(1)}, f32[2048]{0:T(1024)}, u32[]{:S(2)}) copy-start(f32[2048]{0:T(1024)} %param.24) | copy-start | bytes 24580
  57.2 29.3 %copy-start.3 = (f32[2048]{0:T(1024)S(1)}, f32[2048]{0:T(1024)}, u32[]{:S(2)}) copy-start(f32[2048]{0:T(1024)} %param.31) | copy-start | bytes 24580
  58.7 10.3 %all-to-all-start.3 = ((bf16[8,4,768]{2,1,0:T(4,128)(2,1)}), bf16[8,4,768]{2,1,0:T(4,128)(2,1)S(1)}, u32[]{:S(2)}, u32[]{:S(2)}) async-start(bf16[8,4,768]{2,1,0:T(4,128)(2,1)} %broadcast_in_dim.120), calls=%async_computation.3 | async-start | bytes 98304 | tf_op jit(solution)/shard_map/all_to_all | solution.py:16
  70.0 16.0 %all-to-all-start.4 = ((bf16[16,4,256]{2,1,0:T(4,128)(2,1)}), bf16[16,4,256]{2,1,0:T(4,128)(2,1)S(1)}, u32[]{:S(2)}, u32[]{:S(2)}) async-start(bf16[16,4,256]{2,1,0:T(4,128)(2,1)} %bitcast.20), calls=%async_computation.4 | async-start | bytes 65536 | tf_op jit(solution)/shard_map/all_to_all | solution.py:16
  113.8 10.9 %copy-start.7 = (f32[4,2]{0,1:T(2,128)S(1)}, f32[4,2]{0,1:T(2,128)}, u32[]{:S(2)}) copy-start(f32[4,2]{0,1:T(2,128)} %param.35) | copy-start | bytes 100
  113.8 10.9 %copy-start.10 = (f32[4]{0:T(128)S(1)}, f32[4]{0:T(128)}, u32[]{:S(2)}) copy-start(f32[4]{0:T(128)} %param.34) | copy-start | bytes 52
  116.1 32.7 %copy-start.4 = (f32[1024]{0:T(1024)S(1)}, f32[1024]{0:T(1024)}, u32[]{:S(2)}) copy-start(f32[1024]{0:T(1024)} %param.39) | copy-start | bytes 12292
  117.2 27.6 %all-to-all-start.6 = ((bf16[256,8,128]{2,1,0:T(8,128)(2,1)}), bf16[256,8,128]{2,1,0:T(8,128)(2,1)S(1)}, u32[]{:S(2)}, u32[]{:S(2)}) async-start(bf16[256,8,128]{2,1,0:T(8,128)(2,1)} %reshape.284), calls=%async_computation.6 | async-start | bytes 1048576 | tf_op jit(solution)/shard_map/all_to_all | solution.py:16

commit v2 on v1

v2 whole, which is shorter than its diff:
```python
import jax
import jax.numpy as jnp
from jax import lax
from jax.experimental import pallas as pl
from jax.experimental.pallas import tpu as pltpu
from jax.sharding import Mesh
from jax.sharding import PartitionSpec as P


EPG = 4
EP = ("z", "y", "x")
ROW = ("y", "x")

ALPHA = 2.0**0.25
EPS = 1e-05


def swap(array, axis):
    return lax.all_to_all(array, axis, 0, 0, tiled=True)


def to_all(array, axis):
    return swap(jnp.broadcast_to(array[None], (lax.axis_size(axis), *array.shape)), axis)


def layer_norm(values, gain):
    mean = jnp.mean(values, -1, keepdims=True)
    spread = jnp.mean(jnp.square(values - mean), -1, keepdims=True)
    return (values - mean) * lax.rsqrt(spread + EPS) * gain


def expert_kernel(side_ref, rows_ref, gain_ref, gate_ref, up_ref, down_ref, kept_ref, given_ref, settled_ref):
    halves, sources, deep, part = rows_ref.shape
    line = sources // deep
    slots = line * deep
    width = gate_ref.shape[0]
    half = width // halves

    def piece(c, t):
        block = rows_ref[t, c * line : (c + 1) * line].astype(jnp.float32)
        return block.reshape(slots, part)

    total = jnp.zeros((slots, part), jnp.float32)
    for c in range(deep):
        for t in range(halves):
            total = total + piece(c, t)
    mean = jnp.sum(total, 1, keepdims=True) * (1.0 / width)
    square = jnp.zeros((slots, part), jnp.float32)
    for c in range(deep):
        for t in range(halves):
            off = piece(c, t) - mean
            square = square + off * off
    scale = lax.rsqrt(jnp.sum(square, 1, keepdims=True) * (1.0 / width) + EPS)
    for c in range(deep):
        for t in range(halves):
            at = (c * halves + t) * part
            value = (piece(c, t) - mean) * scale * gain_ref[:, at : at + part]
            settled_ref[:, at : at + part] = value.astype(jnp.bfloat16)
    settled = settled_ref[...]
    gate = jnp.dot(settled, gate_ref[...], preferred_element_type=jnp.float32)
    upward = jnp.dot(settled, up_ref[...], preferred_element_type=jnp.float32)
    hidden = (gate * jax.nn.sigmoid(gate) * upward).astype(jnp.bfloat16)
    side = side_ref[0]

    def spread(output, out_ref):
        tiles = jnp.stack([output[:, j * 128 : (j + 1) * 128] for j in range(half // 128)], 0)
        tiles = jnp.transpose(tiles, (1, 0, 2)).astype(out_ref.dtype)
        for p in range(line):
            for s in range(deep):
                out_ref[s * line + p] = tiles[p * deep + s]

    given = down_ref[:, pl.ds(pl.multiple_of((1 - side) * half, half), half)]
    spread(jnp.dot(hidden, given, preferred_element_type=jnp.float32), given_ref)
    kept = down_ref[:, pl.ds(pl.multiple_of(side * half, half), half)]
    spread(jnp.dot(hidden, kept, preferred_element_type=jnp.float32), kept_ref)


def run_experts(side, rows, gain, gate, up, down):
    halves, sources, _, _ = rows.shape
    width = gate.shape[0]
    vm = pl.BlockSpec(memory_space=pltpu.VMEM)
    shape = (sources, width // halves // 128, 128)
    return pl.pallas_call(
        expert_kernel,
        out_shape=(jax.ShapeDtypeStruct(shape, jnp.float32), jax.ShapeDtypeStruct(shape, jnp.bfloat16)),
        in_specs=[pl.BlockSpec(memory_space=pltpu.SMEM)] + [vm] * 5,
        out_specs=(vm, vm),
        scratch_shapes=[pltpu.VMEM((sources, width), jnp.bfloat16)],
        name="experts",
    )(side.reshape(1), rows, gain.reshape(1, -1), gate, up, down)


def attend_kernel(lengths_ref, lambda_ref, parts_ref, keys_ref, values_ref, gain_ref, out_ref):
    deep, seqs, _ = parts_ref.shape
    _, width = keys_ref.shape[1:]
    hwidth = width // 2
    heads = lambda_ref.shape[0]
    pad = 4
    rows = 2 * pad
    f32 = jnp.float32
    total = parts_ref[0]
    for d in range(1, deep):
        total = total + parts_ref[d]
    total = total.astype(jnp.bfloat16).astype(f32)
    first = lax.broadcasted_iota(jnp.int32, (1, width), 1) < hwidth
    blank = jnp.zeros((1, width), f32)
    at = heads * width
    scores, fresh = [], []
    for s in range(seqs):
        query = [total[s : s + 1, h * width : (h + 1) * width] for h in range(heads)]
        ones = [jnp.where(first, q, 0.0) for q in query] + [blank] * (pad - heads)
        twos = [jnp.where(first, 0.0, q) for q in query] + [blank] * (pad - heads)
        grid = jnp.concatenate(ones + twos, 0)
        new_key = total[s : s + 1, at : at + width]
        fresh.append(jnp.sum(grid * new_key, 1, keepdims=True))
        scores.append(
            lax.dot_general(
                grid.astype(jnp.bfloat16),
                keys_ref[s],
                (((1,), (1,)), ((), ())),
                preferred_element_type=f32,
            )
        )
    scale = hwidth**-0.5
    cached = jnp.concatenate(scores, 0) * scale
    newest = jnp.concatenate(fresh, 0) * scale
    row = lax.broadcasted_iota(jnp.int32, (seqs * rows, 1), 0)
    filled = jnp.zeros((seqs * rows, 1), jnp.int32)
    lam = jnp.zeros((pad, 1), f32)
    for s in range(seqs):
        filled = jnp.where(row // rows == s, lengths_ref[s], filled)
    side_row = lax.broadcasted_iota(jnp.int32, (pad, 1), 0)
    for h in range(heads):
        lam = jnp.where(side_row == h, lambda_ref[h], lam)
    valid = lax.broadcasted_iota(jnp.int32, cached.shape, 1) < filled
    highest = jnp.maximum(jnp.max(jnp.where(valid, cached, -1e30), 1, keepdims=True), newest)
    spread = jnp.where(valid, jnp.exp(cached - highest), 0.0)
    itself = jnp.exp(newest - highest)
    inverse = 1.0 / (jnp.sum(spread, 1, keepdims=True) + itself)
    maps = spread * inverse
    itself = itself * inverse
    gain = gain_ref[...]
    lines = []
    for s in range(seqs):
        one, two = s * rows, s * rows + pad
        weight = maps[one:two] - lam * maps[two : two + pad]
        fresh_weight = itself[one:two] - lam * itself[two : two + pad]
        weight = jnp.concatenate((weight, jnp.zeros_like(weight)), 0).astype(jnp.bfloat16)
        out = jnp.dot(weight, values_ref[s], preferred_element_type=f32)[:pad]
        new_value = total[s : s + 1, at + width : at + 2 * width]
        out = out + fresh_weight.astype(jnp.bfloat16).astype(f32) * new_value
        out = out * lax.rsqrt(jnp.mean(out * out, 1, keepdims=True) + EPS) * gain
        lines.append(jnp.concatenate([out[h : h + 1] for h in range(heads)], 1))
    attended = jnp.concatenate(lines, 0).astype(jnp.bfloat16)
    for d in range(out_ref.shape[0]):
        out_ref[d] = attended


def run_attend(parts, lengths, keys, values, mix_lambda, head_gain):
    deep, seqs, _ = parts.shape
    vm = pl.BlockSpec(memory_space=pltpu.VMEM)
    sm = pl.BlockSpec(memory_space=pltpu.SMEM)
    cols = mix_lambda.shape[0] * head_gain.shape[0]
    return pl.pallas_call(
        attend_kernel,
        out_shape=jax.ShapeDtypeStruct((deep, seqs, cols), jnp.bfloat16),
        in_specs=[sm, sm, vm, vm, vm, vm],
        out_specs=vm,
        name="attend",
    )(lengths, mix_lambda, parts, keys, values, head_gain.reshape(1, -1))


def shards(
    tokens,
    lengths,
    cache_keys,
    cache_values,
    norm0_gain,
    query_weight,
    key_weight,
    value_weight,
    mix_lambda,
    head_gain,
    out_weight,
    norm1_gain,
    group_ids,
    member_ids,
    group_weight,
    member_weights,
    expert_gate,
    expert_up,
    expert_down,
    norm2_gain,
):
    return layer(
        tokens,
        lengths,
        cache_keys,
        cache_values,
        norm0_gain,
        jnp.concatenate((query_weight, key_weight, value_weight), 1),
        mix_lambda,
        head_gain,
        out_weight,
        norm1_gain,
        group_ids,
        member_ids,
        group_weight,
        member_weights,
        expert_gate,
        expert_up,
        expert_down,
        norm2_gain,
    )


def layer(
    tokens,
    lengths,
    cache_keys,
    cache_values,
    norm0_gain,
    proj_weight,
    mix_lambda,
    head_gain,
    out_weight,
    norm1_gain,
    group_ids,
    member_ids,
    group_weight,
    member_weights,
    expert_gate,
    expert_up,
    expert_down,
    norm2_gain,
):
    seqs, width = tokens.shape
    deep = lax.axis_size("z")
    experts = lax.axis_size(EP)
    halves = lax.axis_size("tp")
    side = lax.axis_index("tp")
    half = width // halves
    block = width // deep
    part = block // halves
    proj_cols = proj_weight.shape[1]
    expert_ids = group_ids[:, None] * EPG + member_ids
    share = group_weight[:, None] * member_weights

    weights = to_all(jnp.concatenate((proj_weight, out_weight.T), 1), ROW).reshape(block, -1)
    weight_in, weight_out = weights[:, :proj_cols], weights[:, proj_cols:]

    normed = layer_norm(tokens.astype(jnp.float32), norm0_gain).astype(jnp.bfloat16)
    named = jnp.pad(expert_ids.astype(jnp.bfloat16), ((0, 0), (0, 128 - expert_ids.shape[1])))
    leaving = jnp.concatenate(
        (
            normed.reshape(seqs, deep, block).transpose(1, 0, 2),
            jnp.broadcast_to(named[None], (deep, seqs, 128)),
        ),
        2,
    )
    arrived = swap(leaving, "z")
    columns = arrived[:, :, :block]
    targets = lax.iota(jnp.int32, experts)
    line_ids = arrived[:, :, block : block + expert_ids.shape[1]].astype(jnp.int32)
    select = jnp.any(line_ids[None] == targets[:, None, None, None], 3).astype(jnp.float32)
    partial = jnp.dot(
        columns.reshape(deep * seqs, block), weight_in, preferred_element_type=jnp.float32
    )
    received = swap(partial.reshape(deep, seqs, proj_cols), "z")
    attended = run_attend(received, lengths, cache_keys, cache_values, mix_lambda, head_gain)
    everyone = swap(attended, "z").reshape(deep * seqs, -1)
    partial_mix = lax.dot_general(
        everyone, weight_out, (((1,), (1,)), ((), ())), preferred_element_type=jnp.float32
    )
    mix = jnp.sum(lax.all_gather(partial_mix, "tp"), 0).astype(jnp.bfloat16)
    mix = mix.reshape(deep, seqs, block)
    stream = (ALPHA * columns.astype(jnp.float32) + mix.astype(jnp.float32)).astype(jnp.bfloat16)
    mine = lax.dynamic_slice_in_dim(stream, side * part, part, 2).astype(jnp.float32)
    sending = jnp.sum(select[:, :, :, None] * mine[None], 2).astype(jnp.bfloat16)
    slots = swap(sending, EP)
    own_stream = swap(stream, "z")
    own_stream = own_stream.transpose(1, 0, 2).reshape(seqs, width)
    settled_own = layer_norm(own_stream.astype(jnp.float32), norm1_gain).astype(jnp.bfloat16)

    rows = lax.all_gather(slots, "tp")
    kept, given = run_experts(side, rows, norm1_gain, expert_gate[0], expert_up[0], expert_down[0])
    taken = lax.ppermute(given, "tp", ((0, 1), (1, 0)))
    leaving = (kept + taken.astype(jnp.float32)).astype(jnp.bfloat16)
    returned = swap(leaving, EP)
    combine = jnp.sum(
        jnp.where(expert_ids[:, :, None] == targets[None, None, :], share[:, :, None], 0.0), 1
    )
    routed = jnp.sum(combine[:, :, None, None] * returned.astype(jnp.float32)[None], 1)
    routed = routed.reshape(seqs, half)
    own = lax.dynamic_slice_in_dim(settled_own, side * half, half, 1)
    mixed = ALPHA * own.astype(jnp.float32) + routed
    sums = lax.psum(jnp.stack((jnp.sum(mixed, 1), jnp.sum(mixed * mixed, 1))), "tp")
    mean = sums[0] / width
    spread = sums[1] / width - mean * mean
    result = (mixed - mean[:, None]) * lax.rsqrt(spread[:, None] + EPS) * norm2_gain
    return result.astype(jnp.bfloat16)


def solution(mesh):
    torus = Mesh(mesh.devices.reshape(8, 4, 4, mesh.shape["tp"]), ("z", "y", "x", "tp"))
    return jax.shard_map(
        shards,
        mesh=torus,
        in_specs=(
            P(EP, None),
            P(EP),
            P(EP, None, "tp"),
            P(EP, None, "tp"),
            P(),
            P(EP, "tp"),
            P(EP, "tp"),
            P(EP, "tp"),
            P("tp"),
            P(),
            P("tp", EP),
            P(),
            P(EP),
            P(EP, None),
            P(EP),
            P(EP, None),
            P(EP, None, "tp"),
            P(EP, None, "tp"),
            P(EP, "tp", None),
            P("tp"),
        ),
        out_specs=P(EP, "tp"),
        check_vma=False,
    )
```

time: 150 us -> 145 us (0.967)
  blocking collectives: 49.9 us -> 58 us
  Pallas kernels: 0 us -> 8.09 us
  matrix products: 8.88 us -> 1.1 us
  starting transfers between devices: 31.8 us -> 25.6 us
  local copies, waits for them, and re-layouts: 6.71 us -> 1.82 us
  waiting for transfers between devices: 43.9 us -> 39.7 us
  other arithmetic: 8 us -> 9.99 us
    all_gather x0 -> x2, blocking collectives: none -> 11 us  [the longest x1 6.8 us: layer(): mix = jnp.sum(lax.all_gather(partial_mix, 'tp'), 0).astype(jnp.bfloat16)]
    pallas_call x0 -> x2, Pallas kernels: none -> 8.09 us  [the longest x1 4.14 us: run_attend(): pl.pallas_call(attend_kernel, out_shape=jax.ShapeDtypeStruct((deep, seqs,...]
    dot_general x9 -> x2, matrix products: 8.88 us -> 1.1 us  [the longest x1 0.89 us: layer(): jnp.dot(columns.reshape(deep * seqs, block), weight_in, preferred_element...]
    all_to_all x5, starting transfers between devices: 31.8 us -> 25.2 us  [swap(): return lax.all_to_all(array, axis, 0, 0, tiled=True)]
    all_to_all x2, blocking collectives: 46.9 us -> 41.7 us  [swap(): return lax.all_to_all(array, axis, 0, 0, tiled=True)]
    all_to_all x5, waiting for transfers between devices: 43.9 us -> 39.7 us  [swap(): return lax.all_to_all(array, axis, 0, 0, tiled=True)]
    unnamed x28 -> x12, local copies, waits for them, and re-layouts: 4.09 us -> 0.89 us
    psum x1, blocking collectives: 3.04 us -> 5.39 us  [layer(): lax.psum(jnp.stack((jnp.sum(mixed, 1), jnp.sum(mixed * mixed, 1))), 'tp')]
  transfers between devices with their start and end apart: 5 -> 6, of which waited for: 5 -> 5; matrix products, arithmetic and copies ran while one was open for 4% -> 2% of each run, Pallas kernels for 0% -> 0%
where the time goes in v2:
time: 145 us
  blocking collectives  58 us (40%)
  waiting for transfers between devices  39.7 us (27%)
  starting transfers between devices  25.6 us (18%)
  other arithmetic  9.99 us (7%)
  Pallas kernels  8.09 us (6%)
  local copies, waits for them, and re-layouts  1.82 us (1%)
    all_to_all x2, blocking collectives, swap(): return lax.all_to_all(array, axis, 0, 0, tiled=True)  41.7 us
    all_to_all x5, waiting for transfers between devices, swap(): return lax.all_to_all(array, axis, 0, 0, tiled=True)  39.7 us
    all_to_all x5, starting transfers between devices, swap(): return lax.all_to_all(array, axis, 0, 0, tiled=True)  25.2 us
    all_gather x1, blocking collectives, layer(): mix = jnp.sum(lax.all_gather(partial_mix, 'tp'), 0).astype(jnp.bfloat16)  6.8 us
    psum x1, blocking collectives, layer(): lax.psum(jnp.stack((jnp.sum(mixed, 1), jnp.sum(mixed * mixed, 1))), 'tp')  5.39 us
    all_gather x1, blocking collectives, layer(): rows = lax.all_gather(slots, 'tp')  4.18 us
    pallas_call x1, Pallas kernels, run_attend(): pl.pallas_call(attend_kernel, out_shape=jax.ShapeDtypeStruct((deep, seqs,...  4.14 us
    pallas_call x1, Pallas kernels, run_experts(): pl.pallas_call(expert_kernel, out_shape=(jax.ShapeDtypeStruct(shape, jnp....  3.94 us
  transfers between devices with their start and end apart: 6, of which 5 were waited for; matrix products, arithmetic and copies ran while one was open for 2% of the time, Pallas kernels for 0%

profile of v2, /device:TPU:1, one launch (start us, length us, event | category | flops | bytes accessed | tf_op | source)
XLA Modules:
  0.0 144.5 jit_solution(10065305198766453535)
XLA Ops:
  0.0 0.7 broadcast_multiply_fusion.1
  0.7 0.7 fusion.17
  1.5 0.8 convert_reduce_fusion
  2.3 0.9 fusion.5
  3.2 0.8 fusion.7
  4.1 0.6 pad_maximum_fusion.1
  4.7 9.0 %all-to-all-start = ((bf16[8,4,384]{2,1,0:T(4,128)(2,1)}), bf16[8,4,384]{2,1,0:T(4,128)(2,1)S(1)}, u32[]{:S(2)}, u32[]{:S(2)}) async-start(bf16[8,4,384]{2,1,0:T(4,128)(2,1)} %pad_maximum_fusion.1), calls=%async_computation | async-start | bytes 49152 | tf_op jit(solution)/shard_map/all_to_all | solution.py:19
  13.7 0.8 pad_maximum_fusion
  14.5 5.9 %all-to-all-done = bf16[8,4,384]{2,1,0:T(4,128)(2,1)S(1)} async-done(((bf16[8,4,384]{2,1,0:T(4,128)(2,1)}), bf16[8,4,384]{2,1,0:T(4,128)(2,1)S(1)}, u32[]{:S(2)}, u32[]{:S(2)}) %all-to-all-start) | async-done | bytes 24608 | tf_op jit(solution)/shard_map/all_to_all | solution.py:19
  20.5 22.2 %all_to_all.35 = bf16[16,16,2048]{2,1,0:T(8,128)(2,1)S(1)} all-to-all(bf16[16,16,2048]{2,1,0:T(8,128)(2,1)S(1)} %broadcast_in_dim.15), channel_id=1, replica_groups=mesh['z'=8,'y'=4,'x'=4,'tp'=2] {'y','x'}, dimensions={0} | all-to-all | bytes 2097152 | tf_op jit(solution)/shard_map/all_to_all | solution.py:19
  42.6 0.9 fusion
  43.5 3.4 %all-to-all-start.2 = ((f32[8,4,1280]{2,1,0:T(4,128)}), f32[8,4,1280]{2,1,0:T(4,128)S(1)}, u32[]{:S(2)}, u32[]{:S(2)}) async-start(f32[8,4,1280]{2,1,0:T(4,128)} %fusion), calls=%async_computation.2 | async-start | bytes 327680 | tf_op jit(solution)/shard_map/all_to_all | solution.py:19
  47.1 8.0 %all-to-all-done.2.parts_ref = f32[8,4,1280]{2,1,0:T(4,128)S(1)} async-done(((f32[8,4,1280]{2,1,0:T(4,128)}), f32[8,4,1280]{2,1,0:T(4,128)S(1)}, u32[]{:S(2)}, u32[]{:S(2)}) %all-to-all-start.2) | async-done | bytes 163872 | tf_op jit(solution)/shard_map/all_to_all | solution.py:19
  55.1 0.7 copy-done
  55.8 4.1 %attend.1 = bf16[8,4,768]{2,1,0:T(4,128)(2,1)} custom-call(s32[4]{0:T(128)} %lengths_ref.1, f32[3]{0:T(128)} %lambda_ref.1, f32[8,4,1280]{2,1,0:T(4,128)} %copy-done, bf16[4,1024,256]{2,1,0:T(8,128)(2,1)} %keys_ref.1, bf16[4,1024,256]{2,1,0:T(8,128)(2,1)} %values_ref.1, f32[1,256]{1,0:T(1,128)} %bitcast.50), custom_call_target="tpu_custom_call" | custom-call | tf_op jit(solution)/shard_map/attend/pallas_call | solution.py:164
  59.9 3.3 %all-to-all-start.3 = ((bf16[8,4,768]{2,1,0:T(4,128)(2,1)}), bf16[8,4,768]{2,1,0:T(4,128)(2,1)S(1)}, u32[]{:S(2)}, u32[]{:S(2)}) async-start(bf16[8,4,768]{2,1,0:T(4,128)(2,1)} %attend.1), calls=%async_computation.3 | async-start | bytes 98304 | tf_op jit(solution)/shard_map/all_to_all | solution.py:19
  63.5 6.7 %all-to-all-done.3 = bf16[8,4,768]{2,1,0:T(4,128)(2,1)S(1)} async-done(((bf16[8,4,768]{2,1,0:T(4,128)(2,1)}), bf16[8,4,768]{2,1,0:T(4,128)(2,1)S(1)}, u32[]{:S(2)}, u32[]{:S(2)}) %all-to-all-start.3) | async-done | bytes 49184 | tf_op jit(solution)/shard_map/all_to_all | solution.py:19
  70.5 6.8 %all-gather = f32[64,256]{1,0:T(8,128)S(1)} all-gather(f32[32,256]{1,0:T(8,128)S(1)} %fusion.1), channel_id=2, replica_groups=mesh['z'=8,'y'=4,'x'=4,'tp'=2] {'tp'}, dimensions={0}, use_global_device_ids=true | all-gather | bytes 98304 | tf_op jit(solution)/shard_map/all_gather | solution.py:275
  77.3 0.6 multiply_reduce_fusion.1
  78.0 19.5 %all_to_all.36 = bf16[128,8,128]{2,1,0:T(8,128)(2,1)S(1)} all-to-all(bf16[128,8,128]{2,1,0:T(8,128)(2,1)S(1)} %multiply_reduce_fusion.1), channel_id=1, replica_groups=mesh['z'=8,'y'=4,'x'=4,'tp'=2] {'z','y','x'}, dimensions={0} | all-to-all | bytes 524288 | tf_op jit(solution)/shard_map/all_to_all | solution.py:19
  97.5 4.2 %all-gather.1 = bf16[256,8,128]{2,1,0:T(8,128)(2,1)} all-gather(bf16[128,8,128]{2,1,0:T(8,128)(2,1)S(1)} %all_to_all.36), channel_id=3, replica_groups=mesh['z'=8,'y'=4,'x'=4,'tp'=2] {'tp'}, dimensions={0}, use_global_device_ids=true | all-gather | bytes 786432 | tf_op jit(solution)/shard_map/all_gather | solution.py:285
  101.7 3.9 %experts.1 = (f32[128,8,128]{2,1,0:T(8,128)}, bf16[128,8,128]{2,1,0:T(8,128)(2,1)}) custom-call(s32[1]{0:T(128)} %bitcast.9.side_ref, bf16[2,128,8,128]{3,2,1,0:T(8,128)(2,1)} %bitcast.38, f32[1,2048]{1,0:T(1,128)} %bitcast.47, bf16[2048,256]{1,0:T(8,128)(2,1)} %bitcast.39, bf16[2048,256]{1,0:T(8,128)(2,1)} %bitcast.40, bf16[256,2048]{1,0:T(8,128)(2,1)} %bitcast.41), custom_call_target="tpu_custom_call" | custom-call | tf_op jit(solution)/shard_map/experts/pallas_call | solution.py:83
  105.6 0.4 collective-permute-start
  106.0 0.6 copy.53
  106.6 3.3 %all-to-all-start.4 = ((bf16[8,4,256]{2,1,0:T(4,128)(2,1)}), bf16[8,4,256]{2,1,0:T(4,128)(2,1)S(1)}, u32[]{:S(2)}, u32[]{:S(2)}) async-start(bf16[8,4,256]{2,1,0:T(4,128)(2,1)} %copy.53), calls=%async_computation.4 | async-start | bytes 32768 | tf_op jit(solution)/shard_map/all_to_all | solution.py:19
  110.0 6.5 %all-to-all-done.4 = bf16[8,4,256]{2,1,0:T(4,128)(2,1)S(1)} async-done(((bf16[8,4,256]{2,1,0:T(4,128)(2,1)}), bf16[8,4,256]{2,1,0:T(4,128)(2,1)S(1)}, u32[]{:S(2)}, u32[]{:S(2)}) %all-to-all-start.4) | async-done | bytes 16416 | tf_op jit(solution)/shard_map/all_to_all | solution.py:19
  116.6 1.8 %add_convert_fusion = bf16[128,8,128]{2,1,0:T(8,128)(2,1)} fusion(f32[128,8,128]{2,1,0:T(8,128)} %get-tuple-element.7, bf16[128,8,128]{2,1,0:T(8,128)(2,1)S(1)} %collective-permute-done), kind=kLoop, calls=%fused_computation.4 | loop fusion | flops 393216 | bytes 1048576 | tf_op jit(solution)/shard_map/convert_element_type | solution.py:288
  118.4 6.2 %all-to-all-start.6 = ((bf16[128,8,128]{2,1,0:T(8,128)(2,1)}), bf16[128,8,128]{2,1,0:T(8,128)(2,1)S(1)}, u32[]{:S(2)}, u32[]{:S(2)}) async-start(bf16[128,8,128]{2,1,0:T(8,128)(2,1)} %add_convert_fusion), calls=%async_computation.6 | async-start | bytes 524288 | tf_op jit(solution)/shard_map/all_to_all | solution.py:19
  124.8 12.6 %all-to-all-done.6 = bf16[128,8,128]{2,1,0:T(8,128)(2,1)S(1)} async-done(((bf16[128,8,128]{2,1,0:T(8,128)(2,1)}), bf16[128,8,128]{2,1,0:T(8,128)(2,1)S(1)}, u32[]{:S(2)}, u32[]{:S(2)}) %all-to-all-start.6) | async-done | bytes 262176 | tf_op jit(solution)/shard_map/all_to_all | solution.py:19
  137.5 0.7 multiply_reduce_fusion
  138.4 5.4 %psum.7 = f32[2,4]{1,0:T(2,128)S(1)} all-reduce(f32[2,4]{1,0:T(2,128)S(1)} %pad_maximum_fusion.2), channel_id=1, replica_groups=mesh['z'=8,'y'=4,'x'=4,'tp'=2] {'tp'}, use_global_device_ids=true, to_apply=%region_11.12 | all-reduce | flops 8 | bytes 64 | tf_op jit(solution)/shard_map/psum | solution.py:297
  143.8 0.7 multiply_convert_fusion
  (43 shorter events, 1.6 us)
Async XLA Ops:
  4.7 15.7 %all-to-all-start = ((bf16[8,4,384]{2,1,0:T(4,128)(2,1)}), bf16[8,4,384]{2,1,0:T(4,128)(2,1)S(1)}, u32[]{:S(2)}, u32[]{:S(2)}) async-start(bf16[8,4,384]{2,1,0:T(4,128)(2,1)} %pad_maximum_fusion.1), calls=%async_computation | async-start | bytes 49152 | tf_op jit(solution)/shard_map/all_to_all | solution.py:19
  43.5 11.6 %all-to-all-start.2 = ((f32[8,4,1280]{2,1,0:T(4,128)}), f32[8,4,1280]{2,1,0:T(4,128)S(1)}, u32[]{:S(2)}, u32[]{:S(2)}) async-start(f32[8,4,1280]{2,1,0:T(4,128)} %fusion), calls=%async_computation.2 | async-start | bytes 327680 | tf_op jit(solution)/shard_map/all_to_all | solution.py:19
  55.1 0.7 copy-start
  59.9 10.3 %all-to-all-start.3 = ((bf16[8,4,768]{2,1,0:T(4,128)(2,1)}), bf16[8,4,768]{2,1,0:T(4,128)(2,1)S(1)}, u32[]{:S(2)}, u32[]{:S(2)}) async-start(bf16[8,4,768]{2,1,0:T(4,128)(2,1)} %attend.1), calls=%async_computation.3 | async-start | bytes 98304 | tf_op jit(solution)/shard_map/all_to_all | solution.py:19
  97.5 8.5 %copy-start.3 = (f32[4,2]{0,1:T(2,128)S(1)}, f32[4,2]{0,1:T(2,128)}, u32[]{:S(2)}) copy-start(f32[4,2]{0,1:T(2,128)} %param.35) | copy-start | bytes 100
  97.5 8.5 %copy-start.4 = (f32[4]{0:T(128)S(1)}, f32[4]{0:T(128)}, u32[]{:S(2)}) copy-start(f32[4]{0:T(128)} %param.34) | copy-start | bytes 52
  97.5 12.5 %copy-start.1 = (f32[2048]{0:T(1024)S(1)}, f32[2048]{0:T(1024)}, u32[]{:S(2)}) copy-start(f32[2048]{0:T(1024)} %param.31) | copy-start | bytes 24580
  105.6 38.2 %copy-start.2 = (f32[1024]{0:T(1024)S(1)}, f32[1024]{0:T(1024)}, u32[]{:S(2)}) copy-start(f32[1024]{0:T(1024)} %param.39) | copy-start | bytes 12292
  105.6 11.0 %collective-permute-start = (bf16[128,8,128]{2,1,0:T(8,128)(2,1)}, bf16[128,8,128]{2,1,0:T(8,128)(2,1)S(1)}, u32[]{:S(2)}, u32[]{:S(2)}) collective-permute-start(bf16[128,8,128]{2,1,0:T(8,128)(2,1)} %get-tuple-element.8), channel_id=1, source_target_pairs={{0,1},{1,0},{2,3},{3,2},{4,5},{5,4},{6,7},{7,6},{8,9},{9,8},{10,11... | collective-permute-start | bytes 786440 | tf_op jit(solution)/shard_map/ppermute | solution.py:287
  106.6 9.9 %all-to-all-start.4 = ((bf16[8,4,256]{2,1,0:T(4,128)(2,1)}), bf16[8,4,256]{2,1,0:T(4,128)(2,1)S(1)}, u32[]{:S(2)}, u32[]{:S(2)}) async-start(bf16[8,4,256]{2,1,0:T(4,128)(2,1)} %copy.53), calls=%async_computation.4 | async-start | bytes 32768 | tf_op jit(solution)/shard_map/all_to_all | solution.py:19
  118.4 19.0 %all-to-all-start.6 = ((bf16[128,8,128]{2,1,0:T(8,128)(2,1)}), bf16[128,8,128]{2,1,0:T(8,128)(2,1)S(1)}, u32[]{:S(2)}, u32[]{:S(2)}) async-start(bf16[128,8,128]{2,1,0:T(8,128)(2,1)} %add_convert_fusion), calls=%async_computation.6 | async-start | bytes 524288 | tf_op jit(solution)/shard_map/all_to_all | solution.py:19

commit v3 on v2

v3 whole, which is shorter than its diff:
```python
import jax
import jax.numpy as jnp
from jax import lax
from jax.experimental import pallas as pl
from jax.experimental.pallas import tpu as pltpu
from jax.sharding import Mesh
from jax.sharding import PartitionSpec as P


EPG = 4
EP = ("z", "y", "x")
ROW = ("y", "x")

ALPHA = 2.0**0.25
EPS = 1e-05


def swap(array, axis):
    return lax.all_to_all(array, axis, 0, 0, tiled=True)


def to_all(array, axis):
    return swap(jnp.broadcast_to(array[None], (lax.axis_size(axis), *array.shape)), axis)


def around(array, axis):
    size = lax.axis_size(axis)
    return [array] + [
        lax.ppermute(array, axis, [(i, (i + j) % size) for i in range(size)])
        for j in range(1, size)
    ]


def layer_norm(values, gain):
    mean = jnp.mean(values, -1, keepdims=True)
    spread = jnp.mean(jnp.square(values - mean), -1, keepdims=True)
    return (values - mean) * lax.rsqrt(spread + EPS) * gain


def fast(array):
    return pltpu.with_memory_space_constraint(array, pltpu.VMEM)


VM = pl.BlockSpec(memory_space=pltpu.VMEM)
SM = pl.BlockSpec(memory_space=pltpu.SMEM)
SMALL = pltpu.CompilerParams(vmem_limit_bytes=16 * 2**20)


def order_kernel(place_ref, *refs):
    out_ref = refs[-1]
    tall, wide = len(refs) - 1, refs[0].shape[0] // 16
    for dy in range(tall):
        for dx in range(wide):
            y = lax.rem(place_ref[0] + tall - dy, tall)
            x = lax.rem(place_ref[1] + wide - dx, wide)
            at = pl.multiple_of((y * wide + x) * 16, 16)
            out_ref[pl.ds(at, 16)] = refs[dy][dx * 16 : (dx + 1) * 16]


def order(place, blocks):
    rows, cols = blocks[0].shape
    return pl.pallas_call(
        order_kernel,
        out_shape=jax.ShapeDtypeStruct((rows * len(blocks), cols), blocks[0].dtype),
        in_specs=[SM] + [VM] * len(blocks),
        out_specs=VM,
        compiler_params=SMALL,
        name="order",
    )(place, *(fast(b) for b in blocks))


def outproj_kernel(heads_ref, weight_ref, out_ref, rows_ref):
    deep, seqs, _ = heads_ref.shape
    heads = jnp.concatenate([heads_ref[d].astype(jnp.float32) for d in range(deep)], 0)
    rows_ref[...] = lax.dot_general(
        heads.astype(jnp.bfloat16),
        weight_ref[...],
        (((1,), (1,)), ((), ())),
        preferred_element_type=jnp.float32,
    )
    for i in range(seqs):
        out_ref[i] = jnp.concatenate(
            [rows_ref[d * seqs + i : d * seqs + i + 1] for d in range(deep)], 0
        )


def outproj(heads, weight):
    deep, seqs, _ = heads.shape
    block = weight.shape[0]
    return pl.pallas_call(
        outproj_kernel,
        out_shape=jax.ShapeDtypeStruct((seqs, deep, block), jnp.float32),
        in_specs=[VM, VM],
        out_specs=VM,
        scratch_shapes=[pltpu.VMEM((seqs * deep, block), jnp.float32)],
        compiler_params=SMALL,
        name="outproj",
    )(fast(heads), fast(weight))


def build_kernel(side_ref, own_ref, other_ref, columns_ref, ids_ref, out_ref, stream_ref):
    seqs, _, block = own_ref.shape
    part = block // 2
    at = pl.multiple_of(side_ref[0] * part, part)
    rows, names = [], []
    for i in range(seqs):
        mix = (own_ref[i] + other_ref[i]).astype(jnp.bfloat16).astype(jnp.float32)
        stream_ref[i] = (ALPHA * columns_ref[i] + mix).astype(jnp.bfloat16).astype(jnp.float32)
        rows.append(stream_ref[i, :, pl.ds(at, part)])
        names.append([ids_ref[i, :, k * part : (k + 1) * part] for k in range(2)])
    for e in range(out_ref.shape[0]):
        value = jnp.zeros_like(rows[0])
        for row, (one, two) in zip(rows, names, strict=True):
            value = jnp.where((one == e) | (two == e), row, value)
        out_ref[e] = value.astype(jnp.bfloat16)


def build(side, own, other, columns, ids, experts):
    seqs, deep, block = own.shape
    return pl.pallas_call(
        build_kernel,
        out_shape=(
            jax.ShapeDtypeStruct((experts, deep, block // 2), jnp.bfloat16),
            jax.ShapeDtypeStruct((seqs, deep, block), jnp.float32),
        ),
        in_specs=[SM] + [VM] * 4,
        out_specs=(VM, VM),
        compiler_params=SMALL,
        name="build",
    )(side, fast(own), fast(other), fast(columns), fast(ids))


def lay_kernel(place_ref, stream_ref, *out_refs):
    seqs, deep, _ = stream_ref.shape
    for j, out_ref in enumerate(out_refs):
        z = lax.rem(place_ref[0] + j, deep)
        rows = [stream_ref[i, pl.ds(z, 1), :] for i in range(seqs)]
        out_ref[...] = jnp.concatenate(rows, 0).astype(jnp.bfloat16)


def lay(place, stream):
    seqs, deep, block = stream.shape
    return pl.pallas_call(
        lay_kernel,
        out_shape=(jax.ShapeDtypeStruct((seqs, block), jnp.bfloat16),) * deep,
        in_specs=[SM, VM],
        out_specs=(VM,) * deep,
        compiler_params=SMALL,
        name="lay",
    )(place, stream)


def settle_kernel(place_ref, side_ref, gain_ref, *refs):
    out_ref, row_ref = refs[-2:]
    deep = len(refs) - 2
    block = refs[0].shape[1]
    for j in range(deep):
        z = lax.rem(place_ref[0] + deep - j, deep)
        at = pl.multiple_of(z * block, block)
        row_ref[:, pl.ds(at, block)] = refs[j][...].astype(jnp.float32)
    values = row_ref[...]
    mean = jnp.mean(values, 1, keepdims=True)
    off = values - mean
    scale = lax.rsqrt(jnp.mean(off * off, 1, keepdims=True) + EPS)
    settled = (off * scale * gain_ref[...]).astype(jnp.bfloat16)
    row_ref[...] = ALPHA * settled.astype(jnp.float32)
    tiles = out_ref.shape[1]
    for j in range(tiles):
        at = pl.multiple_of((side_ref[0] * tiles + j) * 128, 128)
        out_ref[:, j, :] = row_ref[:, pl.ds(at, 128)]


def settle(place, side, gain, blocks):
    seqs, block = blocks[0].shape
    width = block * len(blocks)
    return pl.pallas_call(
        settle_kernel,
        out_shape=jax.ShapeDtypeStruct((seqs, width // 256, 128), jnp.float32),
        in_specs=[SM, SM] + [VM] * (1 + len(blocks)),
        out_specs=VM,
        scratch_shapes=[pltpu.VMEM((seqs, width), jnp.float32)],
        compiler_params=SMALL,
        name="settle",
    )(place, side, gain.reshape(1, -1), *blocks)


def combine_kernel(ids_ref, share_ref, returned_ref, residual_ref, mixed_ref, stats_ref):
    seqs, topk = residual_ref.shape[0], 2
    for i in range(seqs):
        mixed = residual_ref[i]
        for k in range(topk):
            row = returned_ref[ids_ref[i * topk + k]].astype(jnp.float32)
            mixed = mixed + share_ref[i * topk + k] * row
        mixed_ref[i] = mixed
        for at, value in ((i, mixed), (seqs + i, mixed * mixed)):
            total = jnp.sum(jnp.sum(value, 0, keepdims=True), 1, keepdims=True)
            stats_ref[at : at + 1] = jnp.broadcast_to(total, (1, 128))


def run_combine(ids, share, returned, residual):
    seqs = residual.shape[0]
    return pl.pallas_call(
        combine_kernel,
        out_shape=(
            jax.ShapeDtypeStruct(residual.shape, jnp.float32),
            jax.ShapeDtypeStruct((2 * seqs, 128), jnp.float32),
        ),
        in_specs=[SM, SM, VM, VM],
        out_specs=(VM, VM),
        compiler_params=SMALL,
        name="combine",
    )(ids.reshape(-1), share.reshape(-1), fast(returned), fast(residual))


def finish_kernel(mixed_ref, own_ref, other_ref, gain_ref, out_ref):
    seqs, tiles, _ = mixed_ref.shape
    width = 2 * tiles * 128
    stats = (own_ref[...] + other_ref[...]) * (1.0 / width)
    mean, second = stats[:seqs], stats[seqs:]
    scale = lax.rsqrt(second - mean * mean + EPS)
    for j in range(tiles):
        at = slice(j * 128, (j + 1) * 128)
        value = (mixed_ref[:, j, :] - mean) * scale * gain_ref[:, at]
        out_ref[:, at] = value.astype(jnp.bfloat16)


def finish(mixed, own, other, gain):
    seqs, tiles, _ = mixed.shape
    return pl.pallas_call(
        finish_kernel,
        out_shape=jax.ShapeDtypeStruct((seqs, tiles * 128), jnp.bfloat16),
        in_specs=[VM] * 4,
        out_specs=VM,
        compiler_params=SMALL,
        name="finish",
    )(fast(mixed), fast(own), fast(other), gain.reshape(1, -1))


def hidden_kernel(
    side_ref, own_ref, other_ref, gain_ref, gate_ref, up_ref, down_ref, hidden_ref, given_ref, settled_ref
):
    sources, deep, part = own_ref.shape
    line = sources // deep
    slots = line * deep
    width = gate_ref.shape[0]
    half = width // 2
    side = side_ref[0]

    def pieces():
        for c in range(deep):
            for ref, t in ((own_ref, side), (other_ref, 1 - side)):
                block = ref[c * line : (c + 1) * line].astype(jnp.float32)
                yield block.reshape(slots, part), pl.multiple_of((2 * c + t) * part, part)

    total = jnp.zeros((slots, part), jnp.float32)
    for piece, _ in pieces():
        total = total + piece
    mean = jnp.sum(total, 1, keepdims=True) * (1.0 / width)
    square = jnp.zeros((slots, part), jnp.float32)
    for piece, _ in pieces():
        off = piece - mean
        square = square + off * off
    scale = lax.rsqrt(jnp.sum(square, 1, keepdims=True) * (1.0 / width) + EPS)
    for piece, at in pieces():
        value = (piece - mean) * scale * gain_ref[:, pl.ds(at, part)]
        settled_ref[:, pl.ds(at, part)] = value.astype(jnp.bfloat16)
    settled = settled_ref[...]
    gate = jnp.dot(settled, gate_ref[...], preferred_element_type=jnp.float32)
    upward = jnp.dot(settled, up_ref[...], preferred_element_type=jnp.float32)
    hidden = (gate * jax.nn.sigmoid(gate) * upward).astype(jnp.bfloat16)
    hidden_ref[...] = hidden
    down = down_ref[:, pl.ds(pl.multiple_of((1 - side) * half, half), half)]
    tiles = in_tiles(jnp.dot(hidden, down, preferred_element_type=jnp.float32))
    tiles = tiles.astype(jnp.bfloat16)
    for p in range(line):
        for s in range(deep):
            given_ref[s * line + p] = tiles[p * deep + s]


def in_tiles(output):
    pieces = [output[:, j * 128 : (j + 1) * 128] for j in range(output.shape[1] // 128)]
    return jnp.transpose(jnp.stack(pieces, 0), (1, 0, 2))


def down_kernel(side_ref, hidden_ref, down_ref, taken_ref, out_ref):
    half = down_ref.shape[1] // 2
    line = 16
    deep = out_ref.shape[0] // line
    down = down_ref[:, pl.ds(pl.multiple_of(side_ref[0] * half, half), half)]
    tiles = in_tiles(jnp.dot(hidden_ref[...], down, preferred_element_type=jnp.float32))
    for p in range(line):
        for s in range(deep):
            both = tiles[p * deep + s] + taken_ref[s * line + p].astype(jnp.float32)
            out_ref[s * line + p] = both.astype(jnp.bfloat16)


def run_hidden(side, own, other, gain, gate, up, down):
    sources, _, _ = own.shape
    width, ff = gate.shape
    return pl.pallas_call(
        hidden_kernel,
        out_shape=(
            pltpu.VMEM((sources, ff), jnp.bfloat16),
            pltpu.VMEM((sources, width // 256, 128), jnp.bfloat16),
        ),
        in_specs=[SM] + [VM] * 6,
        out_specs=(VM, VM),
        scratch_shapes=[pltpu.VMEM((sources, width), jnp.bfloat16)],
        compiler_params=SMALL,
        name="hidden",
    )(side, fast(own), fast(other), gain.reshape(1, -1), fast(gate), fast(up), fast(down))


def run_down(side, hidden, down, taken):
    return pl.pallas_call(
        down_kernel,
        out_shape=pltpu.VMEM(taken.shape, jnp.bfloat16),
        in_specs=[SM] + [VM] * 3,
        out_specs=VM,
        compiler_params=SMALL,
        name="down",
    )(side, fast(hidden), fast(down), fast(taken))


def attend_kernel(
    lengths_ref, lambda_ref, parts_ref, keys_ref, far_ref, gain_ref, out_ref, values_ref, arrived
):
    loading = pltpu.make_async_copy(far_ref, values_ref, arrived)
    loading.start()
    deep, seqs, _ = parts_ref.shape
    _, width = keys_ref.shape[1:]
    hwidth = width // 2
    heads = lambda_ref.shape[0]
    pad = 4
    rows = 2 * pad
    f32 = jnp.float32
    total = parts_ref[0]
    for d in range(1, deep):
        total = total + parts_ref[d]
    total = total.astype(jnp.bfloat16).astype(f32)
    first = lax.broadcasted_iota(jnp.int32, (1, width), 1) < hwidth
    blank = jnp.zeros((1, width), f32)
    at = heads * width
    scores, fresh = [], []
    for s in range(seqs):
        query = [total[s : s + 1, h * width : (h + 1) * width] for h in range(heads)]
        ones = [jnp.where(first, q, 0.0) for q in query] + [blank] * (pad - heads)
        twos = [jnp.where(first, 0.0, q) for q in query] + [blank] * (pad - heads)
        grid = jnp.concatenate(ones + twos, 0)
        new_key = total[s : s + 1, at : at + width]
        fresh.append(jnp.sum(grid * new_key, 1, keepdims=True))
        scores.append(
            lax.dot_general(
                grid.astype(jnp.bfloat16),
                keys_ref[s],
                (((1,), (1,)), ((), ())),
                preferred_element_type=f32,
            )
        )
    scale = hwidth**-0.5
    cached = jnp.concatenate(scores, 0) * scale
    newest = jnp.concatenate(fresh, 0) * scale
    row = lax.broadcasted_iota(jnp.int32, (seqs * rows, 1), 0)
    filled = jnp.zeros((seqs * rows, 1), jnp.int32)
    lam = jnp.zeros((pad, 1), f32)
    for s in range(seqs):
        filled = jnp.where(row // rows == s, lengths_ref[s], filled)
    side_row = lax.broadcasted_iota(jnp.int32, (pad, 1), 0)
    for h in range(heads):
        lam = jnp.where(side_row == h, lambda_ref[h], lam)
    valid = lax.broadcasted_iota(jnp.int32, cached.shape, 1) < filled
    highest = jnp.maximum(jnp.max(jnp.where(valid, cached, -1e30), 1, keepdims=True), newest)
    spread = jnp.where(valid, jnp.exp(cached - highest), 0.0)
    itself = jnp.exp(newest - highest)
    inverse = 1.0 / (jnp.sum(spread, 1, keepdims=True) + itself)
    maps = spread * inverse
    itself = itself * inverse
    gain = gain_ref[...]
    loading.wait()
    lines = []
    for s in range(seqs):
        one, two = s * rows, s * rows + pad
        weight = maps[one:two] - lam * maps[two : two + pad]
        fresh_weight = itself[one:two] - lam * itself[two : two + pad]
        weight = jnp.concatenate((weight, jnp.zeros_like(weight)), 0).astype(jnp.bfloat16)
        out = jnp.dot(weight, values_ref[s], preferred_element_type=f32)[:pad]
        new_value = total[s : s + 1, at + width : at + 2 * width]
        out = out + fresh_weight.astype(jnp.bfloat16).astype(f32) * new_value
        out = out * lax.rsqrt(jnp.mean(out * out, 1, keepdims=True) + EPS) * gain
        lines.append(jnp.concatenate([out[h : h + 1] for h in range(heads)], 1))
    attended = jnp.concatenate(lines, 0).astype(jnp.bfloat16)
    for d in range(out_ref.shape[0]):
        out_ref[d] = attended


def run_attend(parts, lengths, keys, values, mix_lambda, head_gain):
    deep, seqs, _ = parts.shape
    cols = mix_lambda.shape[0] * head_gain.shape[0]
    return pl.pallas_call(
        attend_kernel,
        out_shape=pltpu.VMEM((deep, seqs, cols), jnp.bfloat16),
        in_specs=[SM, SM, VM, VM, pl.BlockSpec(memory_space=pl.ANY), VM],
        out_specs=VM,
        scratch_shapes=[pltpu.VMEM(values.shape, values.dtype), pltpu.SemaphoreType.DMA],
        compiler_params=SMALL,
        name="attend",
    )(lengths, mix_lambda, fast(parts), fast(keys), values, head_gain.reshape(1, -1))


def shards(
    tokens,
    lengths,
    cache_keys,
    cache_values,
    norm0_gain,
    query_weight,
    key_weight,
    value_weight,
    mix_lambda,
    head_gain,
    out_weight,
    norm1_gain,
    group_ids,
    member_ids,
    group_weight,
    member_weights,
    expert_gate,
    expert_up,
    expert_down,
    norm2_gain,
):
    return layer(
        tokens,
        lengths,
        cache_keys,
        cache_values,
        norm0_gain,
        (query_weight, key_weight, value_weight),
        mix_lambda,
        head_gain,
        out_weight,
        norm1_gain,
        group_ids,
        member_ids,
        group_weight,
        member_weights,
        expert_gate,
        expert_up,
        expert_down,
        norm2_gain,
    )


def layer(
    tokens,
    lengths,
    cache_keys,
    cache_values,
    norm0_gain,
    proj_weights,
    mix_lambda,
    head_gain,
    out_weight,
    norm1_gain,
    group_ids,
    member_ids,
    group_weight,
    member_weights,
    expert_gate,
    expert_up,
    expert_down,
    norm2_gain,
):
    seqs, width = tokens.shape
    deep = lax.axis_size("z")
    experts = lax.axis_size(EP)
    halves = lax.axis_size("tp")
    side = lax.axis_index("tp")
    block = width // deep
    part = block // halves
    proj_cols = sum(w.shape[1] for w in proj_weights)
    expert_ids = group_ids[:, None] * EPG + member_ids
    share = group_weight[:, None] * member_weights

    weight_in = to_all(jnp.concatenate(proj_weights, 1), ROW).reshape(block, proj_cols)
    line_out = jnp.concatenate(around(out_weight.T, "x"), 0)
    blocks = around(line_out, "y")
    place = jnp.stack((lax.axis_index("y"), lax.axis_index("x")))
    weight_out = order(place, blocks)

    normed = layer_norm(tokens.astype(jnp.float32), norm0_gain).astype(jnp.bfloat16)
    named = jnp.repeat(expert_ids.astype(jnp.bfloat16), part, axis=1)
    leaving = jnp.concatenate(
        (
            normed.reshape(seqs, deep, block).transpose(1, 0, 2),
            jnp.broadcast_to(named[None], (deep, *named.shape)),
        ),
        2,
    )
    arrived = swap(leaving, "z")
    columns = arrived[:, :, :block].reshape(deep * seqs, block)
    partial = jnp.dot(columns, weight_in, preferred_element_type=jnp.float32)
    received = swap(partial.reshape(deep, seqs, proj_cols), "z")
    line = arrived.astype(jnp.float32).transpose(1, 0, 2)
    line_columns, line_ids = line[:, :, :block], line[:, :, block:]
    attended = run_attend(received, lengths, cache_keys, cache_values, mix_lambda, head_gain)
    everyone = swap(attended, "z")
    core = side.reshape(1)
    depth = lax.axis_index("z").reshape(1)
    partial_mix = outproj(everyone, weight_out)
    other_mix = lax.ppermute(partial_mix, "tp", ((0, 1), (1, 0)))
    sending, stream = build(core, partial_mix, other_mix, line_columns, line_ids, experts)
    slots = swap(sending, EP)
    laid = lay(depth, stream)
    pieces = [laid[0]]
    for j in range(1, deep):
        pairs = [(z, (z + j) % deep) for z in range(deep)]
        pieces.append(lax.ppermute(laid[j], "z", pairs))
    residual = settle(depth, core, norm1_gain, pieces)

    slots_other = lax.ppermute(slots, "tp", ((0, 1), (1, 0)))
    down = expert_down[0]
    hidden, given = run_hidden(
        core, slots, slots_other, norm1_gain, expert_gate[0], expert_up[0], down
    )
    taken = lax.ppermute(given, "tp", ((0, 1), (1, 0)))
    leaving = run_down(core, hidden, down, taken)
    returned = swap(leaving, EP)
    mixed, stats = run_combine(expert_ids, share, returned, residual)
    other_stats = lax.ppermute(stats, "tp", ((0, 1), (1, 0)))
    return finish(mixed, stats, other_stats, norm2_gain)


def solution(mesh):
    torus = Mesh(mesh.devices.reshape(8, 4, 4, mesh.shape["tp"]), ("z", "y", "x", "tp"))
    return jax.shard_map(
        shards,
        mesh=torus,
        in_specs=(
            P(EP, None),
            P(EP),
            P(EP, None, "tp"),
            P(EP, None, "tp"),
            P(),
            P(EP, "tp"),
            P(EP, "tp"),
            P(EP, "tp"),
            P("tp"),
            P(),
            P("tp", EP),
            P(),
            P(EP),
            P(EP, None),
            P(EP),
            P(EP, None),
            P(EP, None, "tp"),
            P(EP, None, "tp"),
            P(EP, "tp", None),
            P("tp"),
        ),
        out_specs=P(EP, "tp"),
        check_vma=False,
    )
```

time: 145 us -> 140 us (0.966)
  starting transfers between devices: 25.6 us -> 64.7 us
  blocking collectives: 58 us -> 22.3 us
  waiting for transfers between devices: 39.7 us -> 27 us
  local copies, waits for them, and re-layouts: 1.82 us -> 6.92 us
  other arithmetic: 9.99 us -> 7.58 us
    ppermute x0 -> x16, starting transfers between devices: none -> 32.1 us  [the longest x7 14.4 us: layer(): pieces.append(lax.ppermute(laid[j], 'z', pairs))]
    all_to_all x5, waiting for transfers between devices: 39.7 us -> 18.7 us  [swap(): return lax.all_to_all(array, axis, 0, 0, tiled=True)]
    all_to_all x2 -> x1, blocking collectives: 41.7 us -> 22.3 us  [swap(): return lax.all_to_all(array, axis, 0, 0, tiled=True)]
    all_gather x2 -> x0, blocking collectives: 11 us -> none  [the longest x1 6.8 us: layer(): mix = jnp.sum(lax.all_gather(partial_mix, 'tp'), 0).astype(jnp.bfloat16)]
    ppermute x0 -> x16, waiting for transfers between devices: none -> 7.16 us  [the longest x6 3.82 us: around(): lax.ppermute(array, axis, [(i, (i + j) % size) for i in range(size)])]
    all_to_all x5, starting transfers between devices: 25.2 us -> 32.1 us  [swap(): return lax.all_to_all(array, axis, 0, 0, tiled=True)]
    psum x1 -> x0, blocking collectives: 5.39 us -> none  [layer(): lax.psum(jnp.stack((jnp.sum(mixed, 1), jnp.sum(mixed * mixed, 1))), 'tp')]
    unnamed x12 -> x39, local copies, waits for them, and re-layouts: 0.89 us -> 4.79 us
  transfers between devices with their start and end apart: 6 -> 22, of which waited for: 5 -> 11; matrix products, arithmetic and copies ran while one was open for 2% -> 3% of each run, Pallas kernels for 0% -> 3%
where the time goes in v3:
time: 140 us; the launch traced here: 139 us
  starting transfers between devices  64.7 us (46%)
  waiting for transfers between devices  27 us (19%)
  blocking collectives  22.3 us (16%)
  Pallas kernels  8.84 us (6%)
  other arithmetic  7.58 us (5%)
  local copies, waits for them, and re-layouts  6.92 us (5%)
    all_to_all x5, starting transfers between devices, swap(): return lax.all_to_all(array, axis, 0, 0, tiled=True)  32.1 us
    all_to_all x1, blocking collectives, swap(): return lax.all_to_all(array, axis, 0, 0, tiled=True)  22.3 us
    all_to_all x5, waiting for transfers between devices, swap(): return lax.all_to_all(array, axis, 0, 0, tiled=True)  18.7 us
    ppermute x7, starting transfers between devices, layer(): pieces.append(lax.ppermute(laid[j], 'z', pairs))  14.4 us
    ppermute x1, starting transfers between devices, layer(): other_mix = lax.ppermute(partial_mix, 'tp', ((0, 1), (1, 0)))  7 us
    ppermute x6, starting transfers between devices, around(): lax.ppermute(array, axis, [(i, (i + j) % size) for i in range(size)])  5.12 us
    unnamed x39, local copies, waits for them, and re-layouts  4.79 us
    ppermute x6, waiting for transfers between devices, around(): lax.ppermute(array, axis, [(i, (i + j) % size) for i in range(size)])  3.82 us
  transfers between devices with their start and end apart: 22, of which 11 were waited for; matrix products, arithmetic and copies ran while one was open for 3% of the time, Pallas kernels for 3%

profile of v3, /device:TPU:1, one launch (start us, length us, event | category | flops | bytes accessed | tf_op | source)
XLA Modules:
  0.0 138.5 jit_solution(658446435939741180)
XLA Ops:
  4.9 9.0 %all-to-all-start = ((bf16[8,4,512]{2,1,0:T(4,128)(2,1)}), bf16[8,4,512]{2,1,0:T(4,128)(2,1)S(1)}, u32[]{:S(2)}, u32[]{:S(2)}) async-start(bf16[8,4,512]{2,1,0:T(4,128)(2,1)} %pad_maximum_fusion.2), calls=%async_computation | async-start | bytes 65536 | tf_op jit(solution)/shard_map/all_to_all | solution.py:19
  14.7 6.1 %all-to-all-done = bf16[8,4,512]{2,1,0:T(4,128)(2,1)S(1)} async-done(((bf16[8,4,512]{2,1,0:T(4,128)(2,1)}), bf16[8,4,512]{2,1,0:T(4,128)(2,1)S(1)}, u32[]{:S(2)}, u32[]{:S(2)}) %all-to-all-start) | async-done | bytes 32800 | tf_op jit(solution)/shard_map/all_to_all | solution.py:19
  21.7 6.8 %all-to-all-start.1 = ((bf16[16,16,1280]{2,1,0:T(8,128)(2,1)}), bf16[16,16,1280]{2,1,0:T(8,128)(2,1)S(1)}, u32[]{:S(2)}, u32[]{:S(2)}) async-start(bf16[16,16,1280]{2,1,0:T(8,128)(2,1)} %broadcast_in_dim.11), calls=%async_computation.1 | async-start | bytes 1310720 | tf_op jit(solution)/shard_map/all_to_all | solution.py:19
  28.5 10.9 %all-to-all-done.1 = bf16[16,16,1280]{2,1,0:T(8,128)(2,1)S(1)} async-done(((bf16[16,16,1280]{2,1,0:T(8,128)(2,1)}), bf16[16,16,1280]{2,1,0:T(8,128)(2,1)S(1)}, u32[]{:S(2)}, u32[]{:S(2)}) %all-to-all-start.1) | async-done | bytes 655392 | tf_op jit(solution)/shard_map/all_to_all | solution.py:19
  40.3 3.4 %all-to-all-start.2 = ((f32[8,4,1280]{2,1,0:T(4,128)}), f32[8,4,1280]{2,1,0:T(4,128)S(1)}, u32[]{:S(2)}, u32[]{:S(2)}) async-start(f32[8,4,1280]{2,1,0:T(4,128)} %fusion.5), calls=%async_computation.2 | async-start | bytes 327680 | tf_op jit(solution)/shard_map/all_to_all | solution.py:19
  44.4 1.5 %collective-permute-start.1 = (bf16[16,768]{1,0:T(8,128)(2,1)S(1)}, bf16[16,768]{1,0:T(8,128)(2,1)S(1)}, u32[]{:S(2)}, u32[]{:S(2)}) collective-permute-start(bf16[16,768]{1,0:T(8,128)(2,1)S(1)} %bitcast.36), channel_id=1, source_target_pairs={{0,4},{2,6},{4,0},{6,2},{1,5},{3,7},{5,1},{7,3},{8,12},{10,14},{12... | collective-permute-start | bytes 73736 | tf_op jit(solution)/shard_map/ppermute | solution.py:29
  46.4 2.1 %collective-permute-done.1 = bf16[16,768]{1,0:T(8,128)(2,1)S(1)} collective-permute-done((bf16[16,768]{1,0:T(8,128)(2,1)S(1)}, bf16[16,768]{1,0:T(8,128)(2,1)S(1)}, u32[]{:S(2)}, u32[]{:S(2)}) %collective-permute-start.1) | collective-permute-done | bytes 24608 | tf_op jit(solution)/shard_map/ppermute | solution.py:29
  48.5 1.2 collective-permute-done
  50.4 1.5 %collective-permute-start.4 = (bf16[64,768]{1,0:T(8,128)(2,1)}, bf16[64,768]{1,0:T(8,128)(2,1)S(1)}, u32[]{:S(2)}, u32[]{:S(2)}) collective-permute-start(bf16[64,768]{1,0:T(8,128)(2,1)} %pad_maximum_fusion.refs_0_), channel_id=1, source_target_pairs={{0,16},{8,24},{16,0},{24,8},{1,17},{9,25},{17,1},{25,9},{2,18},{10... | collective-permute-start | bytes 294920 | tf_op jit(solution)/shard_map/ppermute | solution.py:29
  51.9 1.4 %collective-permute-start.5 = (bf16[64,768]{1,0:T(8,128)(2,1)}, bf16[64,768]{1,0:T(8,128)(2,1)}, u32[]{:S(2)}, u32[]{:S(2)}) collective-permute-start(bf16[64,768]{1,0:T(8,128)(2,1)} %pad_maximum_fusion.refs_0_), channel_id=1, source_target_pairs={{0,24},{8,0},{16,8},{24,16},{1,25},{9,1},{17,9},{25,17},{2,26},{10... | collective-permute-start | bytes 294920 | tf_op jit(solution)/shard_map/ppermute | solution.py:29
  53.4 1.6 %copy-done.2 = bf16[4,1024,256]{2,1,0:T(8,128)(2,1)S(1)} copy-done((bf16[4,1024,256]{2,1,0:T(8,128)(2,1)S(1)}, bf16[4,1024,256]{2,1,0:T(8,128)(2,1)}, u32[]{:S(2)}) %copy-start.2) | copy-done | bytes 2097176
  55.0 2.8 %attend.1 = bf16[8,4,768]{2,1,0:T(4,128)(2,1)} custom-call(s32[4]{0:T(128)S(1)} %copy-done.12, f32[3]{0:T(128)S(1)} %copy-done.13, f32[8,4,1280]{2,1,0:T(4,128)S(1)} %all-to-all-done.2.parts_ref, bf16[4,1024,256]{2,1,0:T(8,128)(2,1)S(1)} %copy-done.1, bf16[4,1024,256]{2,1,0:T(8,128)(2,1)S(1)} %copy-done.2, f32[1,256]{1,0:T(1,128)S(1)} %bitcast.32), custom_call_target="tpu_custom_call" | custom-call | tf_op jit(solution)/shard_map/attend/pallas_call | solution.py:399
  57.8 6.7 %all-to-all-start.3 = ((bf16[8,4,768]{2,1,0:T(4,128)(2,1)}), bf16[8,4,768]{2,1,0:T(4,128)(2,1)}, u32[]{:S(2)}, u32[]{:S(2)}) async-start(bf16[8,4,768]{2,1,0:T(4,128)(2,1)} %attend.1), calls=%async_computation.3 | async-start | bytes 98304 | tf_op jit(solution)/shard_map/all_to_all | solution.py:19
  64.4 1.4 convert_bitcast_fusion
  69.9 1.7 %all-to-all-done.3.heads_ref = bf16[8,4,768]{2,1,0:T(4,128)(2,1)} async-done(((bf16[8,4,768]{2,1,0:T(4,128)(2,1)}), bf16[8,4,768]{2,1,0:T(4,128)(2,1)}, u32[]{:S(2)}, u32[]{:S(2)}) %all-to-all-start.3) | async-done | bytes 49184 | tf_op jit(solution)/shard_map/all_to_all | solution.py:19
  71.6 1.1 outproj.1.own_ref
  72.7 7.0 %collective-permute-start.6 = (f32[4,8,256]{2,1,0:T(8,128)S(1)}, f32[4,8,256]{2,1,0:T(8,128)S(1)}, u32[]{:S(2)}, u32[]{:S(2)}) collective-permute-start(f32[4,8,256]{2,1,0:T(8,128)S(1)} %outproj.1.own_ref), channel_id=1, source_target_pairs={{0,1},{1,0},{2,3},{3,2},{4,5},{5,4},{6,7},{7,6},{8,9},{9,8},{10,11... | collective-permute-start | bytes 98312 | tf_op jit(solution)/shard_map/ppermute | solution.py:511
  80.8 22.3 %all_to_all.30.own_ref = bf16[128,8,128]{2,1,0:T(8,128)(2,1)S(1)} all-to-all(bf16[128,8,128]{2,1,0:T(8,128)(2,1)S(1)} %get-tuple-element.19), channel_id=1, replica_groups=mesh['z'=8,'y'=4,'x'=4,'tp'=2] {'z','y','x'}, dimensions={0} | all-to-all | bytes 524288 | tf_op jit(solution)/shard_map/all_to_all | solution.py:19
  103.1 2.4 %collective-permute-start.7 = (bf16[128,8,128]{2,1,0:T(8,128)(2,1)S(1)}, bf16[128,8,128]{2,1,0:T(8,128)(2,1)S(1)}, u32[]{:S(2)}, u32[]{:S(2)}) collective-permute-start(bf16[128,8,128]{2,1,0:T(8,128)(2,1)S(1)} %all_to_all.30.own_ref), channel_id=1, source_target_pairs={{0,1},{1,0},{2,3},{3,2},{4,5},{5,4},{6,7},{7,6},{8,9},{9,8},{10,11... | collective-permute-start | bytes 786440 | tf_op jit(solution)/shard_map/ppermute | solution.py:521
  105.4 1.2 collective-permute-done.7.other_ref
  106.6 1.2 hidden.1
  108.3 1.2 collective-permute-done.8.taken_ref
  109.4 1.0 down.1
  110.5 6.3 %all-to-all-start.5 = ((bf16[128,8,128]{2,1,0:T(8,128)(2,1)}), bf16[128,8,128]{2,1,0:T(8,128)(2,1)S(1)}, u32[]{:S(2)}, u32[]{:S(2)}) async-start(bf16[128,8,128]{2,1,0:T(8,128)(2,1)} %down.1), calls=%async_computation.5 | async-start | bytes 524288 | tf_op jit(solution)/shard_map/all_to_all | solution.py:19
  117.5 2.3 %collective-permute-start.10 = (bf16[4,256]{1,0:T(4,128)(2,1)S(1)}, bf16[4,256]{1,0:T(4,128)(2,1)S(1)}, u32[]{:S(2)}, u32[]{:S(2)}) collective-permute-start(bf16[4,256]{1,0:T(4,128)(2,1)S(1)} %get-tuple-element.25), channel_id=1, source_target_pairs={{0,64},{32,96},{64,128},{96,160},{128,192},{160,224},{192,0},{224,... | collective-permute-start | bytes 6152 | tf_op jit(solution)/shard_map/ppermute | solution.py:518
  119.8 2.7 %collective-permute-start.11 = (bf16[4,256]{1,0:T(4,128)(2,1)S(1)}, bf16[4,256]{1,0:T(4,128)(2,1)S(1)}, u32[]{:S(2)}, u32[]{:S(2)}) collective-permute-start(bf16[4,256]{1,0:T(4,128)(2,1)S(1)} %get-tuple-element.26), channel_id=1, source_target_pairs={{0,96},{32,128},{64,160},{96,192},{128,224},{160,0},{192,32},{224,... | collective-permute-start | bytes 6152 | tf_op jit(solution)/shard_map/ppermute | solution.py:518
  122.5 1.6 %collective-permute-start.12 = (bf16[4,256]{1,0:T(4,128)(2,1)S(1)}, bf16[4,256]{1,0:T(4,128)(2,1)S(1)}, u32[]{:S(2)}, u32[]{:S(2)}) collective-permute-start(bf16[4,256]{1,0:T(4,128)(2,1)S(1)} %get-tuple-element.27), channel_id=1, source_target_pairs={{0,128},{32,160},{64,192},{96,224},{128,0},{160,32},{192,64},{224,... | collective-permute-start | bytes 6152 | tf_op jit(solution)/shard_map/ppermute | solution.py:518
  124.2 2.9 %collective-permute-start.13 = (bf16[4,256]{1,0:T(4,128)(2,1)S(1)}, bf16[4,256]{1,0:T(4,128)(2,1)S(1)}, u32[]{:S(2)}, u32[]{:S(2)}) collective-permute-start(bf16[4,256]{1,0:T(4,128)(2,1)S(1)} %get-tuple-element.28), channel_id=1, source_target_pairs={{0,160},{32,192},{64,224},{96,0},{128,32},{160,64},{192,96},{224,1... | collective-permute-start | bytes 6152 | tf_op jit(solution)/shard_map/ppermute | solution.py:518
  127.1 3.1 %collective-permute-start.14 = (bf16[4,256]{1,0:T(4,128)(2,1)S(1)}, bf16[4,256]{1,0:T(4,128)(2,1)S(1)}, u32[]{:S(2)}, u32[]{:S(2)}) collective-permute-start(bf16[4,256]{1,0:T(4,128)(2,1)S(1)} %get-tuple-element.29), channel_id=1, source_target_pairs={{0,192},{32,224},{64,0},{96,32},{128,64},{160,96},{192,128},{224,1... | collective-permute-start | bytes 6152 | tf_op jit(solution)/shard_map/ppermute | solution.py:518
  130.2 1.1 collective-permute-start.15
  131.7 1.3 collective-permute-done.15.refs_7_
  133.8 3.3 %collective-permute-start.16 = (f32[8,128]{1,0:T(8,128)S(1)}, f32[8,128]{1,0:T(8,128)S(1)}, u32[]{:S(2)}, u32[]{:S(2)}) collective-permute-start(f32[8,128]{1,0:T(8,128)S(1)} %get-tuple-element.32.own_ref), channel_id=1, source_target_pairs={{0,1},{1,0},{2,3},{3,2},{4,5},{5,4},{6,7},{7,6},{8,9},{9,8},{10,11... | collective-permute-start | bytes 12296 | tf_op jit(solution)/shard_map/ppermute | solution.py:530
  (85 shorter events, 18.5 us)
Async XLA Ops:
  0.0 43.7 %copy-start.15 = (bf16[768,16]{0,1:T(8,128)(2,1)S(1)}, bf16[768,16]{0,1:T(8,128)(2,1)}, u32[]{:S(2)}) copy-start(bf16[768,16]{0,1:T(8,128)(2,1)} %param.30) | copy-start | bytes 73732
  0.0 53.3 %copy-start.12 = (s32[4]{0:T(128)S(1)}, s32[4]{0:T(128)}, u32[]{:S(2)}) copy-start(s32[4]{0:T(128)} %lengths_ref.1) | copy-start | bytes 52
  0.0 53.3 %copy-start.13 = (f32[3]{0:T(128)S(1)}, f32[3]{0:T(128)}, u32[]{:S(2)}) copy-start(f32[3]{0:T(128)} %lambda_ref.1) | copy-start | bytes 40
  0.0 53.3 %copy-start.1 = (bf16[4,1024,256]{2,1,0:T(8,128)(2,1)S(1)}, bf16[4,1024,256]{2,1,0:T(8,128)(2,1)}, u32[]{:S(2)}) copy-start(bf16[4,1024,256]{2,1,0:T(8,128)(2,1)} %keys_ref.1) | copy-start | bytes 6291460
  0.0 53.3 %copy-start.11 = (f32[256]{0:T(256)S(1)}, f32[256]{0:T(256)}, u32[]{:S(2)}) copy-start(f32[256]{0:T(256)} %param.29) | copy-start | bytes 3076
  4.9 15.9 %all-to-all-start = ((bf16[8,4,512]{2,1,0:T(4,128)(2,1)}), bf16[8,4,512]{2,1,0:T(4,128)(2,1)S(1)}, u32[]{:S(2)}, u32[]{:S(2)}) async-start(bf16[8,4,512]{2,1,0:T(4,128)(2,1)} %pad_maximum_fusion.2), calls=%async_computation | async-start | bytes 65536 | tf_op jit(solution)/shard_map/all_to_all | solution.py:19
  20.8 32.5 %copy-start.14 = (bf16[8,4,512]{2,1,0:T(4,128)(2,1)}, bf16[8,4,512]{2,1,0:T(4,128)(2,1)S(1)}, u32[]{:S(2)}) copy-start(bf16[8,4,512]{2,1,0:T(4,128)(2,1)S(1)} %all-to-all-done) | copy-start | bytes 98308
  21.7 17.7 %all-to-all-start.1 = ((bf16[16,16,1280]{2,1,0:T(8,128)(2,1)}), bf16[16,16,1280]{2,1,0:T(8,128)(2,1)S(1)}, u32[]{:S(2)}, u32[]{:S(2)}) async-start(bf16[16,16,1280]{2,1,0:T(8,128)(2,1)} %broadcast_in_dim.11), calls=%async_computation.1 | async-start | bytes 1310720 | tf_op jit(solution)/shard_map/all_to_all | solution.py:19
  40.3 13.1 %all-to-all-start.2 = ((f32[8,4,1280]{2,1,0:T(4,128)}), f32[8,4,1280]{2,1,0:T(4,128)S(1)}, u32[]{:S(2)}, u32[]{:S(2)}) async-start(f32[8,4,1280]{2,1,0:T(4,128)} %fusion.5), calls=%async_computation.2 | async-start | bytes 327680 | tf_op jit(solution)/shard_map/all_to_all | solution.py:19
  43.7 2.8 %collective-permute-start.2 = (bf16[16,768]{1,0:T(8,128)(2,1)S(1)}, bf16[16,768]{1,0:T(8,128)(2,1)S(1)}, u32[]{:S(2)}, u32[]{:S(2)}) collective-permute-start(bf16[16,768]{1,0:T(8,128)(2,1)S(1)} %bitcast.35), channel_id=1, source_target_pairs={{0,6},{2,0},{4,2},{6,4},{1,7},{3,1},{5,3},{7,5},{8,14},{10,8},{12,... | collective-permute-start | bytes 73736 | tf_op jit(solution)/shard_map/ppermute | solution.py:29
  44.4 4.2 %collective-permute-start.1 = (bf16[16,768]{1,0:T(8,128)(2,1)S(1)}, bf16[16,768]{1,0:T(8,128)(2,1)S(1)}, u32[]{:S(2)}, u32[]{:S(2)}) collective-permute-start(bf16[16,768]{1,0:T(8,128)(2,1)S(1)} %bitcast.36), channel_id=1, source_target_pairs={{0,4},{2,6},{4,0},{6,2},{1,5},{3,7},{5,1},{7,3},{8,12},{10,14},{12... | collective-permute-start | bytes 73736 | tf_op jit(solution)/shard_map/ppermute | solution.py:29
  45.9 3.9 %collective-permute-start = (bf16[16,768]{1,0:T(8,128)(2,1)S(1)}, bf16[16,768]{1,0:T(8,128)(2,1)S(1)}, u32[]{:S(2)}, u32[]{:S(2)}) collective-permute-start(bf16[16,768]{1,0:T(8,128)(2,1)S(1)} %bitcast.37), channel_id=1, source_target_pairs={{0,2},{2,4},{4,6},{6,0},{1,3},{3,5},{5,7},{7,1},{8,10},{10,12},{12... | collective-permute-start | bytes 73736 | tf_op jit(solution)/shard_map/ppermute | solution.py:29
  50.4 15.4 %collective-permute-start.3 = (bf16[64,768]{1,0:T(8,128)(2,1)}, bf16[64,768]{1,0:T(8,128)(2,1)S(1)}, u32[]{:S(2)}, u32[]{:S(2)}) collective-permute-start(bf16[64,768]{1,0:T(8,128)(2,1)} %pad_maximum_fusion.refs_0_), channel_id=1, source_target_pairs={{0,8},{8,16},{16,24},{24,0},{1,9},{9,17},{17,25},{25,1},{2,10},{10... | collective-permute-start | bytes 294920 | tf_op jit(solution)/shard_map/ppermute | solution.py:29
  50.4 16.0 %collective-permute-start.4 = (bf16[64,768]{1,0:T(8,128)(2,1)}, bf16[64,768]{1,0:T(8,128)(2,1)S(1)}, u32[]{:S(2)}, u32[]{:S(2)}) collective-permute-start(bf16[64,768]{1,0:T(8,128)(2,1)} %pad_maximum_fusion.refs_0_), channel_id=1, source_target_pairs={{0,16},{8,24},{16,0},{24,8},{1,17},{9,25},{17,1},{25,9},{2,18},{10... | collective-permute-start | bytes 294920 | tf_op jit(solution)/shard_map/ppermute | solution.py:29
  51.9 15.2 %collective-permute-start.5 = (bf16[64,768]{1,0:T(8,128)(2,1)}, bf16[64,768]{1,0:T(8,128)(2,1)}, u32[]{:S(2)}, u32[]{:S(2)}) collective-permute-start(bf16[64,768]{1,0:T(8,128)(2,1)} %pad_maximum_fusion.refs_0_), channel_id=1, source_target_pairs={{0,24},{8,0},{16,8},{24,16},{1,25},{9,1},{17,9},{25,17},{2,26},{10... | collective-permute-start | bytes 294920 | tf_op jit(solution)/shard_map/ppermute | solution.py:29
  55.0 51.6 %copy-start.4 = (bf16[1,2048,256]{2,1,0:T(8,128)(2,1)S(1)}, bf16[1,2048,256]{2,1,0:T(8,128)(2,1)}, u32[]{:S(2)}) copy-start(bf16[1,2048,256]{2,1,0:T(8,128)(2,1)} %param.37) | copy-start | bytes 3145732
  55.0 51.6 %copy-start.9 = (f32[2048]{0:T(1024)S(1)}, f32[2048]{0:T(1024)}, u32[]{:S(2)}) copy-start(f32[2048]{0:T(1024)} %param.31) | copy-start | bytes 24580
  57.7 48.9 %copy-start = (bf16[1,256,2048]{2,1,0:T(8,128)(2,1)S(1)}, bf16[1,256,2048]{2,1,0:T(8,128)(2,1)}, u32[]{:S(2)}) copy-start(bf16[1,256,2048]{2,1,0:T(8,128)(2,1)} %param.38) | copy-start | bytes 3145732
  57.8 48.9 %copy-start.3 = (bf16[1,2048,256]{2,1,0:T(8,128)(2,1)S(1)}, bf16[1,2048,256]{2,1,0:T(8,128)(2,1)}, u32[]{:S(2)}) copy-start(bf16[1,2048,256]{2,1,0:T(8,128)(2,1)} %param.36) | copy-start | bytes 3145732
  57.8 13.8 %all-to-all-start.3 = ((bf16[8,4,768]{2,1,0:T(4,128)(2,1)}), bf16[8,4,768]{2,1,0:T(4,128)(2,1)}, u32[]{:S(2)}, u32[]{:S(2)}) async-start(bf16[8,4,768]{2,1,0:T(4,128)(2,1)} %attend.1), calls=%async_computation.3 | async-start | bytes 98304 | tf_op jit(solution)/shard_map/all_to_all | solution.py:19
  72.7 7.9 %collective-permute-start.6 = (f32[4,8,256]{2,1,0:T(8,128)S(1)}, f32[4,8,256]{2,1,0:T(8,128)S(1)}, u32[]{:S(2)}, u32[]{:S(2)}) collective-permute-start(f32[4,8,256]{2,1,0:T(8,128)S(1)} %outproj.1.own_ref), channel_id=1, source_target_pairs={{0,1},{1,0},{2,3},{3,2},{4,5},{5,4},{6,7},{7,6},{8,9},{9,8},{10,11... | collective-permute-start | bytes 98312 | tf_op jit(solution)/shard_map/ppermute | solution.py:511
  103.1 3.5 %collective-permute-start.7 = (bf16[128,8,128]{2,1,0:T(8,128)(2,1)S(1)}, bf16[128,8,128]{2,1,0:T(8,128)(2,1)S(1)}, u32[]{:S(2)}, u32[]{:S(2)}) collective-permute-start(bf16[128,8,128]{2,1,0:T(8,128)(2,1)S(1)} %all_to_all.30.own_ref), channel_id=1, source_target_pairs={{0,1},{1,0},{2,3},{3,2},{4,5},{5,4},{6,7},{7,6},{8,9},{9,8},{10,11... | collective-permute-start | bytes 786440 | tf_op jit(solution)/shard_map/ppermute | solution.py:521
  107.8 1.6 %collective-permute-start.8 = (bf16[128,8,128]{2,1,0:T(8,128)(2,1)S(1)}, bf16[128,8,128]{2,1,0:T(8,128)(2,1)S(1)}, u32[]{:S(2)}, u32[]{:S(2)}) collective-permute-start(bf16[128,8,128]{2,1,0:T(8,128)(2,1)S(1)} %get-tuple-element.21), channel_id=1, source_target_pairs={{0,1},{1,0},{2,3},{3,2},{4,5},{5,4},{6,7},{7,6},{8,9},{9,8},{10,11... | collective-permute-start | bytes 786440 | tf_op jit(solution)/shard_map/ppermute | solution.py:526
  110.5 22.7 %all-to-all-start.5 = ((bf16[128,8,128]{2,1,0:T(8,128)(2,1)}), bf16[128,8,128]{2,1,0:T(8,128)(2,1)S(1)}, u32[]{:S(2)}, u32[]{:S(2)}) async-start(bf16[128,8,128]{2,1,0:T(8,128)(2,1)} %down.1), calls=%async_computation.5 | async-start | bytes 524288 | tf_op jit(solution)/shard_map/all_to_all | solution.py:19
  116.9 10.3 %collective-permute-start.9 = (bf16[4,256]{1,0:T(4,128)(2,1)S(1)}, bf16[4,256]{1,0:T(4,128)(2,1)S(1)}, u32[]{:S(2)}, u32[]{:S(2)}) collective-permute-start(bf16[4,256]{1,0:T(4,128)(2,1)S(1)} %get-tuple-element.24), channel_id=1, source_target_pairs={{0,32},{32,64},{64,96},{96,128},{128,160},{160,192},{192,224},{224... | collective-permute-start | bytes 6152 | tf_op jit(solution)/shard_map/ppermute | solution.py:518
  117.5 12.7 %collective-permute-start.10 = (bf16[4,256]{1,0:T(4,128)(2,1)S(1)}, bf16[4,256]{1,0:T(4,128)(2,1)S(1)}, u32[]{:S(2)}, u32[]{:S(2)}) collective-permute-start(bf16[4,256]{1,0:T(4,128)(2,1)S(1)} %get-tuple-element.25), channel_id=1, source_target_pairs={{0,64},{32,96},{64,128},{96,160},{128,192},{160,224},{192,0},{224,... | collective-permute-start | bytes 6152 | tf_op jit(solution)/shard_map/ppermute | solution.py:518
  119.8 11.8 %collective-permute-start.11 = (bf16[4,256]{1,0:T(4,128)(2,1)S(1)}, bf16[4,256]{1,0:T(4,128)(2,1)S(1)}, u32[]{:S(2)}, u32[]{:S(2)}) collective-permute-start(bf16[4,256]{1,0:T(4,128)(2,1)S(1)} %get-tuple-element.26), channel_id=1, source_target_pairs={{0,96},{32,128},{64,160},{96,192},{128,224},{160,0},{192,32},{224,... | collective-permute-start | bytes 6152 | tf_op jit(solution)/shard_map/ppermute | solution.py:518
  122.5 9.1 %collective-permute-start.12 = (bf16[4,256]{1,0:T(4,128)(2,1)S(1)}, bf16[4,256]{1,0:T(4,128)(2,1)S(1)}, u32[]{:S(2)}, u32[]{:S(2)}) collective-permute-start(bf16[4,256]{1,0:T(4,128)(2,1)S(1)} %get-tuple-element.27), channel_id=1, source_target_pairs={{0,128},{32,160},{64,192},{96,224},{128,0},{160,32},{192,64},{224,... | collective-permute-start | bytes 6152 | tf_op jit(solution)/shard_map/ppermute | solution.py:518
  124.2 7.5 %collective-permute-start.13 = (bf16[4,256]{1,0:T(4,128)(2,1)S(1)}, bf16[4,256]{1,0:T(4,128)(2,1)S(1)}, u32[]{:S(2)}, u32[]{:S(2)}) collective-permute-start(bf16[4,256]{1,0:T(4,128)(2,1)S(1)} %get-tuple-element.28), channel_id=1, source_target_pairs={{0,160},{32,192},{64,224},{96,0},{128,32},{160,64},{192,96},{224,1... | collective-permute-start | bytes 6152 | tf_op jit(solution)/shard_map/ppermute | solution.py:518
  127.1 4.5 %collective-permute-start.14 = (bf16[4,256]{1,0:T(4,128)(2,1)S(1)}, bf16[4,256]{1,0:T(4,128)(2,1)S(1)}, u32[]{:S(2)}, u32[]{:S(2)}) collective-permute-start(bf16[4,256]{1,0:T(4,128)(2,1)S(1)} %get-tuple-element.29), channel_id=1, source_target_pairs={{0,192},{32,224},{64,0},{96,32},{128,64},{160,96},{192,128},{224,1... | collective-permute-start | bytes 6152 | tf_op jit(solution)/shard_map/ppermute | solution.py:518
  130.2 2.7 %collective-permute-start.15 = (bf16[4,256]{1,0:T(4,128)(2,1)S(1)}, bf16[4,256]{1,0:T(4,128)(2,1)S(1)}, u32[]{:S(2)}, u32[]{:S(2)}) collective-permute-start(bf16[4,256]{1,0:T(4,128)(2,1)S(1)} %get-tuple-element.30), channel_id=1, source_target_pairs={{0,224},{32,0},{64,32},{96,64},{128,96},{160,128},{192,160},{224,1... | collective-permute-start | bytes 6152 | tf_op jit(solution)/shard_map/ppermute | solution.py:518
  133.8 4.1 %collective-permute-start.16 = (f32[8,128]{1,0:T(8,128)S(1)}, f32[8,128]{1,0:T(8,128)S(1)}, u32[]{:S(2)}, u32[]{:S(2)}) collective-permute-start(f32[8,128]{1,0:T(8,128)S(1)} %get-tuple-element.32.own_ref), channel_id=1, source_target_pairs={{0,1},{1,0},{2,3},{3,2},{4,5},{5,4},{6,7},{7,6},{8,9},{9,8},{10,11... | collective-permute-start | bytes 12296 | tf_op jit(solution)/shard_map/ppermute | solution.py:530
  (8 other events, 84.0 us)

commit v4 on v3

--- a/solution.py
+++ b/solution.py
@@ -23,18 +23,21 @@
     return swap(jnp.broadcast_to(array[None], (lax.axis_size(axis), *array.shape)), axis)
 
 
-def around(array, axis):
-    size = lax.axis_size(axis)
-    return [array] + [
-        lax.ppermute(array, axis, [(i, (i + j) % size) for i in range(size)])
-        for j in range(1, size)
-    ]
-
-
-def layer_norm(values, gain):
-    mean = jnp.mean(values, -1, keepdims=True)
-    spread = jnp.mean(jnp.square(values - mean), -1, keepdims=True)
-    return (values - mean) * lax.rsqrt(spread + EPS) * gain
+def trade(array):
+    return lax.ppermute(array, "tp", ((0, 1), (1, 0)))
+
+
+def send(blocks):
+    deep = lax.axis_size("z")
+    moved = []
+    for j in range(1, len(blocks)):
+        pairs = [
+            (2 * z + t, 2 * ((z + (1 - 2 * t) * j) % deep) + t)
+            for z in range(deep)
+            for t in range(2)
+        ]
+        moved.append(lax.ppermute(blocks[j], ("z", "tp"), pairs))
+    return moved
 
 
 def fast(array):
@@ -43,38 +46,98 @@
 
 VM = pl.BlockSpec(memory_space=pltpu.VMEM)
 SM = pl.BlockSpec(memory_space=pltpu.SMEM)
+FAR = pl.BlockSpec(memory_space=pltpu.HBM)
 SMALL = pltpu.CompilerParams(vmem_limit_bytes=16 * 2**20)
 
 
-def order_kernel(place_ref, *refs):
-    out_ref = refs[-1]
-    tall, wide = len(refs) - 1, refs[0].shape[0] // 16
-    for dy in range(tall):
-        for dx in range(wide):
-            y = lax.rem(place_ref[0] + tall - dy, tall)
-            x = lax.rem(place_ref[1] + wide - dx, wide)
-            at = pl.multiple_of((y * wide + x) * 16, 16)
-            out_ref[pl.ds(at, 16)] = refs[dy][dx * 16 : (dx + 1) * 16]
-
-
-def order(place, blocks):
-    rows, cols = blocks[0].shape
-    return pl.pallas_call(
-        order_kernel,
-        out_shape=jax.ShapeDtypeStruct((rows * len(blocks), cols), blocks[0].dtype),
-        in_specs=[SM] + [VM] * len(blocks),
+def norm_kernel(place_ref, side_ref, group_ref, member_ref, tokens_ref, gain_ref, *refs):
+    out_refs, row_ref = refs[:-1], refs[-1]
+    deep = 2 * (len(out_refs) - 1)
+    seqs, width = tokens_ref.shape
+    block = width // deep
+    values = tokens_ref[...].astype(jnp.float32)
+    off = values - jnp.mean(values, 1, keepdims=True)
+    scale = lax.rsqrt(jnp.mean(off * off, 1, keepdims=True) + EPS)
+    row_ref[...] = off * scale * gain_ref[...]
+    names = []
+    for i in range(seqs):
+        ids = [group_ref[i] * EPG + member_ref[2 * i + k] for k in range(2)]
+        names.append(jnp.concatenate([jnp.full((1, block // 2), e, jnp.int32) for e in ids], 1))
+    named = jnp.concatenate(names, 0).astype(jnp.float32).astype(jnp.bfloat16)
+    for j, out_ref in enumerate(out_refs):
+        at = pl.multiple_of(apart(place_ref, side_ref, j, deep) * block, block)
+        out_ref[:, :block] = row_ref[:, pl.ds(at, block)].astype(jnp.bfloat16)
+        out_ref[:, block:] = named
+
+
+def norm(place, side, groups, members, tokens, gain, deep):
+    seqs, width = tokens.shape
+    count = deep // 2 + 1
+    return pl.pallas_call(
+        norm_kernel,
+        out_shape=(jax.ShapeDtypeStruct((seqs, 2 * width // deep), jnp.bfloat16),) * count,
+        in_specs=[SM, SM, SM, SM, VM, VM],
+        out_specs=(VM,) * count,
+        scratch_shapes=[pltpu.VMEM((seqs, width), jnp.float32)],
+        compiler_params=SMALL,
+        name="norm",
+    )(place, side, groups, members.reshape(-1), tokens, gain.reshape(1, -1))
+
+
+def project_kernel(place_ref, side_ref, weight_ref, *refs):
+    blocks, out_ref = refs[:-1], refs[-1]
+    deep = len(blocks)
+    width = weight_ref.shape[0]
+    seqs = blocks[0].shape[0]
+    columns = jnp.concatenate([b[:, :width].astype(jnp.float32) for b in blocks], 0)
+    partial = jnp.dot(
+        columns.astype(jnp.bfloat16),
+        weight_ref[:, : out_ref.shape[2]],
+        preferred_element_type=jnp.float32,
+    )
+    for j in range(deep):
+        out_ref[apart(place_ref, side_ref, -j, deep)] = partial[j * seqs : (j + 1) * seqs]
+
+
+def project(place, side, weights, blocks, cols):
+    return pl.pallas_call(
+        project_kernel,
+        out_shape=jax.ShapeDtypeStruct((len(blocks), blocks[0].shape[0], cols), jnp.float32),
+        in_specs=[SM, SM, VM] + [VM] * len(blocks),
         out_specs=VM,
         compiler_params=SMALL,
-        name="order",
-    )(place, *(fast(b) for b in blocks))
+        name="project",
+    )(place, side, fast(weights), *blocks)
+
+
+def line_kernel(place_ref, side_ref, *refs):
+    blocks, out_ref = refs[:-1], refs[-1]
+    deep = len(blocks)
+    for j in range(deep):
+        z = apart(place_ref, side_ref, -j, deep)
+        values = blocks[j][...].astype(jnp.float32)
+        for i in range(values.shape[0]):
+            out_ref[i, pl.ds(z, 1), :] = values[i : i + 1]
+
+
+def in_line(place, side, blocks):
+    seqs, cols = blocks[0].shape
+    return pl.pallas_call(
+        line_kernel,
+        out_shape=jax.ShapeDtypeStruct((seqs, len(blocks), cols), jnp.float32),
+        in_specs=[SM, SM] + [VM] * len(blocks),
+        out_specs=VM,
+        compiler_params=SMALL,
+        name="line",
+    )(place, side, *blocks)
 
 
 def outproj_kernel(heads_ref, weight_ref, out_ref, rows_ref):
-    deep, seqs, _ = heads_ref.shape
+    deep, seqs, cols = heads_ref.shape
     heads = jnp.concatenate([heads_ref[d].astype(jnp.float32) for d in range(deep)], 0)
     rows_ref[...] = lax.dot_general(
         heads.astype(jnp.bfloat16),
-        weight_ref[...],
+        weight_ref[:, weight_ref.shape[1] - cols :],
         (((1,), (1,)), ((), ())),
         preferred_element_type=jnp.float32,
     )
@@ -98,16 +161,17 @@
     )(fast(heads), fast(weight))
 
 
-def build_kernel(side_ref, own_ref, other_ref, columns_ref, ids_ref, out_ref, stream_ref):
+def build_kernel(side_ref, own_ref, other_ref, line_ref, out_ref, stream_ref):
     seqs, _, block = own_ref.shape
     part = block // 2
     at = pl.multiple_of(side_ref[0] * part, part)
     rows, names = [], []
     for i in range(seqs):
         mix = (own_ref[i] + other_ref[i]).astype(jnp.bfloat16).astype(jnp.float32)
-        stream_ref[i] = (ALPHA * columns_ref[i] + mix).astype(jnp.bfloat16).astype(jnp.float32)
+        stream = ALPHA * line_ref[i, :, :block] + mix
+        stream_ref[i] = stream.astype(jnp.bfloat16).astype(jnp.float32)
         rows.append(stream_ref[i, :, pl.ds(at, part)])
-        names.append([ids_ref[i, :, k * part : (k + 1) * part] for k in range(2)])
+        names.append([line_ref[i, :, block + k * part : block + (k + 1) * part] for k in range(2)])
     for e in range(out_ref.shape[0]):
         value = jnp.zeros_like(rows[0])
         for row, (one, two) in zip(rows, names, strict=True):
@@ -115,7 +179,7 @@
         out_ref[e] = value.astype(jnp.bfloat16)
 
 
-def build(side, own, other, columns, ids, experts):
+def build(side, own, other, line, experts):
     seqs, deep, block = own.shape
     return pl.pallas_call(
         build_kernel,
@@ -123,31 +187,36 @@
             jax.ShapeDtypeStruct((experts, deep, block // 2), jnp.bfloat16),
             jax.ShapeDtypeStruct((seqs, deep, block), jnp.float32),
         ),
-        in_specs=[SM] + [VM] * 4,
+        in_specs=[SM] + [VM] * 3,
         out_specs=(VM, VM),
         compiler_params=SMALL,
         name="build",
-    )(side, fast(own), fast(other), fast(columns), fast(ids))
-
-
-def lay_kernel(place_ref, stream_ref, *out_refs):
+    )(side, fast(own), fast(other), fast(line))
+
+
+def apart(place_ref, side_ref, steps, deep):
+    return lax.rem(place_ref[0] + deep + (1 - 2 * side_ref[0]) * steps, deep)
+
+
+def lay_kernel(place_ref, side_ref, stream_ref, *out_refs):
     seqs, deep, _ = stream_ref.shape
     for j, out_ref in enumerate(out_refs):
-        z = lax.rem(place_ref[0] + j, deep)
+        z = apart(place_ref, side_ref, j, deep)
         rows = [stream_ref[i, pl.ds(z, 1), :] for i in range(seqs)]
         out_ref[...] = jnp.concatenate(rows, 0).astype(jnp.bfloat16)
 
 
-def lay(place, stream):
+def lay(place, side, stream):
     seqs, deep, block = stream.shape
+    count = deep // 2 + 1
     return pl.pallas_call(
         lay_kernel,
-        out_shape=(jax.ShapeDtypeStruct((seqs, block), jnp.bfloat16),) * deep,
-        in_specs=[SM, VM],
-        out_specs=(VM,) * deep,
+        out_shape=(jax.ShapeDtypeStruct((seqs, block), jnp.bfloat16),) * count,
+        in_specs=[SM, SM, VM],
+        out_specs=(VM,) * count,
         compiler_params=SMALL,
         name="lay",
-    )(place, stream)
+    )(place, side, stream)
 
 
 def settle_kernel(place_ref, side_ref, gain_ref, *refs):
@@ -155,8 +224,7 @@
     deep = len(refs) - 2
     block = refs[0].shape[1]
     for j in range(deep):
-        z = lax.rem(place_ref[0] + deep - j, deep)
-        at = pl.multiple_of(z * block, block)
+        at = pl.multiple_of(apart(place_ref, side_ref, -j, deep) * block, block)
         row_ref[:, pl.ds(at, block)] = refs[j][...].astype(jnp.float32)
     values = row_ref[...]
     mean = jnp.mean(values, 1, keepdims=True)
@@ -323,10 +391,23 @@
 
 
 def attend_kernel(
-    lengths_ref, lambda_ref, parts_ref, keys_ref, far_ref, gain_ref, out_ref, values_ref, arrived
+    lengths_ref,
+    lambda_ref,
+    parts_ref,
+    far_keys_ref,
+    far_values_ref,
+    gain_ref,
+    out_ref,
+    keys_ref,
+    values_ref,
+    done,
 ):
-    loading = pltpu.make_async_copy(far_ref, values_ref, arrived)
-    loading.start()
+    loads = []
+    for k, (far, near) in enumerate(((far_keys_ref, keys_ref), (far_values_ref, values_ref))):
+        loads.append([])
+        for s in range(near.shape[0]):
+            loads[k].append(pltpu.make_async_copy(far.at[s], near.at[s], done.at[k, s]))
+            loads[k][s].start()
     deep, seqs, _ = parts_ref.shape
     _, width = keys_ref.shape[1:]
     hwidth = width // 2
@@ -349,6 +430,7 @@
         grid = jnp.concatenate(ones + twos, 0)
         new_key = total[s : s + 1, at : at + width]
         fresh.append(jnp.sum(grid * new_key, 1, keepdims=True))
+        loads[0][s].wait()
         scores.append(
             lax.dot_general(
                 grid.astype(jnp.bfloat16),
@@ -376,13 +458,13 @@
     maps = spread * inverse
     itself = itself * inverse
     gain = gain_ref[...]
-    loading.wait()
     lines = []
     for s in range(seqs):
         one, two = s * rows, s * rows + pad
         weight = maps[one:two] - lam * maps[two : two + pad]
         fresh_weight = itself[one:two] - lam * itself[two : two + pad]
         weight = jnp.concatenate((weight, jnp.zeros_like(weight)), 0).astype(jnp.bfloat16)
+        loads[1][s].wait()
         out = jnp.dot(weight, values_ref[s], preferred_element_type=f32)[:pad]
         new_value = total[s : s + 1, at + width : at + 2 * width]
         out = out + fresh_weight.astype(jnp.bfloat16).astype(f32) * new_value
@@ -399,12 +481,16 @@
     return pl.pallas_call(
         attend_kernel,
         out_shape=pltpu.VMEM((deep, seqs, cols), jnp.bfloat16),
-        in_specs=[SM, SM, VM, VM, pl.BlockSpec(memory_space=pl.ANY), VM],
+        in_specs=[SM, SM, VM, FAR, FAR, VM],
         out_specs=VM,
-        scratch_shapes=[pltpu.VMEM(values.shape, values.dtype), pltpu.SemaphoreType.DMA],
+        scratch_shapes=[
+            pltpu.VMEM(keys.shape, keys.dtype),
+            pltpu.VMEM(values.shape, values.dtype),
+            pltpu.SemaphoreType.DMA((2, seqs)),
+        ],
         compiler_params=SMALL,
         name="attend",
-    )(lengths, mix_lambda, fast(parts), fast(keys), values, head_gain.reshape(1, -1))
+    )(lengths, mix_lambda, fast(parts), keys, values, head_gain.reshape(1, -1))
 
 
 def shards(
@@ -471,63 +557,49 @@
     expert_down,
     norm2_gain,
 ):
-    seqs, width = tokens.shape
+    width = tokens.shape[1]
     deep = lax.axis_size("z")
     experts = lax.axis_size(EP)
-    halves = lax.axis_size("tp")
     side = lax.axis_index("tp")
     block = width // deep
-    part = block // halves
     proj_cols = sum(w.shape[1] for w in proj_weights)
     expert_ids = group_ids[:, None] * EPG + member_ids
     share = group_weight[:, None] * member_weights
 
-    weight_in = to_all(jnp.concatenate(proj_weights, 1), ROW).reshape(block, proj_cols)
-    line_out = jnp.concatenate(around(out_weight.T, "x"), 0)
-    blocks = around(line_out, "y")
-    place = jnp.stack((lax.axis_index("y"), lax.axis_index("x")))
-    weight_out = order(place, blocks)
-
-    normed = layer_norm(tokens.astype(jnp.float32), norm0_gain).astype(jnp.bfloat16)
-    named = jnp.repeat(expert_ids.astype(jnp.bfloat16), part, axis=1)
-    leaving = jnp.concatenate(
-        (
-            normed.reshape(seqs, deep, block).transpose(1, 0, 2),
-            jnp.broadcast_to(named[None], (deep, *named.shape)),
-        ),
-        2,
-    )
-    arrived = swap(leaving, "z")
-    columns = arrived[:, :, :block].reshape(deep * seqs, block)
-    partial = jnp.dot(columns, weight_in, preferred_element_type=jnp.float32)
-    received = swap(partial.reshape(deep, seqs, proj_cols), "z")
-    line = arrived.astype(jnp.float32).transpose(1, 0, 2)
-    line_columns, line_ids = line[:, :, :block], line[:, :, block:]
-    attended = run_attend(received, lengths, cache_keys, cache_values, mix_lambda, head_gain)
-    everyone = swap(attended, "z")
+    own_weights = jnp.concatenate((*proj_weights, out_weight.T), 1)
+    weights = to_all(own_weights, ROW).reshape(block, own_weights.shape[1])
+
     core = side.reshape(1)
     depth = lax.axis_index("z").reshape(1)
-    partial_mix = outproj(everyone, weight_out)
-    other_mix = lax.ppermute(partial_mix, "tp", ((0, 1), (1, 0)))
-    sending, stream = build(core, partial_mix, other_mix, line_columns, line_ids, experts)
+    leaving = norm(depth, core, group_ids, member_ids, tokens, norm0_gain, deep)
+    moved = send(leaving)
+    traded = [trade(m) for m in moved[:-1]]
+    arrived = [leaving[0], *moved, *traded[::-1]]
+    partial = project(depth, core, weights, arrived, proj_cols)
+    received = swap(partial, "z")
+    attended = run_attend(
+        received, lengths, cache_keys, cache_values, mix_lambda, head_gain
+    )
+    everyone = swap(attended, "z")
+    partial_mix = outproj(everyone, weights)
+    other_mix = trade(partial_mix)
+    line = in_line(depth, core, arrived)
+    sending, stream = build(core, partial_mix, other_mix, line, experts)
     slots = swap(sending, EP)
-    laid = lay(depth, stream)
-    pieces = [laid[0]]
-    for j in range(1, deep):
-        pairs = [(z, (z + j) % deep) for z in range(deep)]
-        pieces.append(lax.ppermute(laid[j], "z", pairs))
-    residual = settle(depth, core, norm1_gain, pieces)
-
-    slots_other = lax.ppermute(slots, "tp", ((0, 1), (1, 0)))
+    laid = lay(depth, core, stream)
+    moved = send(laid)
+    traded = [trade(m) for m in moved[:-1]]
+    residual = settle(depth, core, norm1_gain, [laid[0], *moved, *traded[::-1]])
+    slots_other = trade(slots)
     down = expert_down[0]
     hidden, given = run_hidden(
         core, slots, slots_other, norm1_gain, expert_gate[0], expert_up[0], down
     )
-    taken = lax.ppermute(given, "tp", ((0, 1), (1, 0)))
+    taken = trade(given)
     leaving = run_down(core, hidden, down, taken)
     returned = swap(leaving, EP)
     mixed, stats = run_combine(expert_ids, share, returned, residual)
-    other_stats = lax.ppermute(stats, "tp", ((0, 1), (1, 0)))
+    other_stats = trade(stats)
     return finish(mixed, stats, other_stats, norm2_gain)
 
 

time: 140 us -> 115 us (0.82)
  blocking collectives: 22.3 us -> 45.4 us
  waiting for transfers between devices: 27 us -> 6.99 us
  starting transfers between devices: 64.7 us -> 49.3 us
  other arithmetic: 7.58 us -> 0.85 us
  local copies, waits for them, and re-layouts: 6.92 us -> 3.3 us
    all_to_all x1 -> x3, blocking collectives: 22.3 us -> 45.4 us  [swap(): return lax.all_to_all(array, axis, 0, 0, tiled=True)]
    all_to_all x5 -> x2, starting transfers between devices: 32.1 us -> 14.1 us  [swap(): return lax.all_to_all(array, axis, 0, 0, tiled=True)]
    all_to_all x5 -> x2, waiting for transfers between devices: 18.7 us -> 1.73 us  [swap(): return lax.all_to_all(array, axis, 0, 0, tiled=True)]
    ppermute x17 -> x18, waiting for transfers between devices: 8.32 us -> 5.25 us  [the longest x10 5.04 us: trade(): return lax.ppermute(array, 'tp', ((0, 1), (1, 0)))]
    unnamed x39 -> x33, local copies, waits for them, and re-layouts: 4.79 us -> 1.75 us
    ppermute x17 -> x18, starting transfers between devices: 32.6 us -> 35.3 us  [the longest x8 20.7 us: send(): moved.append(lax.ppermute(blocks[j], ('z', 'tp'), pairs))]
    reduce_sum x2 -> x0, other arithmetic: 1.77 us -> none  [the longest x1 0.92 us: layer_norm(): spread = jnp.mean(jnp.square(values - mean), -1, keepdims=True)]
    convert_element_type x2 -> x0, other arithmetic: 1.49 us -> none  [the longest x1 0.8 us: layer(): layer_norm(tokens.astype(jnp.float32), norm0_gain).astype(jnp.bfloat16)]
  transfers between devices with their start and end apart: 22 -> 20, of which waited for: 11 -> 10; matrix products, arithmetic and copies ran while one was open for 3% -> 0% of each run, Pallas kernels for 3% -> 1%
where the time goes in v4:
time: 115 us
  starting transfers between devices  49.3 us (43%)
  blocking collectives  45.4 us (39%)
  Pallas kernels  8.77 us (8%)
  waiting for transfers between devices  6.99 us (6%)
  local copies, waits for them, and re-layouts  3.3 us (3%)
    all_to_all x3, blocking collectives, swap(): return lax.all_to_all(array, axis, 0, 0, tiled=True)  45.4 us
    ppermute x8, starting transfers between devices, send(): moved.append(lax.ppermute(blocks[j], ('z', 'tp'), pairs))  20.7 us
    ppermute x10, starting transfers between devices, trade(): return lax.ppermute(array, 'tp', ((0, 1), (1, 0)))  14.6 us
    all_to_all x2, starting transfers between devices, swap(): return lax.all_to_all(array, axis, 0, 0, tiled=True)  14.1 us
    ppermute x10, waiting for transfers between devices, trade(): return lax.ppermute(array, 'tp', ((0, 1), (1, 0)))  5.04 us
    pallas_call x1, Pallas kernels, run_attend(): pl.pallas_call(attend_kernel, out_shape=pltpu.VMEM((deep, seqs, cols), jn...  3.44 us
  transfers between devices with their start and end apart: 20, of which 10 were waited for; matrix products, arithmetic and copies ran while one was open for 0% of the time, Pallas kernels for 1%

profile of v4, /device:TPU:1, one launch (start us, length us, event | category | flops | bytes accessed | tf_op | source)
XLA Modules:
  0.0 114.9 jit_solution(18014299357295394058)
XLA Ops:
  0.0 0.8 pad_maximum_fusion
  0.9 1.1 broadcast_in_dim.2
  2.0 7.7 %all-to-all-start = ((bf16[16,16,2048]{2,1,0:T(8,128)(2,1)}), bf16[16,16,2048]{2,1,0:T(8,128)(2,1)S(1)}, u32[]{:S(2)}, u32[]{:S(2)}) async-start(bf16[16,16,2048]{2,1,0:T(8,128)(2,1)} %broadcast_in_dim.2), calls=%async_computation | async-start | bytes 2097152 | tf_op jit(solution)/shard_map/all_to_all | solution.py:19
  9.9 0.8 norm.1
  10.7 6.5 %collective-permute-start.2 = (bf16[4,512]{1,0:T(4,128)(2,1)S(1)}, bf16[4,512]{1,0:T(4,128)(2,1)S(1)}, u32[]{:S(2)}, u32[]{:S(2)}) collective-permute-start(bf16[4,512]{1,0:T(4,128)(2,1)S(1)} %get-tuple-element.24), channel_id=1, source_target_pairs={{0,96},{1,161},{32,128},{33,193},{64,160},{65,225},{96,192},{97,1}... | collective-permute-start | bytes 12296 | tf_op jit(solution)/shard_map/ppermute | solution.py:39
  17.9 4.5 %collective-permute-start.3 = (bf16[4,512]{1,0:T(4,128)(2,1)S(1)}, bf16[4,512]{1,0:T(4,128)(2,1)S(1)}, u32[]{:S(2)}, u32[]{:S(2)}) collective-permute-start(bf16[4,512]{1,0:T(4,128)(2,1)S(1)} %get-tuple-element.25), channel_id=1, source_target_pairs={{0,128},{1,129},{32,160},{33,161},{64,192},{65,193},{96,224},{97,2... | collective-permute-start | bytes 12296 | tf_op jit(solution)/shard_map/ppermute | solution.py:39
  22.4 0.5 collective-permute-start.5
  22.9 1.8 %collective-permute-start.6 = (bf16[4,512]{1,0:T(4,128)(2,1)S(1)}, bf16[4,512]{1,0:T(4,128)(2,1)S(1)}, u32[]{:S(2)}, u32[]{:S(2)}) collective-permute-start(bf16[4,512]{1,0:T(4,128)(2,1)S(1)} %collective-permute-done.refs_1_), channel_id=1, source_target_pairs={{0,1},{1,0},{2,3},{3,2},{4,5},{5,4},{6,7},{7,6},{8,9},{9,8},{10,11... | collective-permute-start | bytes 12296 | tf_op jit(solution)/shard_map/ppermute | solution.py:27
  24.7 0.8 collective-permute-done.6.refs_7_
  26.0 16.4 %all_to_all.25.parts_ref = f32[8,4,1280]{2,1,0:T(4,128)S(1)} all-to-all(f32[8,4,1280]{2,1,0:T(4,128)S(1)} %project.1), channel_id=1, replica_groups=mesh['z'=8,'y'=4,'x'=4,'tp'=2] {'z'}, dimensions={0} | all-to-all | bytes 327680 | tf_op jit(solution)/shard_map/all_to_all | solution.py:19
  42.4 1.6 %copy-done.2 = bf16[4,1024,256]{2,1,0:T(8,128)(2,1)S(1)} copy-done((bf16[4,1024,256]{2,1,0:T(8,128)(2,1)S(1)}, bf16[4,1024,256]{2,1,0:T(8,128)(2,1)}, u32[]{:S(2)}) %copy-start.2) | copy-done | bytes 2097176
  44.0 3.4 %attend.1 = bf16[8,4,768]{2,1,0:T(4,128)(2,1)S(1)} custom-call(s32[4]{0:T(128)S(1)} %copy-done.11, f32[3]{0:T(128)S(1)} %copy-done.12, f32[8,4,1280]{2,1,0:T(4,128)S(1)} %all_to_all.25.parts_ref, bf16[4,1024,256]{2,1,0:T(8,128)(2,1)S(1)} %copy-done.1, bf16[4,1024,256]{2,1,0:T(8,128)(2,1)S(1)} %copy-done.2, f32[1,256]{1,0:T(1,128)S(1)} %bitcast.21), custom_call_target="tpu_custom_call" | custom-call | tf_op jit(solution)/shard_map/attend/pallas_call | solution.py:481
  47.5 9.6 %all_to_all.26.heads_ref = bf16[8,4,768]{2,1,0:T(4,128)(2,1)S(1)} all-to-all(bf16[8,4,768]{2,1,0:T(4,128)(2,1)S(1)} %attend.1), channel_id=1, replica_groups=mesh['z'=8,'y'=4,'x'=4,'tp'=2] {'z'}, dimensions={0} | all-to-all | bytes 98304 | tf_op jit(solution)/shard_map/all_to_all | solution.py:19
  57.3 5.1 %collective-permute-start.7 = (f32[4,8,256]{2,1,0:T(8,128)S(1)}, f32[4,8,256]{2,1,0:T(8,128)S(1)}, u32[]{:S(2)}, u32[]{:S(2)}) collective-permute-start(f32[4,8,256]{2,1,0:T(8,128)S(1)} %outproj.1.own_ref), channel_id=1, source_target_pairs={{0,1},{1,0},{2,3},{3,2},{4,5},{5,4},{6,7},{7,6},{8,9},{9,8},{10,11... | collective-permute-start | bytes 98312 | tf_op jit(solution)/shard_map/ppermute | solution.py:27
  62.5 0.8 collective-permute-done.7.other_ref
  63.6 19.5 %all_to_all.27.own_ref = bf16[128,8,128]{2,1,0:T(8,128)(2,1)S(1)} all-to-all(bf16[128,8,128]{2,1,0:T(8,128)(2,1)S(1)} %get-tuple-element.26), channel_id=1, replica_groups=mesh['z'=8,'y'=4,'x'=4,'tp'=2] {'z','y','x'}, dimensions={0} | all-to-all | bytes 524288 | tf_op jit(solution)/shard_map/all_to_all | solution.py:19
  83.1 2.1 %collective-permute-start.8 = (bf16[128,8,128]{2,1,0:T(8,128)(2,1)S(1)}, bf16[128,8,128]{2,1,0:T(8,128)(2,1)S(1)}, u32[]{:S(2)}, u32[]{:S(2)}) collective-permute-start(bf16[128,8,128]{2,1,0:T(8,128)(2,1)S(1)} %all_to_all.27.own_ref), channel_id=1, source_target_pairs={{0,1},{1,0},{2,3},{3,2},{4,5},{5,4},{6,7},{7,6},{8,9},{9,8},{10,11... | collective-permute-start | bytes 786440 | tf_op jit(solution)/shard_map/ppermute | solution.py:27
  85.2 1.2 %collective-permute-done.8.other_ref = bf16[128,8,128]{2,1,0:T(8,128)(2,1)S(1)} collective-permute-done((bf16[128,8,128]{2,1,0:T(8,128)(2,1)S(1)}, bf16[128,8,128]{2,1,0:T(8,128)(2,1)S(1)}, u32[]{:S(2)}, u32[]{:S(2)}) %collective-permute-start.8) | collective-permute-done | bytes 262176 | tf_op jit(solution)/shard_map/ppermute | solution.py:27
  86.4 1.2 %hidden.1 = (bf16[128,256]{1,0:T(8,128)(2,1)S(1)}, bf16[128,8,128]{2,1,0:T(8,128)(2,1)S(1)}) custom-call(s32[1]{0:T(128)} %bitcast.side_ref, bf16[128,8,128]{2,1,0:T(8,128)(2,1)S(1)} %all_to_all.27.own_ref, bf16[128,8,128]{2,1,0:T(8,128)(2,1)S(1)} %collective-permute-done.8.other_ref, f32[1,2048]{1,0:T(1,128)S(1)} %bitcast.17, ...), custom_call_target="tpu_custom_call" | custom-call | tf_op jit(solution)/shard_map/hidden/pallas_call | solution.py:368
  88.1 1.2 %collective-permute-done.9.taken_ref = bf16[128,8,128]{2,1,0:T(8,128)(2,1)S(1)} collective-permute-done((bf16[128,8,128]{2,1,0:T(8,128)(2,1)S(1)}, bf16[128,8,128]{2,1,0:T(8,128)(2,1)S(1)}, u32[]{:S(2)}, u32[]{:S(2)}) %collective-permute-start.9) | collective-permute-done | bytes 262176 | tf_op jit(solution)/shard_map/ppermute | solution.py:27
  89.3 1.0 down.1
  90.3 6.3 %all-to-all-start.4 = ((bf16[128,8,128]{2,1,0:T(8,128)(2,1)}), bf16[128,8,128]{2,1,0:T(8,128)(2,1)S(1)}, u32[]{:S(2)}, u32[]{:S(2)}) async-start(bf16[128,8,128]{2,1,0:T(8,128)(2,1)} %down.1), calls=%async_computation.4 | async-start | bytes 524288 | tf_op jit(solution)/shard_map/all_to_all | solution.py:19
  96.7 2.5 %collective-permute-start.10 = (bf16[4,256]{1,0:T(4,128)(2,1)S(1)}, bf16[4,256]{1,0:T(4,128)(2,1)S(1)}, u32[]{:S(2)}, u32[]{:S(2)}) collective-permute-start(bf16[4,256]{1,0:T(4,128)(2,1)S(1)} %get-tuple-element.31), channel_id=1, source_target_pairs={{0,32},{1,225},{32,64},{33,1},{64,96},{65,33},{96,128},{97,65},{12... | collective-permute-start | bytes 6152 | tf_op jit(solution)/shard_map/ppermute | solution.py:39
  99.2 1.9 %collective-permute-start.11 = (bf16[4,256]{1,0:T(4,128)(2,1)S(1)}, bf16[4,256]{1,0:T(4,128)(2,1)S(1)}, u32[]{:S(2)}, u32[]{:S(2)}) collective-permute-start(bf16[4,256]{1,0:T(4,128)(2,1)S(1)} %get-tuple-element.32), channel_id=1, source_target_pairs={{0,64},{1,193},{32,96},{33,225},{64,128},{65,1},{96,160},{97,33},{... | collective-permute-start | bytes 6152 | tf_op jit(solution)/shard_map/ppermute | solution.py:39
  101.0 0.9 collective-permute-start.12
  101.9 3.7 %collective-permute-start.13 = (bf16[4,256]{1,0:T(4,128)(2,1)S(1)}, bf16[4,256]{1,0:T(4,128)(2,1)S(1)}, u32[]{:S(2)}, u32[]{:S(2)}) collective-permute-start(bf16[4,256]{1,0:T(4,128)(2,1)S(1)} %get-tuple-element.34), channel_id=1, source_target_pairs={{0,128},{1,129},{32,160},{33,161},{64,192},{65,193},{96,224},{97,2... | collective-permute-start | bytes 6152 | tf_op jit(solution)/shard_map/ppermute | solution.py:39
  105.6 1.8 %collective-permute-start.14 = (bf16[4,256]{1,0:T(4,128)(2,1)S(1)}, bf16[4,256]{1,0:T(4,128)(2,1)S(1)}, u32[]{:S(2)}, u32[]{:S(2)}) collective-permute-start(bf16[4,256]{1,0:T(4,128)(2,1)S(1)} %collective-permute-done.12.refs_3_), channel_id=1, source_target_pairs={{0,1},{1,0},{2,3},{3,2},{4,5},{5,4},{6,7},{7,6},{8,9},{9,8},{10,11... | collective-permute-start | bytes 6152 | tf_op jit(solution)/shard_map/ppermute | solution.py:27
  109.0 1.5 %all-to-all-done.4.returned_ref = bf16[128,8,128]{2,1,0:T(8,128)(2,1)S(1)} async-done(((bf16[128,8,128]{2,1,0:T(8,128)(2,1)}), bf16[128,8,128]{2,1,0:T(8,128)(2,1)S(1)}, u32[]{:S(2)}, u32[]{:S(2)}) %all-to-all-start.4) | async-done | bytes 262176 | tf_op jit(solution)/shard_map/all_to_all | solution.py:19
  110.6 0.6 combine.1
  111.2 2.2 %collective-permute-start.17 = (f32[8,128]{1,0:T(8,128)S(1)}, f32[8,128]{1,0:T(8,128)S(1)}, u32[]{:S(2)}, u32[]{:S(2)}) collective-permute-start(f32[8,128]{1,0:T(8,128)S(1)} %get-tuple-element.36.own_ref), channel_id=1, source_target_pairs={{0,1},{1,0},{2,3},{3,2},{4,5},{5,4},{6,7},{7,6},{8,9},{9,8},{10,11... | collective-permute-start | bytes 12296 | tf_op jit(solution)/shard_map/ppermute | solution.py:27
  113.4 0.8 collective-permute-done.17.other_ref
  114.3 0.6 finish.1
  (66 shorter events, 4.1 us)
Async XLA Ops:
  0.0 9.9 %copy-start.6 = (bf16[4,2048]{1,0:T(4,128)(2,1)S(1)}, bf16[4,2048]{1,0:T(4,128)(2,1)}, u32[]{:S(2)}) copy-start(bf16[4,2048]{1,0:T(4,128)(2,1)} %tokens_ref.1) | copy-start | bytes 49156
  2.0 40.4 %copy-start.1 = (bf16[4,1024,256]{2,1,0:T(8,128)(2,1)S(1)}, bf16[4,1024,256]{2,1,0:T(8,128)(2,1)}, u32[]{:S(2)}) copy-start(bf16[4,1024,256]{2,1,0:T(8,128)(2,1)} %far_keys_ref.1) | copy-start | bytes 6291460
  2.0 40.4 %copy-start.9 = (f32[256]{0:T(256)S(1)}, f32[256]{0:T(256)}, u32[]{:S(2)}) copy-start(f32[256]{0:T(256)} %param.29) | copy-start | bytes 3076
  2.0 40.4 %copy-start.11 = (s32[4]{0:T(128)S(1)}, s32[4]{0:T(128)}, u32[]{:S(2)}) copy-start(s32[4]{0:T(128)} %lengths_ref.1) | copy-start | bytes 52
  2.0 40.4 %copy-start.12 = (f32[3]{0:T(128)S(1)}, f32[3]{0:T(128)}, u32[]{:S(2)}) copy-start(f32[3]{0:T(128)} %lambda_ref.1) | copy-start | bytes 40
  2.0 23.8 %all-to-all-start = ((bf16[16,16,2048]{2,1,0:T(8,128)(2,1)}), bf16[16,16,2048]{2,1,0:T(8,128)(2,1)S(1)}, u32[]{:S(2)}, u32[]{:S(2)}) async-start(bf16[16,16,2048]{2,1,0:T(8,128)(2,1)} %broadcast_in_dim.2), calls=%async_computation | async-start | bytes 2097152 | tf_op jit(solution)/shard_map/all_to_all | solution.py:19
  10.7 11.8 %collective-permute-start.2 = (bf16[4,512]{1,0:T(4,128)(2,1)S(1)}, bf16[4,512]{1,0:T(4,128)(2,1)S(1)}, u32[]{:S(2)}, u32[]{:S(2)}) collective-permute-start(bf16[4,512]{1,0:T(4,128)(2,1)S(1)} %get-tuple-element.24), channel_id=1, source_target_pairs={{0,96},{1,161},{32,128},{33,193},{64,160},{65,225},{96,192},{97,1}... | collective-permute-start | bytes 12296 | tf_op jit(solution)/shard_map/ppermute | solution.py:39
  17.2 5.2 %collective-permute-start.1 = (bf16[4,512]{1,0:T(4,128)(2,1)S(1)}, bf16[4,512]{1,0:T(4,128)(2,1)S(1)}, u32[]{:S(2)}, u32[]{:S(2)}) collective-permute-start(bf16[4,512]{1,0:T(4,128)(2,1)S(1)} %get-tuple-element.23), channel_id=1, source_target_pairs={{0,64},{1,193},{32,96},{33,225},{64,128},{65,1},{96,160},{97,33},{... | collective-permute-start | bytes 12296 | tf_op jit(solution)/shard_map/ppermute | solution.py:39
  17.5 5.5 %collective-permute-start = (bf16[4,512]{1,0:T(4,128)(2,1)S(1)}, bf16[4,512]{1,0:T(4,128)(2,1)S(1)}, u32[]{:S(2)}, u32[]{:S(2)}) collective-permute-start(bf16[4,512]{1,0:T(4,128)(2,1)S(1)} %get-tuple-element.22), channel_id=1, source_target_pairs={{0,32},{1,225},{32,64},{33,1},{64,96},{65,33},{96,128},{97,65},{12... | collective-permute-start | bytes 12296 | tf_op jit(solution)/shard_map/ppermute | solution.py:39
  17.9 6.8 %collective-permute-start.3 = (bf16[4,512]{1,0:T(4,128)(2,1)S(1)}, bf16[4,512]{1,0:T(4,128)(2,1)S(1)}, u32[]{:S(2)}, u32[]{:S(2)}) collective-permute-start(bf16[4,512]{1,0:T(4,128)(2,1)S(1)} %get-tuple-element.25), channel_id=1, source_target_pairs={{0,128},{1,129},{32,160},{33,161},{64,192},{65,193},{96,224},{97,2... | collective-permute-start | bytes 12296 | tf_op jit(solution)/shard_map/ppermute | solution.py:39
  22.4 2.3 %collective-permute-start.4 = (bf16[4,512]{1,0:T(4,128)(2,1)S(1)}, bf16[4,512]{1,0:T(4,128)(2,1)S(1)}, u32[]{:S(2)}, u32[]{:S(2)}) collective-permute-start(bf16[4,512]{1,0:T(4,128)(2,1)S(1)} %collective-permute-done.2.refs_3_), channel_id=1, source_target_pairs={{0,1},{1,0},{2,3},{3,2},{4,5},{5,4},{6,7},{7,6},{8,9},{9,8},{10,11... | collective-permute-start | bytes 12296 | tf_op jit(solution)/shard_map/ppermute | solution.py:27
  22.4 2.3 %collective-permute-start.5 = (bf16[4,512]{1,0:T(4,128)(2,1)S(1)}, bf16[4,512]{1,0:T(4,128)(2,1)S(1)}, u32[]{:S(2)}, u32[]{:S(2)}) collective-permute-start(bf16[4,512]{1,0:T(4,128)(2,1)S(1)} %collective-permute-done.1.refs_2_), channel_id=1, source_target_pairs={{0,1},{1,0},{2,3},{3,2},{4,5},{5,4},{6,7},{7,6},{8,9},{9,8},{10,11... | collective-permute-start | bytes 12296 | tf_op jit(solution)/shard_map/ppermute | solution.py:27
  22.9 2.6 %collective-permute-start.6 = (bf16[4,512]{1,0:T(4,128)(2,1)S(1)}, bf16[4,512]{1,0:T(4,128)(2,1)S(1)}, u32[]{:S(2)}, u32[]{:S(2)}) collective-permute-start(bf16[4,512]{1,0:T(4,128)(2,1)S(1)} %collective-permute-done.refs_1_), channel_id=1, source_target_pairs={{0,1},{1,0},{2,3},{3,2},{4,5},{5,4},{6,7},{7,6},{8,9},{9,8},{10,11... | collective-permute-start | bytes 12296 | tf_op jit(solution)/shard_map/ppermute | solution.py:27
  44.0 42.4 %copy-start.3 = (bf16[1,2048,256]{2,1,0:T(8,128)(2,1)S(1)}, bf16[1,2048,256]{2,1,0:T(8,128)(2,1)}, u32[]{:S(2)}) copy-start(bf16[1,2048,256]{2,1,0:T(8,128)(2,1)} %param.36) | copy-start | bytes 3145732
  44.0 42.4 %copy-start.4 = (bf16[1,2048,256]{2,1,0:T(8,128)(2,1)S(1)}, bf16[1,2048,256]{2,1,0:T(8,128)(2,1)}, u32[]{:S(2)}) copy-start(bf16[1,2048,256]{2,1,0:T(8,128)(2,1)} %param.37) | copy-start | bytes 3145732
  44.0 42.4 %copy-start.5 = (f32[2048]{0:T(1024)S(1)}, f32[2048]{0:T(1024)}, u32[]{:S(2)}) copy-start(f32[2048]{0:T(1024)} %param.31) | copy-start | bytes 24580
  47.4 38.9 %copy-start = (bf16[1,256,2048]{2,1,0:T(8,128)(2,1)S(1)}, bf16[1,256,2048]{2,1,0:T(8,128)(2,1)}, u32[]{:S(2)}) copy-start(bf16[1,256,2048]{2,1,0:T(8,128)(2,1)} %param.38) | copy-start | bytes 3145732
  57.3 6.0 %collective-permute-start.7 = (f32[4,8,256]{2,1,0:T(8,128)S(1)}, f32[4,8,256]{2,1,0:T(8,128)S(1)}, u32[]{:S(2)}, u32[]{:S(2)}) collective-permute-start(f32[4,8,256]{2,1,0:T(8,128)S(1)} %outproj.1.own_ref), channel_id=1, source_target_pairs={{0,1},{1,0},{2,3},{3,2},{4,5},{5,4},{6,7},{7,6},{8,9},{9,8},{10,11... | collective-permute-start | bytes 98312 | tf_op jit(solution)/shard_map/ppermute | solution.py:27
  83.1 3.3 %collective-permute-start.8 = (bf16[128,8,128]{2,1,0:T(8,128)(2,1)S(1)}, bf16[128,8,128]{2,1,0:T(8,128)(2,1)S(1)}, u32[]{:S(2)}, u32[]{:S(2)}) collective-permute-start(bf16[128,8,128]{2,1,0:T(8,128)(2,1)S(1)} %all_to_all.27.own_ref), channel_id=1, source_target_pairs={{0,1},{1,0},{2,3},{3,2},{4,5},{5,4},{6,7},{7,6},{8,9},{9,8},{10,11... | collective-permute-start | bytes 786440 | tf_op jit(solution)/shard_map/ppermute | solution.py:27
  86.4 21.6 %copy-start.14 = (f32[4,2]{0,1:T(2,128)S(1)}, f32[4,2]{0,1:T(2,128)}, u32[]{:S(2)}) copy-start(f32[4,2]{0,1:T(2,128)} %param.35) | copy-start | bytes 100
  86.4 21.6 %copy-start.15 = (f32[4]{0:T(128)S(1)}, f32[4]{0:T(128)}, u32[]{:S(2)}) copy-start(f32[4]{0:T(128)} %param.34) | copy-start | bytes 52
  87.6 26.7 %copy-start.8 = (f32[1024]{0:T(1024)S(1)}, f32[1024]{0:T(1024)}, u32[]{:S(2)}) copy-start(f32[1024]{0:T(1024)} %param.39) | copy-start | bytes 12292
  87.6 1.6 %collective-permute-start.9 = (bf16[128,8,128]{2,1,0:T(8,128)(2,1)S(1)}, bf16[128,8,128]{2,1,0:T(8,128)(2,1)S(1)}, u32[]{:S(2)}, u32[]{:S(2)}) collective-permute-start(bf16[128,8,128]{2,1,0:T(8,128)(2,1)S(1)} %get-tuple-element.28), channel_id=1, source_target_pairs={{0,1},{1,0},{2,3},{3,2},{4,5},{5,4},{6,7},{7,6},{8,9},{9,8},{10,11... | collective-permute-start | bytes 786440 | tf_op jit(solution)/shard_map/ppermute | solution.py:27
  90.3 20.3 %all-to-all-start.4 = ((bf16[128,8,128]{2,1,0:T(8,128)(2,1)}), bf16[128,8,128]{2,1,0:T(8,128)(2,1)S(1)}, u32[]{:S(2)}, u32[]{:S(2)}) async-start(bf16[128,8,128]{2,1,0:T(8,128)(2,1)} %down.1), calls=%async_computation.4 | async-start | bytes 524288 | tf_op jit(solution)/shard_map/all_to_all | solution.py:19
  96.7 10.8 %collective-permute-start.10 = (bf16[4,256]{1,0:T(4,128)(2,1)S(1)}, bf16[4,256]{1,0:T(4,128)(2,1)S(1)}, u32[]{:S(2)}, u32[]{:S(2)}) collective-permute-start(bf16[4,256]{1,0:T(4,128)(2,1)S(1)} %get-tuple-element.31), channel_id=1, source_target_pairs={{0,32},{1,225},{32,64},{33,1},{64,96},{65,33},{96,128},{97,65},{12... | collective-permute-start | bytes 6152 | tf_op jit(solution)/shard_map/ppermute | solution.py:39
  99.2 8.3 %collective-permute-start.11 = (bf16[4,256]{1,0:T(4,128)(2,1)S(1)}, bf16[4,256]{1,0:T(4,128)(2,1)S(1)}, u32[]{:S(2)}, u32[]{:S(2)}) collective-permute-start(bf16[4,256]{1,0:T(4,128)(2,1)S(1)} %get-tuple-element.32), channel_id=1, source_target_pairs={{0,64},{1,193},{32,96},{33,225},{64,128},{65,1},{96,160},{97,33},{... | collective-permute-start | bytes 6152 | tf_op jit(solution)/shard_map/ppermute | solution.py:39
  101.0 4.6 %collective-permute-start.12 = (bf16[4,256]{1,0:T(4,128)(2,1)S(1)}, bf16[4,256]{1,0:T(4,128)(2,1)S(1)}, u32[]{:S(2)}, u32[]{:S(2)}) collective-permute-start(bf16[4,256]{1,0:T(4,128)(2,1)S(1)} %get-tuple-element.33), channel_id=1, source_target_pairs={{0,96},{1,161},{32,128},{33,193},{64,160},{65,225},{96,192},{97,1}... | collective-permute-start | bytes 6152 | tf_op jit(solution)/shard_map/ppermute | solution.py:39
  101.9 6.6 %collective-permute-start.13 = (bf16[4,256]{1,0:T(4,128)(2,1)S(1)}, bf16[4,256]{1,0:T(4,128)(2,1)S(1)}, u32[]{:S(2)}, u32[]{:S(2)}) collective-permute-start(bf16[4,256]{1,0:T(4,128)(2,1)S(1)} %get-tuple-element.34), channel_id=1, source_target_pairs={{0,128},{1,129},{32,160},{33,161},{64,192},{65,193},{96,224},{97,2... | collective-permute-start | bytes 6152 | tf_op jit(solution)/shard_map/ppermute | solution.py:39
  105.6 2.9 %collective-permute-start.14 = (bf16[4,256]{1,0:T(4,128)(2,1)S(1)}, bf16[4,256]{1,0:T(4,128)(2,1)S(1)}, u32[]{:S(2)}, u32[]{:S(2)}) collective-permute-start(bf16[4,256]{1,0:T(4,128)(2,1)S(1)} %collective-permute-done.12.refs_3_), channel_id=1, source_target_pairs={{0,1},{1,0},{2,3},{3,2},{4,5},{5,4},{6,7},{7,6},{8,9},{9,8},{10,11... | collective-permute-start | bytes 6152 | tf_op jit(solution)/shard_map/ppermute | solution.py:27
  107.5 1.2 %collective-permute-start.15 = (bf16[4,256]{1,0:T(4,128)(2,1)S(1)}, bf16[4,256]{1,0:T(4,128)(2,1)S(1)}, u32[]{:S(2)}, u32[]{:S(2)}) collective-permute-start(bf16[4,256]{1,0:T(4,128)(2,1)S(1)} %collective-permute-done.11.refs_2_), channel_id=1, source_target_pairs={{0,1},{1,0},{2,3},{3,2},{4,5},{5,4},{6,7},{7,6},{8,9},{9,8},{10,11... | collective-permute-start | bytes 6152 | tf_op jit(solution)/shard_map/ppermute | solution.py:27
  107.5 1.3 %collective-permute-start.16 = (bf16[4,256]{1,0:T(4,128)(2,1)S(1)}, bf16[4,256]{1,0:T(4,128)(2,1)S(1)}, u32[]{:S(2)}, u32[]{:S(2)}) collective-permute-start(bf16[4,256]{1,0:T(4,128)(2,1)S(1)} %collective-permute-done.10.refs_1_), channel_id=1, source_target_pairs={{0,1},{1,0},{2,3},{3,2},{4,5},{5,4},{6,7},{7,6},{8,9},{9,8},{10,11... | collective-permute-start | bytes 6152 | tf_op jit(solution)/shard_map/ppermute | solution.py:27
  111.2 3.1 %collective-permute-start.17 = (f32[8,128]{1,0:T(8,128)S(1)}, f32[8,128]{1,0:T(8,128)S(1)}, u32[]{:S(2)}, u32[]{:S(2)}) collective-permute-start(f32[8,128]{1,0:T(8,128)S(1)} %get-tuple-element.36.own_ref), channel_id=1, source_target_pairs={{0,1},{1,0},{2,3},{3,2},{4,5},{5,4},{6,7},{7,6},{8,9},{9,8},{10,11... | collective-permute-start | bytes 12296 | tf_op jit(solution)/shard_map/ppermute | solution.py:27
  (4 other events, 31.1 us)

commit v5 on v4

--- a/solution.py
+++ b/solution.py
@@ -42,6 +42,10 @@
 
 def fast(array):
     return pltpu.with_memory_space_constraint(array, pltpu.VMEM)
+
+
+def far(array):
+    return pltpu.with_memory_space_constraint(array, pltpu.HBM)
 
 
 VM = pl.BlockSpec(memory_space=pltpu.VMEM)
@@ -302,6 +306,29 @@
         compiler_params=SMALL,
         name="finish",
     )(fast(mixed), fast(own), fast(other), gain.reshape(1, -1))
+
+
+def load_kernel(*refs):
+    half = len(refs) // 2
+    done = refs[-1]
+    copies = []
+    for k in range(half):
+        copies.append(pltpu.make_async_copy(refs[k], refs[half + k], done.at[k]))
+        copies[k].start()
+    for copy in copies:
+        copy.wait()
+
+
+def load(*arrays):
+    return pl.pallas_call(
+        load_kernel,
+        out_shape=tuple(pltpu.VMEM(a.shape, a.dtype) for a in arrays),
+        in_specs=[FAR] * len(arrays),
+        out_specs=(VM,) * len(arrays),
+        scratch_shapes=[pltpu.SemaphoreType.DMA((len(arrays),))],
+        compiler_params=SMALL,
+        name="load",
+    )(*(far(a) for a in arrays))
 
 
 def hidden_kernel(
@@ -394,20 +421,17 @@
     lengths_ref,
     lambda_ref,
     parts_ref,
-    far_keys_ref,
-    far_values_ref,
+    keys_ref,
+    far_ref,
     gain_ref,
     out_ref,
-    keys_ref,
     values_ref,
     done,
 ):
     loads = []
-    for k, (far, near) in enumerate(((far_keys_ref, keys_ref), (far_values_ref, values_ref))):
-        loads.append([])
-        for s in range(near.shape[0]):
-            loads[k].append(pltpu.make_async_copy(far.at[s], near.at[s], done.at[k, s]))
-            loads[k][s].start()
+    for s in range(far_ref.shape[0]):
+        loads.append(pltpu.make_async_copy(far_ref.at[s], values_ref.at[s], done.at[s]))
+        loads[s].start()
     deep, seqs, _ = parts_ref.shape
     _, width = keys_ref.shape[1:]
     hwidth = width // 2
@@ -430,7 +454,6 @@
         grid = jnp.concatenate(ones + twos, 0)
         new_key = total[s : s + 1, at : at + width]
         fresh.append(jnp.sum(grid * new_key, 1, keepdims=True))
-        loads[0][s].wait()
         scores.append(
             lax.dot_general(
                 grid.astype(jnp.bfloat16),
@@ -464,7 +487,7 @@
         weight = maps[one:two] - lam * maps[two : two + pad]
         fresh_weight = itself[one:two] - lam * itself[two : two + pad]
         weight = jnp.concatenate((weight, jnp.zeros_like(weight)), 0).astype(jnp.bfloat16)
-        loads[1][s].wait()
+        loads[s].wait()
         out = jnp.dot(weight, values_ref[s], preferred_element_type=f32)[:pad]
         new_value = total[s : s + 1, at + width : at + 2 * width]
         out = out + fresh_weight.astype(jnp.bfloat16).astype(f32) * new_value
@@ -481,16 +504,15 @@
     return pl.pallas_call(
         attend_kernel,
         out_shape=pltpu.VMEM((deep, seqs, cols), jnp.bfloat16),
-        in_specs=[SM, SM, VM, FAR, FAR, VM],
+        in_specs=[SM, SM, VM, VM, FAR, VM],
         out_specs=VM,
         scratch_shapes=[
-            pltpu.VMEM(keys.shape, keys.dtype),
             pltpu.VMEM(values.shape, values.dtype),
-            pltpu.SemaphoreType.DMA((2, seqs)),
+            pltpu.SemaphoreType.DMA((seqs,)),
         ],
         compiler_params=SMALL,
         name="attend",
-    )(lengths, mix_lambda, fast(parts), keys, values, head_gain.reshape(1, -1))
+    )(lengths, mix_lambda, fast(parts), fast(keys), far(values), head_gain.reshape(1, -1))
 
 
 def shards(
@@ -591,10 +613,9 @@
     traded = [trade(m) for m in moved[:-1]]
     residual = settle(depth, core, norm1_gain, [laid[0], *moved, *traded[::-1]])
     slots_other = trade(slots)
+    (upward,) = load(expert_up[0])
     down = expert_down[0]
-    hidden, given = run_hidden(
-        core, slots, slots_other, norm1_gain, expert_gate[0], expert_up[0], down
-    )
+    hidden, given = run_hidden(core, slots, slots_other, norm1_gain, expert_gate[0], upward, down)
     taken = trade(given)
     leaving = run_down(core, hidden, down, taken)
     returned = swap(leaving, EP)

time: 115 us -> 113 us (0.983)
  local copies, waits for them, and re-layouts: 3.3 us -> 1.7 us
    unnamed x33 -> x29, local copies, waits for them, and re-layouts: 1.75 us -> 0.16 us
    pallas_call x0 -> x1, Pallas kernels: none -> 1.23 us  [load(): pl.pallas_call(load_kernel, out_shape=tuple((pltpu.VMEM(a.shape, a.dtype)...]
    ppermute x10, waiting for transfers between devices: 5.04 us -> 3.86 us  [trade(): return lax.ppermute(array, 'tp', ((0, 1), (1, 0)))]
  transfers between devices with their start and end apart: 20 -> 20, of which waited for: 10 -> 8; matrix products, arithmetic and copies ran while one was open for 0% -> 0% of each run, Pallas kernels for 1% -> 2%
where the time goes in v5:
time: 113 us
  starting transfers between devices  49 us (43%)
  blocking collectives  45.4 us (40%)
  Pallas kernels  9.44 us (8%)
  waiting for transfers between devices  6.2 us (5%)
  local copies, waits for them, and re-layouts  1.7 us (2%)
    all_to_all x3, blocking collectives, swap(): return lax.all_to_all(array, axis, 0, 0, tiled=True)  45.4 us
    ppermute x8, starting transfers between devices, send(): moved.append(lax.ppermute(blocks[j], ('z', 'tp'), pairs))  20.7 us
    ppermute x10, starting transfers between devices, trade(): return lax.ppermute(array, 'tp', ((0, 1), (1, 0)))  14.2 us
    all_to_all x2, starting transfers between devices, swap(): return lax.all_to_all(array, axis, 0, 0, tiled=True)  14.1 us
    ppermute x10, waiting for transfers between devices, trade(): return lax.ppermute(array, 'tp', ((0, 1), (1, 0)))  3.86 us
    pallas_call x1, Pallas kernels, run_attend(): pl.pallas_call(attend_kernel, out_shape=pltpu.VMEM((deep, seqs, cols), jn...  2.87 us
  transfers between devices with their start and end apart: 20, of which 8 were waited for; matrix products, arithmetic and copies ran while one was open for 0% of the time, Pallas kernels for 2%

profile of v5, /device:TPU:1, one launch (start us, length us, event | category | flops | bytes accessed | tf_op | source)
XLA Modules:
  0.0 112.8 jit_solution(15873314890582604579)
XLA Ops:
  0.0 0.8 pad_maximum_fusion
  0.9 1.1 broadcast_in_dim.2
  2.0 7.7 %all-to-all-start = ((bf16[16,16,2048]{2,1,0:T(8,128)(2,1)}), bf16[16,16,2048]{2,1,0:T(8,128)(2,1)S(1)}, u32[]{:S(2)}, u32[]{:S(2)}) async-start(bf16[16,16,2048]{2,1,0:T(8,128)(2,1)} %broadcast_in_dim.2), calls=%async_computation | async-start | bytes 2097152 | tf_op jit(solution)/shard_map/all_to_all | solution.py:19
  9.9 0.8 norm.1
  10.6 6.5 %collective-permute-start.2 = (bf16[4,512]{1,0:T(4,128)(2,1)S(1)}, bf16[4,512]{1,0:T(4,128)(2,1)S(1)}, u32[]{:S(2)}, u32[]{:S(2)}) collective-permute-start(bf16[4,512]{1,0:T(4,128)(2,1)S(1)} %get-tuple-element.24), channel_id=1, source_target_pairs={{0,96},{1,161},{32,128},{33,193},{64,160},{65,225},{96,192},{97,1}... | collective-permute-start | bytes 12296 | tf_op jit(solution)/shard_map/ppermute | solution.py:39
  17.9 4.5 %collective-permute-start.3 = (bf16[4,512]{1,0:T(4,128)(2,1)S(1)}, bf16[4,512]{1,0:T(4,128)(2,1)S(1)}, u32[]{:S(2)}, u32[]{:S(2)}) collective-permute-start(bf16[4,512]{1,0:T(4,128)(2,1)S(1)} %get-tuple-element.25), channel_id=1, source_target_pairs={{0,128},{1,129},{32,160},{33,161},{64,192},{65,193},{96,224},{97,2... | collective-permute-start | bytes 12296 | tf_op jit(solution)/shard_map/ppermute | solution.py:39
  22.4 0.5 collective-permute-start.5
  22.9 1.8 %collective-permute-start.6 = (bf16[4,512]{1,0:T(4,128)(2,1)S(1)}, bf16[4,512]{1,0:T(4,128)(2,1)S(1)}, u32[]{:S(2)}, u32[]{:S(2)}) collective-permute-start(bf16[4,512]{1,0:T(4,128)(2,1)S(1)} %collective-permute-done.refs_1_), channel_id=1, source_target_pairs={{0,1},{1,0},{2,3},{3,2},{4,5},{5,4},{6,7},{7,6},{8,9},{9,8},{10,11... | collective-permute-start | bytes 12296 | tf_op jit(solution)/shard_map/ppermute | solution.py:27
  24.7 0.8 collective-permute-done.6.refs_7_
  26.0 16.4 %all_to_all.25.parts_ref = f32[8,4,1280]{2,1,0:T(4,128)S(1)} all-to-all(f32[8,4,1280]{2,1,0:T(4,128)S(1)} %project.1), channel_id=1, replica_groups=mesh['z'=8,'y'=4,'x'=4,'tp'=2] {'z'}, dimensions={0} | all-to-all | bytes 327680 | tf_op jit(solution)/shard_map/all_to_all | solution.py:19
  42.4 2.9 %attend.1 = bf16[8,4,768]{2,1,0:T(4,128)(2,1)S(1)} custom-call(s32[4]{0:T(128)S(1)} %copy-done.9, f32[3]{0:T(128)S(1)} %copy-done.10, f32[8,4,1280]{2,1,0:T(4,128)S(1)} %all_to_all.25.parts_ref, bf16[4,1024,256]{2,1,0:T(8,128)(2,1)S(1)} %copy-done.1, bf16[4,1024,256]{2,1,0:T(8,128)(2,1)} %far_ref.1, f32[1,256]{1,0:T(1,128)S(1)} %bitcast.20), custom_call_target="tpu_custom_call" | custom-call | tf_op jit(solution)/shard_map/attend/pallas_call | solution.py:504
  45.3 9.6 %all_to_all.26.heads_ref = bf16[8,4,768]{2,1,0:T(4,128)(2,1)S(1)} all-to-all(bf16[8,4,768]{2,1,0:T(4,128)(2,1)S(1)} %attend.1), channel_id=1, replica_groups=mesh['z'=8,'y'=4,'x'=4,'tp'=2] {'z'}, dimensions={0} | all-to-all | bytes 98304 | tf_op jit(solution)/shard_map/all_to_all | solution.py:19
  55.1 5.1 %collective-permute-start.7 = (f32[4,8,256]{2,1,0:T(8,128)S(1)}, f32[4,8,256]{2,1,0:T(8,128)S(1)}, u32[]{:S(2)}, u32[]{:S(2)}) collective-permute-start(f32[4,8,256]{2,1,0:T(8,128)S(1)} %outproj.1.own_ref), channel_id=1, source_target_pairs={{0,1},{1,0},{2,3},{3,2},{4,5},{5,4},{6,7},{7,6},{8,9},{9,8},{10,11... | collective-permute-start | bytes 98312 | tf_op jit(solution)/shard_map/ppermute | solution.py:27
  60.3 0.8 collective-permute-done.7.other_ref
  61.4 19.5 %all_to_all.27.own_ref = bf16[128,8,128]{2,1,0:T(8,128)(2,1)S(1)} all-to-all(bf16[128,8,128]{2,1,0:T(8,128)(2,1)S(1)} %get-tuple-element.26), channel_id=1, replica_groups=mesh['z'=8,'y'=4,'x'=4,'tp'=2] {'z','y','x'}, dimensions={0} | all-to-all | bytes 524288 | tf_op jit(solution)/shard_map/all_to_all | solution.py:19
  80.9 2.1 %collective-permute-start.8 = (bf16[128,8,128]{2,1,0:T(8,128)(2,1)S(1)}, bf16[128,8,128]{2,1,0:T(8,128)(2,1)S(1)}, u32[]{:S(2)}, u32[]{:S(2)}) collective-permute-start(bf16[128,8,128]{2,1,0:T(8,128)(2,1)S(1)} %all_to_all.27.own_ref), channel_id=1, source_target_pairs={{0,1},{1,0},{2,3},{3,2},{4,5},{5,4},{6,7},{7,6},{8,9},{9,8},{10,11... | collective-permute-start | bytes 786440 | tf_op jit(solution)/shard_map/ppermute | solution.py:27
  83.0 1.2 %load.1.up_ref = bf16[2048,256]{1,0:T(8,128)(2,1)S(1)} custom-call(bf16[2048,256]{1,0:T(8,128)(2,1)} %bitcast.21), custom_call_target="tpu_custom_call" | custom-call | tf_op jit(solution)/shard_map/load/pallas_call | solution.py:323
  84.3 1.2 %hidden.1 = (bf16[128,256]{1,0:T(8,128)(2,1)S(1)}, bf16[128,8,128]{2,1,0:T(8,128)(2,1)S(1)}) custom-call(s32[1]{0:T(128)} %bitcast.side_ref, bf16[128,8,128]{2,1,0:T(8,128)(2,1)S(1)} %all_to_all.27.own_ref, bf16[128,8,128]{2,1,0:T(8,128)(2,1)S(1)} %collective-permute-done.8.other_ref, f32[1,2048]{1,0:T(1,128)S(1)} %bitcast.16, ...), custom_call_target="tpu_custom_call" | custom-call | tf_op jit(solution)/shard_map/hidden/pallas_call | solution.py:395
  85.9 1.3 %collective-permute-done.9.taken_ref = bf16[128,8,128]{2,1,0:T(8,128)(2,1)S(1)} collective-permute-done((bf16[128,8,128]{2,1,0:T(8,128)(2,1)S(1)}, bf16[128,8,128]{2,1,0:T(8,128)(2,1)S(1)}, u32[]{:S(2)}, u32[]{:S(2)}) %collective-permute-start.9) | collective-permute-done | bytes 262176 | tf_op jit(solution)/shard_map/ppermute | solution.py:27
  87.2 1.0 down.1
  88.2 6.3 %all-to-all-start.4 = ((bf16[128,8,128]{2,1,0:T(8,128)(2,1)}), bf16[128,8,128]{2,1,0:T(8,128)(2,1)S(1)}, u32[]{:S(2)}, u32[]{:S(2)}) async-start(bf16[128,8,128]{2,1,0:T(8,128)(2,1)} %down.1), calls=%async_computation.4 | async-start | bytes 524288 | tf_op jit(solution)/shard_map/all_to_all | solution.py:19
  94.6 2.5 %collective-permute-start.10 = (bf16[4,256]{1,0:T(4,128)(2,1)S(1)}, bf16[4,256]{1,0:T(4,128)(2,1)S(1)}, u32[]{:S(2)}, u32[]{:S(2)}) collective-permute-start(bf16[4,256]{1,0:T(4,128)(2,1)S(1)} %get-tuple-element.31), channel_id=1, source_target_pairs={{0,32},{1,225},{32,64},{33,1},{64,96},{65,33},{96,128},{97,65},{12... | collective-permute-start | bytes 6152 | tf_op jit(solution)/shard_map/ppermute | solution.py:39
  97.1 1.9 %collective-permute-start.11 = (bf16[4,256]{1,0:T(4,128)(2,1)S(1)}, bf16[4,256]{1,0:T(4,128)(2,1)S(1)}, u32[]{:S(2)}, u32[]{:S(2)}) collective-permute-start(bf16[4,256]{1,0:T(4,128)(2,1)S(1)} %get-tuple-element.32), channel_id=1, source_target_pairs={{0,64},{1,193},{32,96},{33,225},{64,128},{65,1},{96,160},{97,33},{... | collective-permute-start | bytes 6152 | tf_op jit(solution)/shard_map/ppermute | solution.py:39
  99.0 0.9 collective-permute-start.12
  99.8 3.7 %collective-permute-start.13 = (bf16[4,256]{1,0:T(4,128)(2,1)S(1)}, bf16[4,256]{1,0:T(4,128)(2,1)S(1)}, u32[]{:S(2)}, u32[]{:S(2)}) collective-permute-start(bf16[4,256]{1,0:T(4,128)(2,1)S(1)} %get-tuple-element.34), channel_id=1, source_target_pairs={{0,128},{1,129},{32,160},{33,161},{64,192},{65,193},{96,224},{97,2... | collective-permute-start | bytes 6152 | tf_op jit(solution)/shard_map/ppermute | solution.py:39
  103.6 1.7 %collective-permute-start.14 = (bf16[4,256]{1,0:T(4,128)(2,1)S(1)}, bf16[4,256]{1,0:T(4,128)(2,1)S(1)}, u32[]{:S(2)}, u32[]{:S(2)}) collective-permute-start(bf16[4,256]{1,0:T(4,128)(2,1)S(1)} %collective-permute-done.12.refs_3_), channel_id=1, source_target_pairs={{0,1},{1,0},{2,3},{3,2},{4,5},{5,4},{6,7},{7,6},{8,9},{9,8},{10,11... | collective-permute-start | bytes 6152 | tf_op jit(solution)/shard_map/ppermute | solution.py:27
  105.3 0.5 collective-permute-start.16
  106.8 1.8 %all-to-all-done.4.returned_ref = bf16[128,8,128]{2,1,0:T(8,128)(2,1)S(1)} async-done(((bf16[128,8,128]{2,1,0:T(8,128)(2,1)}), bf16[128,8,128]{2,1,0:T(8,128)(2,1)S(1)}, u32[]{:S(2)}, u32[]{:S(2)}) %all-to-all-start.4) | async-done | bytes 262176 | tf_op jit(solution)/shard_map/all_to_all | solution.py:19
  108.7 0.6 combine.1
  109.3 2.1 %collective-permute-start.17 = (f32[8,128]{1,0:T(8,128)S(1)}, f32[8,128]{1,0:T(8,128)S(1)}, u32[]{:S(2)}, u32[]{:S(2)}) collective-permute-start(f32[8,128]{1,0:T(8,128)S(1)} %get-tuple-element.36.own_ref), channel_id=1, source_target_pairs={{0,1},{1,0},{2,3},{3,2},{4,5},{5,4},{6,7},{7,6},{8,9},{9,8},{10,11... | collective-permute-start | bytes 12296 | tf_op jit(solution)/shard_map/ppermute | solution.py:27
  111.4 0.8 collective-permute-done.17.other_ref
  112.2 0.6 finish.1
  (63 shorter events, 3.5 us)
Async XLA Ops:
  0.0 9.9 %copy-start.8 = (s32[4]{0:T(128)S(1)}, s32[4]{0:T(128)}, u32[]{:S(2)}) copy-start(s32[4]{0:T(128)} %group_ref.1) | copy-start | bytes 52
  0.0 9.9 %copy-start.4 = (bf16[4,2048]{1,0:T(4,128)(2,1)S(1)}, bf16[4,2048]{1,0:T(4,128)(2,1)}, u32[]{:S(2)}) copy-start(bf16[4,2048]{1,0:T(4,128)(2,1)} %tokens_ref.1) | copy-start | bytes 49156
  1.9 40.4 %copy-start.1 = (bf16[4,1024,256]{2,1,0:T(8,128)(2,1)S(1)}, bf16[4,1024,256]{2,1,0:T(8,128)(2,1)}, u32[]{:S(2)}) copy-start(bf16[4,1024,256]{2,1,0:T(8,128)(2,1)} %keys_ref.1) | copy-start | bytes 6291460
  2.0 40.4 %copy-start.7 = (f32[256]{0:T(256)S(1)}, f32[256]{0:T(256)}, u32[]{:S(2)}) copy-start(f32[256]{0:T(256)} %param.29) | copy-start | bytes 3076
  2.0 40.4 %copy-start.9 = (s32[4]{0:T(128)S(1)}, s32[4]{0:T(128)}, u32[]{:S(2)}) copy-start(s32[4]{0:T(128)} %lengths_ref.1) | copy-start | bytes 52
  2.0 40.4 %copy-start.10 = (f32[3]{0:T(128)S(1)}, f32[3]{0:T(128)}, u32[]{:S(2)}) copy-start(f32[3]{0:T(128)} %lambda_ref.1) | copy-start | bytes 40
  2.0 23.8 %all-to-all-start = ((bf16[16,16,2048]{2,1,0:T(8,128)(2,1)}), bf16[16,16,2048]{2,1,0:T(8,128)(2,1)S(1)}, u32[]{:S(2)}, u32[]{:S(2)}) async-start(bf16[16,16,2048]{2,1,0:T(8,128)(2,1)} %broadcast_in_dim.2), calls=%async_computation | async-start | bytes 2097152 | tf_op jit(solution)/shard_map/all_to_all | solution.py:19
  10.6 11.8 %collective-permute-start.2 = (bf16[4,512]{1,0:T(4,128)(2,1)S(1)}, bf16[4,512]{1,0:T(4,128)(2,1)S(1)}, u32[]{:S(2)}, u32[]{:S(2)}) collective-permute-start(bf16[4,512]{1,0:T(4,128)(2,1)S(1)} %get-tuple-element.24), channel_id=1, source_target_pairs={{0,96},{1,161},{32,128},{33,193},{64,160},{65,225},{96,192},{97,1}... | collective-permute-start | bytes 12296 | tf_op jit(solution)/shard_map/ppermute | solution.py:39
  17.2 5.2 %collective-permute-start.1 = (bf16[4,512]{1,0:T(4,128)(2,1)S(1)}, bf16[4,512]{1,0:T(4,128)(2,1)S(1)}, u32[]{:S(2)}, u32[]{:S(2)}) collective-permute-start(bf16[4,512]{1,0:T(4,128)(2,1)S(1)} %get-tuple-element.23), channel_id=1, source_target_pairs={{0,64},{1,193},{32,96},{33,225},{64,128},{65,1},{96,160},{97,33},{... | collective-permute-start | bytes 12296 | tf_op jit(solution)/shard_map/ppermute | solution.py:39
  17.5 5.5 %collective-permute-start = (bf16[4,512]{1,0:T(4,128)(2,1)S(1)}, bf16[4,512]{1,0:T(4,128)(2,1)S(1)}, u32[]{:S(2)}, u32[]{:S(2)}) collective-permute-start(bf16[4,512]{1,0:T(4,128)(2,1)S(1)} %get-tuple-element.22), channel_id=1, source_target_pairs={{0,32},{1,225},{32,64},{33,1},{64,96},{65,33},{96,128},{97,65},{12... | collective-permute-start | bytes 12296 | tf_op jit(solution)/shard_map/ppermute | solution.py:39
  17.9 6.8 %collective-permute-start.3 = (bf16[4,512]{1,0:T(4,128)(2,1)S(1)}, bf16[4,512]{1,0:T(4,128)(2,1)S(1)}, u32[]{:S(2)}, u32[]{:S(2)}) collective-permute-start(bf16[4,512]{1,0:T(4,128)(2,1)S(1)} %get-tuple-element.25), channel_id=1, source_target_pairs={{0,128},{1,129},{32,160},{33,161},{64,192},{65,193},{96,224},{97,2... | collective-permute-start | bytes 12296 | tf_op jit(solution)/shard_map/ppermute | solution.py:39
  22.4 2.3 %collective-permute-start.4 = (bf16[4,512]{1,0:T(4,128)(2,1)S(1)}, bf16[4,512]{1,0:T(4,128)(2,1)S(1)}, u32[]{:S(2)}, u32[]{:S(2)}) collective-permute-start(bf16[4,512]{1,0:T(4,128)(2,1)S(1)} %collective-permute-done.2.refs_3_), channel_id=1, source_target_pairs={{0,1},{1,0},{2,3},{3,2},{4,5},{5,4},{6,7},{7,6},{8,9},{9,8},{10,11... | collective-permute-start | bytes 12296 | tf_op jit(solution)/shard_map/ppermute | solution.py:27
  22.4 2.3 %collective-permute-start.5 = (bf16[4,512]{1,0:T(4,128)(2,1)S(1)}, bf16[4,512]{1,0:T(4,128)(2,1)S(1)}, u32[]{:S(2)}, u32[]{:S(2)}) collective-permute-start(bf16[4,512]{1,0:T(4,128)(2,1)S(1)} %collective-permute-done.1.refs_2_), channel_id=1, source_target_pairs={{0,1},{1,0},{2,3},{3,2},{4,5},{5,4},{6,7},{7,6},{8,9},{9,8},{10,11... | collective-permute-start | bytes 12296 | tf_op jit(solution)/shard_map/ppermute | solution.py:27
  22.9 2.6 %collective-permute-start.6 = (bf16[4,512]{1,0:T(4,128)(2,1)S(1)}, bf16[4,512]{1,0:T(4,128)(2,1)S(1)}, u32[]{:S(2)}, u32[]{:S(2)}) collective-permute-start(bf16[4,512]{1,0:T(4,128)(2,1)S(1)} %collective-permute-done.refs_1_), channel_id=1, source_target_pairs={{0,1},{1,0},{2,3},{3,2},{4,5},{5,4},{6,7},{7,6},{8,9},{9,8},{10,11... | collective-permute-start | bytes 12296 | tf_op jit(solution)/shard_map/ppermute | solution.py:27
  45.2 39.0 %copy-start = (bf16[1,256,2048]{2,1,0:T(8,128)(2,1)S(1)}, bf16[1,256,2048]{2,1,0:T(8,128)(2,1)}, u32[]{:S(2)}) copy-start(bf16[1,256,2048]{2,1,0:T(8,128)(2,1)} %param.38) | copy-start | bytes 3145732
  45.3 39.0 %copy-start.2 = (bf16[1,2048,256]{2,1,0:T(8,128)(2,1)S(1)}, bf16[1,2048,256]{2,1,0:T(8,128)(2,1)}, u32[]{:S(2)}) copy-start(bf16[1,2048,256]{2,1,0:T(8,128)(2,1)} %param.36) | copy-start | bytes 3145732
  45.3 39.0 %copy-start.3 = (f32[2048]{0:T(1024)S(1)}, f32[2048]{0:T(1024)}, u32[]{:S(2)}) copy-start(f32[2048]{0:T(1024)} %param.31) | copy-start | bytes 24580
  55.1 6.0 %collective-permute-start.7 = (f32[4,8,256]{2,1,0:T(8,128)S(1)}, f32[4,8,256]{2,1,0:T(8,128)S(1)}, u32[]{:S(2)}, u32[]{:S(2)}) collective-permute-start(f32[4,8,256]{2,1,0:T(8,128)S(1)} %outproj.1.own_ref), channel_id=1, source_target_pairs={{0,1},{1,0},{2,3},{3,2},{4,5},{5,4},{6,7},{7,6},{8,9},{9,8},{10,11... | collective-permute-start | bytes 98312 | tf_op jit(solution)/shard_map/ppermute | solution.py:27
  80.9 3.4 %collective-permute-start.8 = (bf16[128,8,128]{2,1,0:T(8,128)(2,1)S(1)}, bf16[128,8,128]{2,1,0:T(8,128)(2,1)S(1)}, u32[]{:S(2)}, u32[]{:S(2)}) collective-permute-start(bf16[128,8,128]{2,1,0:T(8,128)(2,1)S(1)} %all_to_all.27.own_ref), channel_id=1, source_target_pairs={{0,1},{1,0},{2,3},{3,2},{4,5},{5,4},{6,7},{7,6},{8,9},{9,8},{10,11... | collective-permute-start | bytes 786440 | tf_op jit(solution)/shard_map/ppermute | solution.py:27
  84.3 21.5 %copy-start.12 = (f32[4,2]{0,1:T(2,128)S(1)}, f32[4,2]{0,1:T(2,128)}, u32[]{:S(2)}) copy-start(f32[4,2]{0,1:T(2,128)} %param.35) | copy-start | bytes 100
  84.3 21.4 %copy-start.13 = (f32[4]{0:T(128)S(1)}, f32[4]{0:T(128)}, u32[]{:S(2)}) copy-start(f32[4]{0:T(128)} %param.34) | copy-start | bytes 52
  85.5 26.7 %copy-start.6 = (f32[1024]{0:T(1024)S(1)}, f32[1024]{0:T(1024)}, u32[]{:S(2)}) copy-start(f32[1024]{0:T(1024)} %param.39) | copy-start | bytes 12292
  85.6 1.6 %collective-permute-start.9 = (bf16[128,8,128]{2,1,0:T(8,128)(2,1)S(1)}, bf16[128,8,128]{2,1,0:T(8,128)(2,1)S(1)}, u32[]{:S(2)}, u32[]{:S(2)}) collective-permute-start(bf16[128,8,128]{2,1,0:T(8,128)(2,1)S(1)} %get-tuple-element.28), channel_id=1, source_target_pairs={{0,1},{1,0},{2,3},{3,2},{4,5},{5,4},{6,7},{7,6},{8,9},{9,8},{10,11... | collective-permute-start | bytes 786440 | tf_op jit(solution)/shard_map/ppermute | solution.py:27
  88.2 20.4 %all-to-all-start.4 = ((bf16[128,8,128]{2,1,0:T(8,128)(2,1)}), bf16[128,8,128]{2,1,0:T(8,128)(2,1)S(1)}, u32[]{:S(2)}, u32[]{:S(2)}) async-start(bf16[128,8,128]{2,1,0:T(8,128)(2,1)} %down.1), calls=%async_computation.4 | async-start | bytes 524288 | tf_op jit(solution)/shard_map/all_to_all | solution.py:19
  94.6 10.7 %collective-permute-start.10 = (bf16[4,256]{1,0:T(4,128)(2,1)S(1)}, bf16[4,256]{1,0:T(4,128)(2,1)S(1)}, u32[]{:S(2)}, u32[]{:S(2)}) collective-permute-start(bf16[4,256]{1,0:T(4,128)(2,1)S(1)} %get-tuple-element.31), channel_id=1, source_target_pairs={{0,32},{1,225},{32,64},{33,1},{64,96},{65,33},{96,128},{97,65},{12... | collective-permute-start | bytes 6152 | tf_op jit(solution)/shard_map/ppermute | solution.py:39
  97.1 8.1 %collective-permute-start.11 = (bf16[4,256]{1,0:T(4,128)(2,1)S(1)}, bf16[4,256]{1,0:T(4,128)(2,1)S(1)}, u32[]{:S(2)}, u32[]{:S(2)}) collective-permute-start(bf16[4,256]{1,0:T(4,128)(2,1)S(1)} %get-tuple-element.32), channel_id=1, source_target_pairs={{0,64},{1,193},{32,96},{33,225},{64,128},{65,1},{96,160},{97,33},{... | collective-permute-start | bytes 6152 | tf_op jit(solution)/shard_map/ppermute | solution.py:39
  99.0 4.6 %collective-permute-start.12 = (bf16[4,256]{1,0:T(4,128)(2,1)S(1)}, bf16[4,256]{1,0:T(4,128)(2,1)S(1)}, u32[]{:S(2)}, u32[]{:S(2)}) collective-permute-start(bf16[4,256]{1,0:T(4,128)(2,1)S(1)} %get-tuple-element.33), channel_id=1, source_target_pairs={{0,96},{1,161},{32,128},{33,193},{64,160},{65,225},{96,192},{97,1}... | collective-permute-start | bytes 6152 | tf_op jit(solution)/shard_map/ppermute | solution.py:39
  99.8 6.6 %collective-permute-start.13 = (bf16[4,256]{1,0:T(4,128)(2,1)S(1)}, bf16[4,256]{1,0:T(4,128)(2,1)S(1)}, u32[]{:S(2)}, u32[]{:S(2)}) collective-permute-start(bf16[4,256]{1,0:T(4,128)(2,1)S(1)} %get-tuple-element.34), channel_id=1, source_target_pairs={{0,128},{1,129},{32,160},{33,161},{64,192},{65,193},{96,224},{97,2... | collective-permute-start | bytes 6152 | tf_op jit(solution)/shard_map/ppermute | solution.py:39
  103.6 2.9 %collective-permute-start.14 = (bf16[4,256]{1,0:T(4,128)(2,1)S(1)}, bf16[4,256]{1,0:T(4,128)(2,1)S(1)}, u32[]{:S(2)}, u32[]{:S(2)}) collective-permute-start(bf16[4,256]{1,0:T(4,128)(2,1)S(1)} %collective-permute-done.12.refs_3_), channel_id=1, source_target_pairs={{0,1},{1,0},{2,3},{3,2},{4,5},{5,4},{6,7},{7,6},{8,9},{9,8},{10,11... | collective-permute-start | bytes 6152 | tf_op jit(solution)/shard_map/ppermute | solution.py:27
  105.3 1.2 %collective-permute-start.15 = (bf16[4,256]{1,0:T(4,128)(2,1)S(1)}, bf16[4,256]{1,0:T(4,128)(2,1)S(1)}, u32[]{:S(2)}, u32[]{:S(2)}) collective-permute-start(bf16[4,256]{1,0:T(4,128)(2,1)S(1)} %collective-permute-done.11.refs_2_), channel_id=1, source_target_pairs={{0,1},{1,0},{2,3},{3,2},{4,5},{5,4},{6,7},{7,6},{8,9},{9,8},{10,11... | collective-permute-start | bytes 6152 | tf_op jit(solution)/shard_map/ppermute | solution.py:27
  105.3 1.3 %collective-permute-start.16 = (bf16[4,256]{1,0:T(4,128)(2,1)S(1)}, bf16[4,256]{1,0:T(4,128)(2,1)S(1)}, u32[]{:S(2)}, u32[]{:S(2)}) collective-permute-start(bf16[4,256]{1,0:T(4,128)(2,1)S(1)} %collective-permute-done.10.refs_1_), channel_id=1, source_target_pairs={{0,1},{1,0},{2,3},{3,2},{4,5},{5,4},{6,7},{7,6},{8,9},{9,8},{10,11... | collective-permute-start | bytes 6152 | tf_op jit(solution)/shard_map/ppermute | solution.py:27
  109.3 2.9 %collective-permute-start.17 = (f32[8,128]{1,0:T(8,128)S(1)}, f32[8,128]{1,0:T(8,128)S(1)}, u32[]{:S(2)}, u32[]{:S(2)}) collective-permute-start(f32[8,128]{1,0:T(8,128)S(1)} %get-tuple-element.36.own_ref), channel_id=1, source_target_pairs={{0,1},{1,0},{2,3},{3,2},{4,5},{5,4},{6,7},{7,6},{8,9},{9,8},{10,11... | collective-permute-start | bytes 12296 | tf_op jit(solution)/shard_map/ppermute | solution.py:27
  (2 other events, 19.6 us)
